TPU v7x, 32 devices: a whole 2x2x4 slice. The times are simulated.
32 devices in a mesh: ep: 8 (over z, core), tp: 4 (over y, x).
Axes of the slice: x: 2, y: 2, z: 4, core: 2. Of those that a mesh axis runs over, the one named last changes fastest.
Arguments:
- tokens: bfloat16 [512, 2048], P('ep'), may hold values from -6 to 6
- mix_gain: float32 [2048], replicated, may hold values from 0.1 to 1.9
- w_in: bfloat16 [2048, 1024], P(None, 'tp'), may hold values from -0.125 to 0.125
- decay_re: float32 [64, 64], P('tp'), may hold values from -1 to -0.1
- freq: float32 [64, 64], P('tp'), may hold values from 0 to 100
- log_step: float32 [64], P('tp'), may hold values from -3.9 to 0
- in_re: bfloat16 [64, 16, 64], P('tp'), may hold values from -1 to 1
- in_im: bfloat16 [64, 16, 64], P('tp'), may hold values from -1 to 1
- out_re: bfloat16 [64, 16, 64], P('tp'), may hold values from -0.75 to 0.75
- out_im: bfloat16 [64, 16, 64], P('tp'), may hold values from -0.75 to 0.75
- skip: float32 [64, 16], P('tp'), may hold values from -4 to 4
- state_re: float32 [512, 64, 64], P('ep', 'tp'), may hold values from -6 to 6
- state_im: float32 [512, 64, 64], P('ep', 'tp'), may hold values from -6 to 6
- glu_weight: bfloat16 [1024, 1024], P(None, 'tp'), may hold values from -0.1875 to 0.1875
- glu_bias: float32 [1024], P('tp'), may hold values from -4 to 4
- out_weight: bfloat16 [1024, 2048], P('tp'), may hold values from -0.1875 to 0.1875
- ffn_gain: float32 [2048], replicated, may hold values from 0.1 to 1.9
- route: int32 [512, 2], P('ep'), may hold values from 0 to 7, all different within a row; in each aligned block of 64 rows (0 to 63, 64 to 127, ...) at most 24 rows name the same one
- route_weight: float32 [512, 2], P('ep'), may hold values from 0.2 to 1
- expert_gate: bfloat16 [8, 2048, 3584], P('ep', None, 'tp'), may hold values from -0.125 to 0.125
- expert_up: bfloat16 [8, 2048, 3584], P('ep', None, 'tp'), may hold values from -0.125 to 0.125
- expert_down: bfloat16 [8, 3584, 2048], P('ep', 'tp'), may hold values from -0.09375 to 0.09375
Outputs:
- mixed: bfloat16 [512, 2048], P('ep', 'tp')
- new_re: float32 [512, 64, 64], P('ep', 'tp')
- new_im: float32 [512, 64, 64], P('ep', 'tp')
Inputs may be any that keep to these rules, and one draw needn't show every extreme that they name: `route`: each row names 2 different experts. Within the 64 rows of one index of ep no expert is named more than 24 times, and in every draw some expert is named exactly 24 times by the rows of some index of ep.
All inputs are finite; a program needn't handle non-finite values.
Results may differ from a plain program's by a relative error of at most 0.015.
Values may be sent and summed in bfloat16 or wider, within the bound.
No kernel may reach another device: no remote copies, remote signals or barrier semaphores. Data moves between devices by JAX's collectives and lax.ppermute only.
A program may use at most 64 MiB of HBM per device.

v0:
```python
import jax
import jax.numpy as jnp
from jax import lax
from jax.sharding import PartitionSpec as P

norm_eps = 1e-06


def rms_scale(rows, gain):
    values = rows.astype(jnp.float32)
    scaled = values * lax.rsqrt(jnp.mean(values * values, axis=-1, keepdims=True) + norm_eps)
    return (scaled * gain).astype(jnp.bfloat16)


def state_step(
    inputs, state_re, state_im, decay_re, freq, log_step, in_re, in_im, out_re, out_im, skip
):
    highest = lax.Precision.HIGHEST
    step = jnp.exp(log_step)[:, None]
    magnitude = jnp.exp(decay_re * step)
    turn_re = magnitude * jnp.cos(freq * step)
    turn_im = magnitude * jnp.sin(freq * step)
    denom = decay_re * decay_re + freq * freq
    coef_re = ((turn_re - 1.0) * decay_re + turn_im * freq) / denom
    coef_im = (turn_im * decay_re - (turn_re - 1.0) * freq) / denom
    drive_re = jnp.einsum("sgh,ghp->sgp", inputs, in_re, preferred_element_type=jnp.float32)
    drive_im = jnp.einsum("sgh,ghp->sgp", inputs, in_im, preferred_element_type=jnp.float32)
    push_re = coef_re * drive_re - coef_im * drive_im
    push_im = coef_re * drive_im + coef_im * drive_re
    new_re = turn_re * state_re - turn_im * state_im + push_re
    new_im = turn_re * state_im + turn_im * state_re + push_im
    read = jnp.einsum("ghp,sgp->sgh", out_re.astype(jnp.float32), new_re, precision=highest)
    read = read - jnp.einsum("ghp,sgp->sgh", out_im.astype(jnp.float32), new_im, precision=highest)
    read = read + skip * inputs.astype(jnp.float32)
    return (read, new_re, new_im)


def local(
    tokens,
    mix_gain,
    w_in,
    decay_re,
    freq,
    log_step,
    in_re,
    in_im,
    out_re,
    out_im,
    skip,
    state_re,
    state_im,
    glu_weight,
    glu_bias,
    out_weight,
    ffn_gain,
    route,
    route_weight,
    expert_gate,
    expert_up,
    expert_down,
):
    seq_count = tokens.shape[0]
    groups_local = decay_re.shape[0]
    model_width = tokens.shape[1]
    local_width = model_width // lax.axis_size("tp")
    experts = lax.axis_size("ep")
    top_count = route.shape[1]
    slot_cap = (3 * seq_count * top_count + 2 * experts - 1) // (2 * experts)
    col_start = lax.axis_index("tp") * local_width
    normed = rms_scale(tokens, mix_gain)
    drive = jnp.dot(normed, w_in, preferred_element_type=jnp.float32).astype(jnp.bfloat16)
    inputs = drive.reshape(seq_count, groups_local, -1)
    read, new_re, new_im = state_step(
        inputs, state_re, state_im, decay_re, freq, log_step, in_re, in_im, out_re, out_im, skip
    )
    mixed_in = jax.nn.gelu(read).reshape(seq_count, -1).astype(jnp.bfloat16)
    gate = jnp.dot(
        lax.all_gather(mixed_in, "tp", axis=1, tiled=True),
        glu_weight,
        preferred_element_type=jnp.float32,
    )
    gated = (mixed_in.astype(jnp.float32) * jax.nn.sigmoid(gate + glu_bias)).astype(jnp.bfloat16)
    partial_value = jnp.dot(gated, out_weight, preferred_element_type=jnp.float32)
    mix_part = lax.psum_scatter(
        partial_value.astype(jnp.bfloat16), "tp", scatter_dimension=1, tiled=True
    ).astype(jnp.float32)
    token_part = lax.dynamic_slice_in_dim(tokens, col_start, local_width, 1)
    resid_part = (token_part.astype(jnp.float32) + mix_part).astype(jnp.bfloat16)
    part_values = resid_part.astype(jnp.float32)
    squares = lax.psum(jnp.sum(part_values * part_values, axis=1), "tp")
    row_scale = lax.rsqrt(squares / model_width + norm_eps)
    gain_part = lax.dynamic_slice_in_dim(ffn_gain, col_start, local_width, 0)
    own_cols = (part_values * row_scale[:, None] * gain_part).astype(jnp.bfloat16)
    flat_route = route.reshape(-1)
    hits = (flat_route[:, None] == jnp.arange(experts)[None, :]).astype(jnp.int32)
    rank = jnp.sum((jnp.cumsum(hits, axis=0) - hits) * hits, axis=1)
    slot = flat_route * slot_cap + rank
    slot_ids = jnp.arange(experts * slot_cap)
    picks = (slot[None, :] == slot_ids[:, None]).reshape(experts * slot_cap, seq_count, top_count)
    select = jnp.any(picks, axis=2).astype(jnp.bfloat16)
    combine = jnp.einsum("ask,sk->sa", picks.astype(jnp.float32), route_weight)
    gate_local = expert_gate[0]
    up_local = expert_up[0]
    down_local = expert_down[0]
    normed2 = lax.all_gather(own_cols, "tp", axis=1, tiled=True)
    outbound = jnp.dot(select, normed2, preferred_element_type=jnp.float32).astype(jnp.bfloat16)
    arrived = lax.all_to_all(
        outbound.reshape(experts, slot_cap, model_width),
        "ep",
        split_axis=0,
        concat_axis=0,
        tiled=True,
    )
    arrived = arrived.reshape(experts * slot_cap, model_width)
    gate_rows = jnp.dot(arrived, gate_local, preferred_element_type=jnp.float32)
    up_rows = jnp.dot(arrived, up_local, preferred_element_type=jnp.float32)
    hidden = (jax.nn.silu(gate_rows) * up_rows).astype(jnp.bfloat16)
    back_rows = lax.psum_scatter(
        lax.dot_general(
            down_local, hidden, (((0,), (1,)), ((), ())), preferred_element_type=jnp.float32
        ).astype(jnp.bfloat16),
        "tp",
        scatter_dimension=0,
        tiled=True,
    ).astype(jnp.float32)
    back_rows = back_rows.astype(jnp.bfloat16).reshape(local_width, experts, slot_cap)
    returned = lax.all_to_all(back_rows, "ep", split_axis=1, concat_axis=1, tiled=True)
    returned = returned.reshape(local_width, experts * slot_cap).astype(jnp.float32)
    expert_total = lax.dot_general(
        combine, returned, (((1,), (1,)), ((), ())), precision=lax.Precision.HIGHEST
    )
    mixed = (resid_part.astype(jnp.float32) + expert_total).astype(jnp.bfloat16)
    return (mixed, new_re, new_im)


def solution(mesh):
    in_specs = (
        P("ep", None),
        P(),
        P(None, "tp"),
        P("tp", None),
        P("tp", None),
        P("tp"),
        P("tp", None, None),
        P("tp", None, None),
        P("tp", None, None),
        P("tp", None, None),
        P("tp", None),
        P("ep", "tp", None),
        P("ep", "tp", None),
        P(None, "tp"),
        P("tp"),
        P("tp", None),
        P(),
        P("ep", None),
        P("ep", None),
        P("ep", None, "tp"),
        P("ep", None, "tp"),
        P("ep", "tp", None),
    )
    out_specs = (P("ep", "tp"), P("ep", "tp", None), P("ep", "tp", None))
    return jax.shard_map(local, mesh=mesh, in_specs=in_specs, out_specs=out_specs, check_vma=False)
```

profile of v0, /device:TPU:0, one launch (start us, length us, event | category | flops | bytes accessed | tf_op | source)
XLA Modules:
  0.0 152.2 jit_solution(17979574548107421040)
XLA Ops:
  7.2 0.0 copy-start
  7.2 0.0 reduce-scatter.3.cloned.1.call-start
  7.3 0.8 exp.13
  8.0 1.1 fusion.34
  9.2 1.7 %convolution_convert_fusion.2 = bf16[64,256]{1,0:T(8,128)(2,1)S(1)} fusion(bf16[2048,256]{1,0:T(8,128)(2,1)} %param.24, bf16[64,2048]{1,0:T(8,128)(2,1)} %param.22, f32[2048]{0:T(1024)} %param.23, f32[64]{0:T(128)S(1)} %add_rsqrt_fusion.1), kind=kOutput, calls=%fused_computation.24 | convolution fusion | flops 67649536 | bytes 1351936 | tf_op jit(solution)/shard_map/dot_general | solution.py:71
  10.8 0.1 copy.61
  11.0 1.1 fusion.64
  12.1 0.0 copy-start.5
  12.1 0.8 cosine_multiply_fusion
  12.9 1.8 %bitcast_add_fusion = (f32[64,16,64]{2,0,1:T(8,128)S(1)}, f32[64,16,64]{2,0,1:T(8,128)S(1)}) fusion(f32[16,64,64]{2,1,0:T(8,128)S(1)} %fusion.64, f32[64,16,64]{2,1,0:T(8,128)} %param.34, f32[64,16,64]{2,1,0:T(8,128)} %param.33, f32[16,64]{1,0:T(8,128)S(1)} %get-tuple-element.21, f32[16,64]{1,0:T(8,128)S(1)} %get-tuple-element.22, ...), kind=kOutput, calls=%fused_computation.35 | convolution fusion | flops 3014656 | bytes 1392640 | tf_op jit(solution)/shard_map/sgh,ghp->sgp/dot_general | solution.py:26
  14.7 0.0 copy-done.2
  14.7 0.5 fusion.65
  15.2 0.5 fusion.50
  15.8 10.5 %all_gather.6 = bf16[64,1024]{0,1:T(8,128)(2,1)S(1)} all-gather(bf16[64,256]{0,1:T(8,128)(2,1)S(1)} %bitcast.68), channel_id=1, replica_groups=mesh['ep'=8,'tp'=4] {'tp'}, dimensions={1}, use_global_device_ids=true | all-gather | bytes 163840 | tf_op jit(solution)/shard_map/all_gather | solution.py:78
  26.3 0.1 copy.64
  26.4 0.0 copy-done
  26.4 0.0 copy-done.1
  26.4 0.0 copy-done.6
  26.4 1.3 convolution_convert_fusion.1
  27.7 0.0 reduce-scatter.3.cloned.1.call-update
  27.8 0.0 reduce-scatter.5.cloned.1.call-start
  27.8 0.1 copy.65
  27.9 0.1 eq.29
  28.1 0.1 fusion.56
  28.2 0.2 reduce_window_sum.11
  28.3 0.2 select_reduce_fusion
  28.5 0.1 reduce_sum.31
  28.6 0.1 copy.66
  28.7 0.8 dynamic_slice.7
  29.5 0.1 iota_compare_fusion
  29.6 22.9 %reduce-scatter.3.cloned.1.call-done = bf16[64,512]{1,0:T(8,128)(2,1)} async-done(((bf16[64,2048]{1,0:T(8,128)(2,1)}), bf16[64,512]{1,0:T(8,128)(2,1)}) %reduce-scatter.3.cloned.1.call-update) | async-done | bytes 65552 | tf_op jit(solution)/shard_map/reduce_scatter | solution.py:84
  52.5 1.0 fusion.51
  53.5 8.9 %psum.7 = f32[64]{0:T(128)S(1)} all-reduce(f32[64]{0:T(128)S(1)} %get-tuple-element.15), channel_id=1, replica_groups=mesh['ep'=8,'tp'=4] {'tp'}, use_global_device_ids=true, to_apply=%region_6.7 | all-reduce | flops 64 | bytes 512 | tf_op jit(solution)/shard_map/psum | solution.py:90
  62.5 0.1 fusion.53
  62.6 8.9 %all_gather.7 = bf16[64,2048]{1,0:T(8,128)(2,1)S(1)} all-gather(bf16[64,512]{1,0:T(8,128)(2,1)S(1)} %fusion.53), channel_id=1, replica_groups=mesh['ep'=8,'tp'=4] {'tp'}, dimensions={1}, use_global_device_ids=true | all-gather | bytes 327680 | tf_op jit(solution)/shard_map/all_gather | solution.py:105
  71.5 0.4 convolution_convert_fusion
  71.9 25.4 %all_to_all.10 = bf16[8,24,2048]{2,1,0:T(8,128)(2,1)S(1)} all-to-all(bf16[8,24,2048]{2,1,0:T(8,128)(2,1)S(1)} %bitcast.63), channel_id=1, replica_groups=mesh['ep'=8,'tp'=4] {'ep'}, dimensions={0} | all-to-all | bytes 1572864 | tf_op jit(solution)/shard_map/all_to_all | solution.py:107
  97.3 3.9 %fusion.4 = f32[192,896]{1,0:T(8,128)} fusion(bf16[192,2048]{1,0:T(8,128)(2,1)S(1)} %bitcast.61, bf16[1,2048,896]{2,1,0:T(8,128)(2,1)} %param.41), kind=kOutput, calls=%fused_computation.4 | convolution fusion | flops 704643072 | bytes 5144576 | tf_op jit(solution)/shard_map/dot_general | solution.py:115
  101.2 6.1 %fusion.9 = bf16[2048,192]{0,1:T(8,128)(2,1)} fusion(bf16[1,896,2048]{2,1,0:T(8,128)(2,1)} %param.43, bf16[192,2048]{1,0:T(8,128)(2,1)S(1)} %bitcast.62, bf16[1,2048,896]{2,1,0:T(8,128)(2,1)} %param.42, f32[192,896]{1,0:T(8,128)} %fusion.4), kind=kOutput, calls=%fused_computation.8 | convolution fusion | flops 1410711552 | bytes 9601024 | tf_op jit(solution)/shard_map/dot_general | solution.py:119
  107.3 0.0 reduce-scatter.5.cloned.1.call-update
  107.3 24.3 %reduce-scatter.5.cloned.1.call-done = bf16[512,192]{0,1:T(8,128)(2,1)} async-done(((bf16[2048,192]{0,1:T(8,128)(2,1)}), bf16[512,192]{0,1:T(8,128)(2,1)}) %reduce-scatter.5.cloned.1.call-update) | async-done | bytes 196624 | tf_op jit(solution)/shard_map/reduce_scatter | solution.py:118
  131.6 4.6 %all-to-all-start.1 = ((bf16[512,8,24]{0,2,1:T(8,128)(2,1)}), bf16[512,8,24]{0,2,1:T(8,128)(2,1)S(1)}, u32[]{:S(2)}, u32[]{:S(2)}) async-start(bf16[512,8,24]{0,2,1:T(8,128)(2,1)} %bitcast.70), calls=%async_computation.3 | async-start | bytes 393216 | tf_op jit(solution)/shard_map/all_to_all | solution.py:127
  136.2 1.1 copy.67
  137.3 1.1 copy.68
  138.4 0.1 copy.70
  138.5 0.2 fusion.41
  138.7 5.7 %all-to-all-done.1 = bf16[512,8,24]{0,2,1:T(8,128)(2,1)S(1)} async-done(((bf16[512,8,24]{0,2,1:T(8,128)(2,1)}), bf16[512,8,24]{0,2,1:T(8,128)(2,1)S(1)}, u32[]{:S(2)}, u32[]{:S(2)}) %all-to-all-start.1) | async-done | bytes 196640 | tf_op jit(solution)/shard_map/all_to_all | solution.py:127
  144.5 0.9 fusion.20
  (13 shorter events, 0.0 us)
Async XLA Ops:
  7.2 19.2 %copy-start = (bf16[256,2048]{1,0:T(8,128)(2,1)S(1)}, bf16[256,2048]{1,0:T(8,128)(2,1)}, u32[]{:S(2)}) copy-start(bf16[256,2048]{1,0:T(8,128)(2,1)} %param.37) | copy-start | bytes 3145732
  7.2 7.5 %copy-start.2 = (bf16[16,16,64]{2,1,0:T(8,128)(2,1)S(1)}, bf16[16,16,64]{2,1,0:T(8,128)(2,1)}, u32[]{:S(2)}) copy-start(bf16[16,16,64]{2,1,0:T(8,128)(2,1)} %param.30) | copy-start | bytes 98308
  7.2 8.0 %copy-start.3 = (bf16[16,16,64]{2,1,0:T(8,128)(2,1)S(1)}, bf16[16,16,64]{2,1,0:T(8,128)(2,1)}, u32[]{:S(2)}) copy-start(bf16[16,16,64]{2,1,0:T(8,128)(2,1)} %param.31) | copy-start | bytes 98308
  7.2 8.0 %copy-start.4 = (f32[16,16]{1,0:T(8,128)S(1)}, f32[16,16]{1,0:T(8,128)}, u32[]{:S(2)}) copy-start(f32[16,16]{1,0:T(8,128)} %param.32) | copy-start | bytes 3076
  7.2 19.2 %copy-start.1 = (bf16[1024,256]{1,0:T(8,128)(2,1)S(1)}, bf16[1024,256]{1,0:T(8,128)(2,1)}, u32[]{:S(2)}) copy-start(bf16[1024,256]{1,0:T(8,128)(2,1)} %param.35) | copy-start | bytes 1572868
  7.2 19.2 %copy-start.6 = (f32[256]{0:T(256)S(1)}, f32[256]{0:T(256)}, u32[]{:S(2)}) copy-start(f32[256]{0:T(256)} %param.36) | copy-start | bytes 3076
  7.2 45.3 %reduce-scatter.3.cloned.1.call-start = ((), (), s32[]{:S(2)}) async-start(), calls=%async_computation.4 | async-start | bytes 327680 | tf_op jit(solution)/shard_map/reduce_scatter | solution.py:84
  12.1 15.7 %copy-start.5 = (s32[64,2]{0,1:T(2,128)S(1)}, s32[64,2]{0,1:T(2,128)}, u32[]{:S(2)}) copy-start(s32[64,2]{0,1:T(2,128)} %param.39) | copy-start | bytes 1540
  27.8 103.8 %reduce-scatter.5.cloned.1.call-start = ((), (), s32[]{:S(2)}) async-start(), calls=%async_computation.5 | async-start | bytes 983040 | tf_op jit(solution)/shard_map/reduce_scatter | solution.py:118
  101.2 37.2 %copy-start.7 = (f32[64,2]{0,1:T(2,128)S(1)}, f32[64,2]{0,1:T(2,128)}, u32[]{:S(2)}) copy-start(f32[64,2]{0,1:T(2,128)} %param.40) | copy-start | bytes 1540
  131.6 12.9 %all-to-all-start.1 = ((bf16[512,8,24]{0,2,1:T(8,128)(2,1)}), bf16[512,8,24]{0,2,1:T(8,128)(2,1)S(1)}, u32[]{:S(2)}, u32[]{:S(2)}) async-start(bf16[512,8,24]{0,2,1:T(8,128)(2,1)} %bitcast.70), calls=%async_computation.3 | async-start | bytes 393216 | tf_op jit(solution)/shard_map/all_to_all | solution.py:127
Sparse Core Ops, SparseCore 0:
  27.9 24.6 reduce-scatter.2
  107.4 24.0 reduce-scatter.4
where the time goes:
time: 153 us; the launch traced here: 152 us
  blocking collectives  53.7 us (35%)
  waiting for transfers between devices  53 us (35%)
  matrix products  18.4 us (12%)
  between operations  14.3 us (9%)
  starting transfers between devices  4.69 us (3%)
  local copies, waits for them, and re-layouts  4.55 us (3%)
  other arithmetic  3.57 us (2%)
    all_to_all x1, blocking collectives, local(): lax.all_to_all(outbound.reshape(experts, slot_cap, model_width), 'ep', sp...  25.4 us
    reduce_scatter x1, waiting for transfers between devices, local(): lax.psum_scatter(lax.dot_general(down_local, hidden, (((0,), (1,)), ((),...  24.3 us
    reduce_scatter x1, waiting for transfers between devices, local(): lax.psum_scatter(partial_value.astype(jnp.bfloat16), 'tp', scatter_dimens...  22.9 us
    all_gather x1, blocking collectives, local(): lax.all_gather(mixed_in, 'tp', axis=1, tiled=True)  10.5 us
    all_gather x1, blocking collectives, local(): normed2 = lax.all_gather(own_cols, 'tp', axis=1, tiled=True)  8.93 us
    psum x1, blocking collectives, local(): squares = lax.psum(jnp.sum(part_values * part_values, axis=1), 'tp')  8.93 us
    dot_general x1, matrix products, local(): lax.dot_general(down_local, hidden, (((0,), (1,)), ((), ())), preferred_e...  6.1 us
    all_to_all x1, waiting for transfers between devices, local(): lax.all_to_all(back_rows, 'ep', split_axis=1, concat_axis=1, tiled=True)  5.74 us
  transfers between devices with their start and end apart: 3, of which 3 were waited for; matrix products, arithmetic and copies ran while one was open for 3% of the time, Pallas kernels for 0%

commit v1 on v0

v1 whole, which is shorter than its diff:
```python
import jax
import jax.numpy as jnp
from jax import lax
from jax.sharding import PartitionSpec as P

norm_eps = 1e-06


def rms_scale(rows, gain):
    values = rows.astype(jnp.float32)
    scaled = values * lax.rsqrt(jnp.mean(values * values, axis=-1, keepdims=True) + norm_eps)
    return (scaled * gain).astype(jnp.bfloat16)


def state_step(
    inputs, state_re, state_im, decay_re, freq, log_step, in_re, in_im, out_re, out_im, skip
):
    highest = lax.Precision.HIGHEST
    step = jnp.exp(log_step)[:, None]
    magnitude = jnp.exp(decay_re * step)
    turn_re = magnitude * jnp.cos(freq * step)
    turn_im = magnitude * jnp.sin(freq * step)
    denom = decay_re * decay_re + freq * freq
    coef_re = ((turn_re - 1.0) * decay_re + turn_im * freq) / denom
    coef_im = (turn_im * decay_re - (turn_re - 1.0) * freq) / denom
    drive_re = jnp.einsum("sgh,ghp->sgp", inputs, in_re, preferred_element_type=jnp.float32)
    drive_im = jnp.einsum("sgh,ghp->sgp", inputs, in_im, preferred_element_type=jnp.float32)
    push_re = coef_re * drive_re - coef_im * drive_im
    push_im = coef_re * drive_im + coef_im * drive_re
    new_re = turn_re * state_re - turn_im * state_im + push_re
    new_im = turn_re * state_im + turn_im * state_re + push_im
    read = jnp.einsum("ghp,sgp->sgh", out_re.astype(jnp.float32), new_re, precision=highest)
    read = read - jnp.einsum("ghp,sgp->sgh", out_im.astype(jnp.float32), new_im, precision=highest)
    read = read + skip * inputs.astype(jnp.float32)
    return (read, new_re, new_im)


def partner_swap(value, offset):
    count = lax.axis_size("tp")
    return lax.ppermute(value, "tp", [(source, source ^ offset) for source in range(count)])


def local(
    tokens,
    mix_gain,
    w_in,
    decay_re,
    freq,
    log_step,
    in_re,
    in_im,
    out_re,
    out_im,
    skip,
    state_re,
    state_im,
    glu_weight,
    glu_bias,
    out_weight,
    ffn_gain,
    route,
    route_weight,
    expert_gate,
    expert_up,
    expert_down,
):
    seq_count = tokens.shape[0]
    groups_local = decay_re.shape[0]
    model_width = tokens.shape[1]
    shards = lax.axis_size("tp")
    local_width = model_width // shards
    experts = lax.axis_size("ep")
    top_count = route.shape[1]
    slot_cap = (3 * seq_count * top_count + 2 * experts - 1) // (2 * experts)
    rows_all = experts * slot_cap
    own = lax.axis_index("tp")
    offsets = list(range(1, shards))
    gate_local = expert_gate[0]
    up_local = expert_up[0]
    down_local = expert_down[0]

    def rows_of(array, offset, width):
        return lax.dynamic_slice_in_dim(array, (own ^ offset) * width, width, 0)

    def cols_of(array, offset, width):
        return lax.dynamic_slice_in_dim(array, (own ^ offset) * width, width, 1)

    normed = rms_scale(tokens, mix_gain)
    drive = jnp.dot(normed, w_in, preferred_element_type=jnp.float32).astype(jnp.bfloat16)
    inputs = drive.reshape(seq_count, groups_local, -1)
    read, new_re, new_im = state_step(
        inputs, state_re, state_im, decay_re, freq, log_step, in_re, in_im, out_re, out_im, skip
    )
    mixed_in = jax.nn.gelu(read).reshape(seq_count, -1).astype(jnp.bfloat16)
    chan_width = mixed_in.shape[1]

    arrived_mix = [partner_swap(mixed_in, offset) for offset in offsets]
    gate = jnp.dot(
        mixed_in, rows_of(glu_weight, 0, chan_width), preferred_element_type=jnp.float32
    )
    for offset, block in zip(offsets, arrived_mix):
        gate = gate + jnp.dot(
            block, rows_of(glu_weight, offset, chan_width), preferred_element_type=jnp.float32
        )
    gated = (mixed_in.astype(jnp.float32) * jax.nn.sigmoid(gate + glu_bias)).astype(jnp.bfloat16)

    def share(offset):
        block = jnp.dot(
            gated, cols_of(out_weight, offset, local_width), preferred_element_type=jnp.float32
        )
        return block.astype(jnp.bfloat16)

    arrived_shares = [partner_swap(share(offset), offset) for offset in offsets]
    mix_part = share(0).astype(jnp.float32)
    for block in arrived_shares:
        mix_part = mix_part + block.astype(jnp.float32)
    resid_part = (cols_of(tokens, 0, local_width).astype(jnp.float32) + mix_part).astype(
        jnp.bfloat16
    )

    flat_route = route.reshape(-1)
    hits = (flat_route[:, None] == jnp.arange(experts)[None, :]).astype(jnp.int32)
    rank = jnp.sum((jnp.cumsum(hits, axis=0) - hits) * hits, axis=1)
    slot = flat_route * slot_cap + rank
    slot_ids = jnp.arange(rows_all)
    picks = (slot[None, :] == slot_ids[:, None]).reshape(rows_all, seq_count, top_count)
    select = jnp.any(picks, axis=2).astype(jnp.bfloat16)
    combine = jnp.einsum("ask,sk->sa", picks.astype(jnp.float32), route_weight)

    outbound = jnp.dot(select, resid_part, preferred_element_type=jnp.float32).astype(jnp.bfloat16)
    arrived = lax.all_to_all(
        outbound.reshape(experts, slot_cap, local_width),
        "ep",
        split_axis=0,
        concat_axis=0,
        tiled=True,
    ).reshape(rows_all, local_width)
    blocks = [(0, arrived)] + [(offset, partner_swap(arrived, offset)) for offset in offsets]
    gate_rows = up_rows = squares = 0.0
    for offset, block in blocks:
        values = block.astype(jnp.float32)
        squares = squares + jnp.sum(values * values, axis=1, keepdims=True)
        gain = lax.dynamic_slice_in_dim(ffn_gain, (own ^ offset) * local_width, local_width, 0)
        scaled = (values * gain).astype(jnp.bfloat16)
        gate_rows = gate_rows + jnp.dot(
            scaled, rows_of(gate_local, offset, local_width), preferred_element_type=jnp.float32
        )
        up_rows = up_rows + jnp.dot(
            scaled, rows_of(up_local, offset, local_width), preferred_element_type=jnp.float32
        )
    row_scale = lax.rsqrt(squares / model_width + norm_eps)
    hidden = (jax.nn.silu(gate_rows * row_scale) * (up_rows * row_scale)).astype(jnp.bfloat16)

    def result(offset):
        block = jnp.dot(
            hidden, cols_of(down_local, offset, local_width), preferred_element_type=jnp.float32
        )
        return block.astype(jnp.bfloat16)

    arrived_results = [partner_swap(result(offset), offset) for offset in offsets]
    back_rows = result(0).astype(jnp.float32)
    for block in arrived_results:
        back_rows = back_rows + block.astype(jnp.float32)
    returned = lax.all_to_all(
        back_rows.astype(jnp.bfloat16).reshape(experts, slot_cap, local_width),
        "ep",
        split_axis=0,
        concat_axis=0,
        tiled=True,
    ).reshape(rows_all, local_width)
    expert_total = lax.dot_general(
        combine,
        returned.astype(jnp.float32),
        (((1,), (0,)), ((), ())),
        precision=lax.Precision.HIGHEST,
    )
    mixed = (resid_part.astype(jnp.float32) + expert_total).astype(jnp.bfloat16)
    return (mixed, new_re, new_im)


def solution(mesh):
    in_specs = (
        P("ep", None),
        P(),
        P(None, "tp"),
        P("tp", None),
        P("tp", None),
        P("tp"),
        P("tp", None, None),
        P("tp", None, None),
        P("tp", None, None),
        P("tp", None, None),
        P("tp", None),
        P("ep", "tp", None),
        P("ep", "tp", None),
        P(None, "tp"),
        P("tp"),
        P("tp", None),
        P(),
        P("ep", None),
        P("ep", None),
        P("ep", None, "tp"),
        P("ep", None, "tp"),
        P("ep", "tp", None),
    )
    out_specs = (P("ep", "tp"), P("ep", "tp", None), P("ep", "tp", None))
    return jax.shard_map(local, mesh=mesh, in_specs=in_specs, out_specs=out_specs, check_vma=False)
```

time: 153 us -> 91.5 us (0.60)
  blocking collectives: 53.7 us -> 0 us
  waiting for transfers between devices: 53 us -> 27 us
  starting transfers between devices: 4.69 us -> 25 us
  between operations: 14.3 us -> 1.07 us
  matrix products: 18.4 us -> 24.9 us
  other arithmetic: 3.57 us -> 8.17 us
    reduce_scatter x2 -> x0, waiting for transfers between devices: 47.2 us -> none  [the longest x1 24.3 us: local(): lax.psum_scatter(lax.dot_general(down_local, hidden, (((0,), (1,)), ((),...]
    all_to_all x1 -> x0, blocking collectives: 25.4 us -> none  [local(): lax.all_to_all(outbound.reshape(experts, slot_cap, model_width), 'ep', sp...]
    all_gather x2 -> x0, blocking collectives: 19.4 us -> none  [the longest x1 10.5 us: local(): lax.all_gather(mixed_in, 'tp', axis=1, tiled=True)]
    ppermute x0 -> x12, starting transfers between devices: none -> 15.3 us  [partner_swap(): lax.ppermute(value, 'tp', [(source, source ^ offset) for source in range(...]
    ppermute x0 -> x12, waiting for transfers between devices: none -> 12.9 us  [partner_swap(): lax.ppermute(value, 'tp', [(source, source ^ offset) for source in range(...]
    psum x1 -> x0, blocking collectives: 8.93 us -> none  [local(): squares = lax.psum(jnp.sum(part_values * part_values, axis=1), 'tp')]
    all_to_all x1 -> x2, waiting for transfers between devices: 5.74 us -> 14.1 us  [the longest x1 8.31 us: local(): lax.all_to_all(outbound.reshape(experts, slot_cap, local_width), 'ep', sp...]
    dot_general x5 -> x22, matrix products: 12.6 us -> 19 us  [the longest x4 6.67 us: local(): jnp.dot(scaled, rows_of(up_local, offset, local_width), preferred_element...]
  transfers between devices with their start and end apart: 3 -> 14, of which waited for: 3 -> 9; matrix products, arithmetic and copies ran while one was open for 3% -> 14% of each run, Pallas kernels for 0% -> 0%
where the time goes in v1:
time: 91.5 us; the launch traced here: 90.6 us
  waiting for transfers between devices  27 us (30%)
  starting transfers between devices  25 us (27%)
  matrix products  24.9 us (27%)
  other arithmetic  8.17 us (9%)
  local copies, waits for them, and re-layouts  4.54 us (5%)
  between operations  1.07 us (1%)
    ppermute x12, starting transfers between devices, partner_swap(): lax.ppermute(value, 'tp', [(source, source ^ offset) for source in range(...  15.3 us
    ppermute x12, waiting for transfers between devices, partner_swap(): lax.ppermute(value, 'tp', [(source, source ^ offset) for source in range(...  12.9 us
    all_to_all x1, waiting for transfers between devices, local(): lax.all_to_all(outbound.reshape(experts, slot_cap, local_width), 'ep', sp...  8.31 us
    dot_general x4, matrix products, local(): jnp.dot(scaled, rows_of(up_local, offset, local_width), preferred_element...  6.67 us
    dot_general x4, matrix products, local(): jnp.dot(scaled, rows_of(gate_local, offset, local_width), preferred_eleme...  6.03 us
    all_to_all x1, waiting for transfers between devices, local(): lax.all_to_all(back_rows.astype(jnp.bfloat16).reshape(experts, slot_cap,...  5.74 us
    all_to_all x1, starting transfers between devices, local(): lax.all_to_all(outbound.reshape(experts, slot_cap, local_width), 'ep', sp...  4.88 us
    all_to_all x1, starting transfers between devices, local(): lax.all_to_all(back_rows.astype(jnp.bfloat16).reshape(experts, slot_cap,...  4.85 us
  transfers between devices with their start and end apart: 14, of which 9 were waited for; matrix products, arithmetic and copies ran while one was open for 14% of the time, Pallas kernels for 0%

profile of v1, /device:TPU:0, one launch (start us, length us, event | category | flops | bytes accessed | tf_op | source)
XLA Modules:
  0.0 90.6 jit_solution(3459519420991320487)
XLA Ops:
  0.7 0.8 exp.13
  1.5 1.1 %fusion.44 = f32[64]{0:T(128)S(1)} fusion(bf16[64,2048]{1,0:T(8,128)(2,1)} %param.22), kind=kLoop, calls=%fused_computation.64 | loop fusion | flops 393152 | bytes 262400 | tf_op jit(solution)/shard_map/reduce_sum | solution.py:11
  2.6 1.7 %convolution_convert_fusion.9 = bf16[64,256]{1,0:T(8,128)(2,1)S(1)} fusion(bf16[2048,256]{1,0:T(8,128)(2,1)} %param.24, bf16[64,2048]{1,0:T(8,128)(2,1)} %param.22, f32[2048]{0:T(1024)} %param.23, f32[64]{0:T(128)S(1)} %add_rsqrt_fusion.1), kind=kOutput, calls=%fused_computation.31 | convolution fusion | flops 67649536 | bytes 1351936 | tf_op jit(solution)/shard_map/dot_general | solution.py:89
  4.4 1.1 %fusion.119 = f32[16,64,64]{2,1,0:T(8,128)S(1)} fusion(bf16[64,16,16]{0,2,1:T(8,128)(2,1)S(1)} %bitcast.94, bf16[16,16,64]{2,1,0:T(8,128)(2,1)} %param.29), kind=kOutput, calls=%fused_computation.149 | convolution fusion | flops 2097152 | bytes 327680 | tf_op jit(solution)/shard_map/sgh,ghp->sgp/dot_general | solution.py:27
  5.5 0.8 cosine_multiply_fusion
  6.4 1.8 %bitcast_add_fusion = (f32[64,16,64]{2,0,1:T(8,128)S(1)}, f32[64,16,64]{2,0,1:T(8,128)S(1)}) fusion(f32[16,64,64]{2,1,0:T(8,128)S(1)} %fusion.119, f32[64,16,64]{2,1,0:T(8,128)} %param.34, f32[64,16,64]{2,1,0:T(8,128)} %param.33, f32[16,64]{1,0:T(8,128)S(1)} %get-tuple-element.21, f32[16,64]{1,0:T(8,128)S(1)} %get-tuple-element.22, ...), kind=kOutput, calls=%fused_computation.67 | convolution fusion | flops 3014656 | bytes 1392640 | tf_op jit(solution)/shard_map/sgh,ghp->sgp/dot_general | solution.py:26
  9.2 3.0 %collective-permute-start = (bf16[64,256]{0,1:T(8,128)(2,1)S(1)}, bf16[64,256]{0,1:T(8,128)(2,1)S(1)}, u32[]{:S(2)}, u32[]{:S(2)}) collective-permute-start(bf16[64,256]{0,1:T(8,128)(2,1)S(1)} %bitcast.98), channel_id=1, source_target_pairs={{0,1},{1,0},{2,3},{3,2},{4,5},{5,4},{6,7},{7,6},{8,9},{9,8},{10,11... | collective-permute-start | bytes 98312 | tf_op jit(solution)/shard_map/ppermute | solution.py:40
  12.3 1.5 %collective-permute-start.2 = (bf16[64,256]{0,1:T(8,128)(2,1)S(1)}, bf16[64,256]{0,1:T(8,128)(2,1)S(1)}, u32[]{:S(2)}, u32[]{:S(2)}) collective-permute-start(bf16[64,256]{0,1:T(8,128)(2,1)S(1)} %bitcast.99), channel_id=1, source_target_pairs={{0,3},{1,2},{2,1},{3,0},{4,7},{5,6},{6,5},{7,4},{8,11},{9,10},{10,... | collective-permute-start | bytes 98312 | tf_op jit(solution)/shard_map/ppermute | solution.py:40
  15.3 2.2 %collective-permute-done.2 = bf16[64,256]{0,1:T(8,128)(2,1)S(1)} collective-permute-done((bf16[64,256]{0,1:T(8,128)(2,1)S(1)}, bf16[64,256]{0,1:T(8,128)(2,1)S(1)}, u32[]{:S(2)}, u32[]{:S(2)}) %collective-permute-start.2) | collective-permute-done | bytes 32800 | tf_op jit(solution)/shard_map/ppermute | solution.py:40
  18.7 1.3 %collective-permute-start.3 = (bf16[64,512]{1,0:T(8,128)(2,1)S(1)}, bf16[64,512]{1,0:T(8,128)(2,1)S(1)}, u32[]{:S(2)}, u32[]{:S(2)}) collective-permute-start(bf16[64,512]{1,0:T(8,128)(2,1)S(1)} %convolution_convert_fusion.7), channel_id=1, source_target_pairs={{0,1},{1,0},{2,3},{3,2},{4,5},{5,4},{6,7},{7,6},{8,9},{9,8},{10,11... | collective-permute-start | bytes 196616 | tf_op jit(solution)/shard_map/ppermute | solution.py:40
  20.2 0.9 collective-permute-start.4
  21.2 1.5 %collective-permute-start.5 = (bf16[64,512]{1,0:T(8,128)(2,1)S(1)}, bf16[64,512]{1,0:T(8,128)(2,1)S(1)}, u32[]{:S(2)}, u32[]{:S(2)}) collective-permute-start(bf16[64,512]{1,0:T(8,128)(2,1)S(1)} %convolution_convert_fusion.5), channel_id=1, source_target_pairs={{0,3},{1,2},{2,1},{3,0},{4,7},{5,6},{6,5},{7,4},{8,11},{9,10},{10,... | collective-permute-start | bytes 196616 | tf_op jit(solution)/shard_map/ppermute | solution.py:40
  22.7 0.7 iota_compare_fusion
  23.4 1.7 %collective-permute-done.4 = bf16[64,512]{1,0:T(8,128)(2,1)S(1)} collective-permute-done((bf16[64,512]{1,0:T(8,128)(2,1)S(1)}, bf16[64,512]{1,0:T(8,128)(2,1)S(1)}, u32[]{:S(2)}, u32[]{:S(2)}) %collective-permute-start.4) | collective-permute-done | bytes 65568 | tf_op jit(solution)/shard_map/ppermute | solution.py:40
  25.1 1.3 %collective-permute-done.5 = bf16[64,512]{1,0:T(8,128)(2,1)S(1)} collective-permute-done((bf16[64,512]{1,0:T(8,128)(2,1)S(1)}, bf16[64,512]{1,0:T(8,128)(2,1)S(1)}, u32[]{:S(2)}, u32[]{:S(2)}) %collective-permute-start.5) | collective-permute-done | bytes 65568 | tf_op jit(solution)/shard_map/ppermute | solution.py:40
  26.4 1.0 %add_convert_fusion.2 = bf16[64,512]{1,0:T(8,128)(2,1)S(1)} fusion(bf16[64,512]{1,0:T(8,128)(2,1)S(1)} %collective-permute-done.5, bf16[64,512]{1,0:T(8,128)(2,1)S(1)} %collective-permute-done.4, bf16[64,512]{1,0:T(8,128)(2,1)S(1)} %collective-permute-done.3, bf16[64,2048]{1,0:T(8,128)(2,1)} %param.22, s32[]{:T(128)S(6)} %select_n.16, ...), kind=kOutput, calls=%fused_computation.105 | convolution fusion | flops 17137664 | bytes 623616 | tf_op jit(solution)/shard_map/dot_general | solution.py:108
  27.4 0.9 %convolution_convert_fusion = bf16[192,512]{1,0:T(8,128)(2,1)} fusion(pred[192,64]{0,1:T(8,128)(4,1)S(1)} %get-tuple-element.28, bf16[64,512]{1,0:T(8,128)(2,1)S(1)} %add_convert_fusion.2), kind=kOutput, calls=%fused_computation.8 | convolution fusion | flops 12681216 | bytes 274432 | tf_op jit(solution)/shard_map/dot_general | solution.py:130
  28.4 4.9 %all-to-all-start = ((bf16[8,24,512]{2,1,0:T(8,128)(2,1)}), bf16[8,24,512]{2,1,0:T(8,128)(2,1)}, u32[]{:S(2)}, u32[]{:S(2)}) async-start(bf16[8,24,512]{2,1,0:T(8,128)(2,1)} %bitcast.7), calls=%async_computation | async-start | bytes 393216 | tf_op jit(solution)/shard_map/all_to_all | solution.py:131
  33.3 8.3 %all-to-all-done = bf16[8,24,512]{2,1,0:T(8,128)(2,1)} async-done(((bf16[8,24,512]{2,1,0:T(8,128)(2,1)}), bf16[8,24,512]{2,1,0:T(8,128)(2,1)}, u32[]{:S(2)}, u32[]{:S(2)}) %all-to-all-start) | async-done | bytes 196640 | tf_op jit(solution)/shard_map/all_to_all | solution.py:131
  41.7 1.0 %collective-permute-start.6 = (bf16[192,512]{1,0:T(8,128)(2,1)}, bf16[192,512]{1,0:T(8,128)(2,1)}, u32[]{:S(2)}, u32[]{:S(2)}) collective-permute-start(bf16[192,512]{1,0:T(8,128)(2,1)} %bitcast.10), channel_id=1, source_target_pairs={{0,1},{1,0},{2,3},{3,2},{4,5},{5,4},{6,7},{7,6},{8,9},{9,8},{10,11... | collective-permute-start | bytes 589832 | tf_op jit(solution)/shard_map/ppermute | solution.py:40
  42.6 1.1 %collective-permute-start.7 = (bf16[192,512]{1,0:T(8,128)(2,1)}, bf16[192,512]{1,0:T(8,128)(2,1)}, u32[]{:S(2)}, u32[]{:S(2)}) collective-permute-start(bf16[192,512]{1,0:T(8,128)(2,1)} %bitcast.10), channel_id=1, source_target_pairs={{0,2},{1,3},{2,0},{3,1},{4,6},{5,7},{6,4},{7,5},{8,10},{9,11},{10,... | collective-permute-start | bytes 589832 | tf_op jit(solution)/shard_map/ppermute | solution.py:40
  43.7 1.5 %collective-permute-start.8 = (bf16[192,512]{1,0:T(8,128)(2,1)}, bf16[192,512]{1,0:T(8,128)(2,1)}, u32[]{:S(2)}, u32[]{:S(2)}) collective-permute-start(bf16[192,512]{1,0:T(8,128)(2,1)} %bitcast.10), channel_id=1, source_target_pairs={{0,3},{1,2},{2,1},{3,0},{4,7},{5,6},{6,5},{7,4},{8,11},{9,10},{10,... | collective-permute-start | bytes 589832 | tf_op jit(solution)/shard_map/ppermute | solution.py:40
  45.2 1.1 %fusion.48 = (f32[8,24]{1,0:T(8,128)S(1)}, bf16[8,24,512]{2,1,0:T(8,128)(2,1)S(1)}) fusion(bf16[8,24,512]{2,1,0:T(8,128)(2,1)} %all-to-all-done, f32[512]{0:T(512)S(1)} %get-tuple-element.25), kind=kLoop, calls=%fused_computation.78 | loop fusion | flops 491328 | bytes 396032 | tf_op jit(solution)/shard_map/reduce_sum | solution.py:142
  46.2 1.6 %fusion.24 = f32[192,896]{1,0:T(8,128)S(1)} fusion(bf16[192,512]{1,0:T(8,128)(2,1)S(1)} %bitcast.92, bf16[1,2048,896]{2,1,0:T(8,128)(2,1)} %param.42, s32[]{:T(128)S(6)} %select_n.16), kind=kOutput, calls=%fused_computation.41 | convolution fusion | flops 176160768 | bytes 1802244 | tf_op jit(solution)/shard_map/dot_general | solution.py:148
  47.8 1.6 %fusion.30 = f32[192,896]{1,0:T(8,128)S(1)} fusion(bf16[192,512]{1,0:T(8,128)(2,1)S(1)} %bitcast.93, bf16[1,2048,896]{2,1,0:T(8,128)(2,1)} %param.41, s32[]{:T(128)S(6)} %select_n.16), kind=kOutput, calls=%fused_computation.47 | convolution fusion | flops 176160768 | bytes 1802244 | tf_op jit(solution)/shard_map/dot_general | solution.py:145
  49.4 0.6 reduce_sum.62
  50.0 1.2 %fusion.50 = f32[192]{0:T(256)S(1)} fusion(bf16[192,512]{1,0:T(8,128)(2,1)} %collective-permute-done.6), kind=kLoop, calls=%fused_computation.80 | loop fusion | flops 294720 | bytes 197376 | tf_op jit(solution)/shard_map/reduce_sum | solution.py:142
  51.2 1.3 %collective-permute-done.7 = bf16[192,512]{1,0:T(8,128)(2,1)} collective-permute-done((bf16[192,512]{1,0:T(8,128)(2,1)}, bf16[192,512]{1,0:T(8,128)(2,1)}, u32[]{:S(2)}, u32[]{:S(2)}) %collective-permute-start.7) | collective-permute-done | bytes 196640 | tf_op jit(solution)/shard_map/ppermute | solution.py:40
  52.5 1.0 %fusion.52 = f32[192]{0:T(256)S(1)} fusion(bf16[192,512]{1,0:T(8,128)(2,1)} %collective-permute-done.7), kind=kLoop, calls=%fused_computation.82 | loop fusion | flops 294720 | bytes 197376 | tf_op jit(solution)/shard_map/reduce_sum | solution.py:142
  53.6 1.0 %fusion.54 = f32[192]{0:T(256)S(1)} fusion(bf16[192,512]{1,0:T(8,128)(2,1)} %collective-permute-done.8), kind=kLoop, calls=%fused_computation.84 | loop fusion | flops 294720 | bytes 197376 | tf_op jit(solution)/shard_map/reduce_sum | solution.py:142
  54.7 0.7 add_rsqrt_fusion
  55.3 1.7 %fusion.26 = f32[192,896]{1,0:T(8,128)S(1)} fusion(bf16[1,2048,896]{2,1,0:T(8,128)(2,1)} %param.41, s32[]{:T(128)S(6)} %select_n.23, bf16[192,512]{1,0:T(8,128)(2,1)} %collective-permute-done.8, f32[512]{0:T(512)S(1)} %get-tuple-element.26), kind=kOutput, calls=%fused_computation.43 | convolution fusion | flops 176455680 | bytes 1804292 | tf_op jit(solution)/shard_map/dot_general | solution.py:145
  57.0 1.7 %fusion.20 = f32[192,896]{1,0:T(8,128)S(1)} fusion(bf16[1,2048,896]{2,1,0:T(8,128)(2,1)} %param.42, s32[]{:T(128)S(6)} %select_n.23, bf16[192,512]{1,0:T(8,128)(2,1)} %collective-permute-done.8, f32[512]{0:T(512)S(1)} %get-tuple-element.26), kind=kOutput, calls=%fused_computation.37 | convolution fusion | flops 176455680 | bytes 1804292 | tf_op jit(solution)/shard_map/dot_general | solution.py:148
  58.7 1.7 %convolution_add_fusion.1 = f32[192,896]{1,0:T(8,128)S(1)} fusion(f32[192,896]{1,0:T(8,128)S(1)} %fusion.24, bf16[1,2048,896]{2,1,0:T(8,128)(2,1)} %param.42, s32[]{:T(128)S(6)} %select_n.21, bf16[192,512]{1,0:T(8,128)(2,1)} %collective-permute-done.6, f32[512]{0:T(512)S(1)} %get-tuple-element.24), kind=kOutput, calls=%fused_computation.1 | convolution fusion | flops 176627712 | bytes 2492420 | tf_op jit(solution)/shard_map/dot_general | solution.py:148
  60.4 1.3 %convolution_add_fusion.3 = f32[192,896]{1,0:T(8,128)S(1)} fusion(f32[192,896]{1,0:T(8,128)S(1)} %fusion.30, bf16[1,2048,896]{2,1,0:T(8,128)(2,1)S(1)} %copy-done.1, s32[]{:T(128)S(6)} %select_n.21, bf16[192,512]{1,0:T(8,128)(2,1)} %collective-permute-done.6, f32[512]{0:T(512)S(1)} %get-tuple-element.24), kind=kOutput, calls=%fused_computation.3 | convolution fusion | flops 176627712 | bytes 2492420 | tf_op jit(solution)/shard_map/dot_general | solution.py:145
  61.8 1.5 %fusion.1 = f32[192,896]{1,0:T(8,128)S(1)} fusion(f32[192,896]{1,0:T(8,128)S(1)} %fusion.26, f32[192,896]{1,0:T(8,128)S(1)} %convolution_add_fusion.3, bf16[1,2048,896]{2,1,0:T(8,128)(2,1)S(1)} %copy-done.1, s32[]{:T(128)S(6)} %select_n.22, f32[192]{0:T(256)S(1)} %add_rsqrt_fusion, bf16[192,512]{1,0:T(8,128)(2,1)} %collective-permute-done.7, ...), kind=kOutput, calls=%fused_computation.5 | convolution fusion | flops 176971776 | bytes 3181572 | tf_op jit(solution)/shard_map/dot_general | solution.py:145
  63.2 1.7 %multiply_convert_fusion = bf16[192,896]{1,0:T(8,128)(2,1)S(1)} fusion(f32[192,896]{1,0:T(8,128)S(1)} %fusion.1, f32[192]{0:T(256)S(1)} %add_rsqrt_fusion, f32[192,896]{1,0:T(8,128)S(1)} %fusion.20, f32[192,896]{1,0:T(8,128)S(1)} %convolution_add_fusion.1, bf16[1,2048,896]{2,1,0:T(8,128)(2,1)} %param.42, s32[]{:T(128)S(6)} %select_n.22, ...), kind=kOutput, calls=%fused_computation.61 | convolution fusion | flops 178003968 | bytes 3525380 | tf_op jit(solution)/shard_map/dot_general | solution.py:148
  66.2 1.0 %collective-permute-start.10 = (bf16[192,512]{1,0:T(8,128)(2,1)S(1)}, bf16[192,512]{1,0:T(8,128)(2,1)S(1)}, u32[]{:S(2)}, u32[]{:S(2)}) collective-permute-start(bf16[192,512]{1,0:T(8,128)(2,1)S(1)} %convolution_convert_fusion.2), channel_id=1, source_target_pairs={{0,2},{1,3},{2,0},{3,1},{4,6},{5,7},{6,4},{7,5},{8,10},{9,11},{10,... | collective-permute-start | bytes 589832 | tf_op jit(solution)/shard_map/ppermute | solution.py:40
  67.2 1.2 %collective-permute-start.9 = (bf16[192,512]{1,0:T(8,128)(2,1)S(1)}, bf16[192,512]{1,0:T(8,128)(2,1)S(1)}, u32[]{:S(2)}, u32[]{:S(2)}) collective-permute-start(bf16[192,512]{1,0:T(8,128)(2,1)S(1)} %convolution_convert_fusion.3), channel_id=1, source_target_pairs={{0,1},{1,0},{2,3},{3,2},{4,5},{5,4},{6,7},{7,6},{8,9},{9,8},{10,11... | collective-permute-start | bytes 589832 | tf_op jit(solution)/shard_map/ppermute | solution.py:40
  68.4 1.3 %collective-permute-start.11 = (bf16[192,512]{1,0:T(8,128)(2,1)S(1)}, bf16[192,512]{1,0:T(8,128)(2,1)S(1)}, u32[]{:S(2)}, u32[]{:S(2)}) collective-permute-start(bf16[192,512]{1,0:T(8,128)(2,1)S(1)} %convolution_convert_fusion.1), channel_id=1, source_target_pairs={{0,3},{1,2},{2,1},{3,0},{4,7},{5,6},{6,5},{7,4},{8,11},{9,10},{10,... | collective-permute-start | bytes 589832 | tf_op jit(solution)/shard_map/ppermute | solution.py:40
  69.8 3.2 %collective-permute-done.10 = bf16[192,512]{1,0:T(8,128)(2,1)S(1)} collective-permute-done((bf16[192,512]{1,0:T(8,128)(2,1)S(1)}, bf16[192,512]{1,0:T(8,128)(2,1)S(1)}, u32[]{:S(2)}, u32[]{:S(2)}) %collective-permute-start.10) | collective-permute-done | bytes 196640 | tf_op jit(solution)/shard_map/ppermute | solution.py:40
  73.0 2.6 %collective-permute-done.11 = bf16[192,512]{1,0:T(8,128)(2,1)S(1)} collective-permute-done((bf16[192,512]{1,0:T(8,128)(2,1)S(1)}, bf16[192,512]{1,0:T(8,128)(2,1)S(1)}, u32[]{:S(2)}, u32[]{:S(2)}) %collective-permute-start.11) | collective-permute-done | bytes 196640 | tf_op jit(solution)/shard_map/ppermute | solution.py:40
  75.5 1.1 %add_convert_fusion = bf16[192,512]{1,0:T(8,128)(2,1)} fusion(bf16[192,512]{1,0:T(8,128)(2,1)S(1)} %collective-permute-done.11, bf16[192,512]{1,0:T(8,128)(2,1)S(1)} %collective-permute-done.10, bf16[192,512]{1,0:T(8,128)(2,1)S(1)} %collective-permute-done.9, bf16[192,896]{1,0:T(8,128)(2,1)S(1)} %multiply_convert_fusion, ...), kind=kOutput, calls=%fused_computation.85 | convolution fusion | flops 177045504 | bytes 2048004 | tf_op jit(solution)/shard_map/dot_general | solution.py:155
  76.6 4.9 %all-to-all-start.1 = ((bf16[8,24,512]{2,1,0:T(8,128)(2,1)}), bf16[8,24,512]{2,1,0:T(8,128)(2,1)S(1)}, u32[]{:S(2)}, u32[]{:S(2)}) async-start(bf16[8,24,512]{2,1,0:T(8,128)(2,1)} %bitcast.22), calls=%async_computation.1 | async-start | bytes 393216 | tf_op jit(solution)/shard_map/all_to_all | solution.py:164
  81.5 1.1 %copy.69 = f32[64,16,64]{2,1,0:T(8,128)} copy(f32[64,16,64]{2,0,1:T(8,128)S(1)} %get-tuple-element.16) | data formatting | bytes 524288
  82.6 1.1 %copy.70 = f32[64,16,64]{2,1,0:T(8,128)} copy(f32[64,16,64]{2,0,1:T(8,128)S(1)} %get-tuple-element.15) | data formatting | bytes 524288
  84.0 5.7 %all-to-all-done.1 = bf16[8,24,512]{2,1,0:T(8,128)(2,1)S(1)} async-done(((bf16[8,24,512]{2,1,0:T(8,128)(2,1)}), bf16[8,24,512]{2,1,0:T(8,128)(2,1)S(1)}, u32[]{:S(2)}, u32[]{:S(2)}) %all-to-all-start.1) | async-done | bytes 196640 | tf_op jit(solution)/shard_map/all_to_all | solution.py:164
  89.8 0.9 add_convert_fusion.1
  (57 shorter events, 5.8 us)
Async XLA Ops:
  0.6 17.9 %copy-start = (bf16[256,2048]{1,0:T(8,128)(2,1)S(1)}, bf16[256,2048]{1,0:T(8,128)(2,1)}, u32[]{:S(2)}) copy-start(bf16[256,2048]{1,0:T(8,128)(2,1)} %param.37) | copy-start | bytes 3145732
  0.6 7.5 %copy-start.4 = (bf16[16,16,64]{2,1,0:T(8,128)(2,1)S(1)}, bf16[16,16,64]{2,1,0:T(8,128)(2,1)}, u32[]{:S(2)}) copy-start(bf16[16,16,64]{2,1,0:T(8,128)(2,1)} %param.30) | copy-start | bytes 98308
  0.7 8.0 %copy-start.5 = (bf16[16,16,64]{2,1,0:T(8,128)(2,1)S(1)}, bf16[16,16,64]{2,1,0:T(8,128)(2,1)}, u32[]{:S(2)}) copy-start(bf16[16,16,64]{2,1,0:T(8,128)(2,1)} %param.31) | copy-start | bytes 98308
  0.7 8.0 %copy-start.7 = (f32[16,16]{1,0:T(8,128)S(1)}, f32[16,16]{1,0:T(8,128)}, u32[]{:S(2)}) copy-start(f32[16,16]{1,0:T(8,128)} %param.32) | copy-start | bytes 3076
  0.7 13.1 %copy-start.9 = (s32[64,2]{0,1:T(2,128)S(1)}, s32[64,2]{0,1:T(2,128)}, u32[]{:S(2)}) copy-start(s32[64,2]{0,1:T(2,128)} %param.39) | copy-start | bytes 1540
  0.7 14.0 %copy-start.3 = (bf16[1024,256]{1,0:T(8,128)(2,1)S(1)}, bf16[1024,256]{1,0:T(8,128)(2,1)}, u32[]{:S(2)}) copy-start(bf16[1024,256]{1,0:T(8,128)(2,1)} %param.35) | copy-start | bytes 1572868
  2.6 15.7 %copy-start.11 = (f32[256]{0:T(256)S(1)}, f32[256]{0:T(256)}, u32[]{:S(2)}) copy-start(f32[256]{0:T(256)} %param.36) | copy-start | bytes 3076
  6.4 26.9 %copy-start.8 = (f32[2048]{0:T(1024)S(1)}, f32[2048]{0:T(1024)}, u32[]{:S(2)}) copy-start(f32[2048]{0:T(1024)} %param.38) | copy-start | bytes 24580
  9.2 5.8 %collective-permute-start = (bf16[64,256]{0,1:T(8,128)(2,1)S(1)}, bf16[64,256]{0,1:T(8,128)(2,1)S(1)}, u32[]{:S(2)}, u32[]{:S(2)}) collective-permute-start(bf16[64,256]{0,1:T(8,128)(2,1)S(1)} %bitcast.98), channel_id=1, source_target_pairs={{0,1},{1,0},{2,3},{3,2},{4,5},{5,4},{6,7},{7,6},{8,9},{9,8},{10,11... | collective-permute-start | bytes 98312 | tf_op jit(solution)/shard_map/ppermute | solution.py:40
  12.3 5.2 %collective-permute-start.2 = (bf16[64,256]{0,1:T(8,128)(2,1)S(1)}, bf16[64,256]{0,1:T(8,128)(2,1)S(1)}, u32[]{:S(2)}, u32[]{:S(2)}) collective-permute-start(bf16[64,256]{0,1:T(8,128)(2,1)S(1)} %bitcast.99), channel_id=1, source_target_pairs={{0,3},{1,2},{2,1},{3,0},{4,7},{5,6},{6,5},{7,4},{8,11},{9,10},{10,... | collective-permute-start | bytes 98312 | tf_op jit(solution)/shard_map/ppermute | solution.py:40
  13.8 4.5 %collective-permute-start.1 = (bf16[64,256]{0,1:T(8,128)(2,1)S(1)}, bf16[64,256]{0,1:T(8,128)(2,1)S(1)}, u32[]{:S(2)}, u32[]{:S(2)}) collective-permute-start(bf16[64,256]{0,1:T(8,128)(2,1)S(1)} %bitcast.100), channel_id=1, source_target_pairs={{0,2},{1,3},{2,0},{3,1},{4,6},{5,7},{6,4},{7,5},{8,10},{9,11},{10,... | collective-permute-start | bytes 98312 | tf_op jit(solution)/shard_map/ppermute | solution.py:40
  18.7 4.7 %collective-permute-start.3 = (bf16[64,512]{1,0:T(8,128)(2,1)S(1)}, bf16[64,512]{1,0:T(8,128)(2,1)S(1)}, u32[]{:S(2)}, u32[]{:S(2)}) collective-permute-start(bf16[64,512]{1,0:T(8,128)(2,1)S(1)} %convolution_convert_fusion.7), channel_id=1, source_target_pairs={{0,1},{1,0},{2,3},{3,2},{4,5},{5,4},{6,7},{7,6},{8,9},{9,8},{10,11... | collective-permute-start | bytes 196616 | tf_op jit(solution)/shard_map/ppermute | solution.py:40
  20.2 4.9 %collective-permute-start.4 = (bf16[64,512]{1,0:T(8,128)(2,1)S(1)}, bf16[64,512]{1,0:T(8,128)(2,1)S(1)}, u32[]{:S(2)}, u32[]{:S(2)}) collective-permute-start(bf16[64,512]{1,0:T(8,128)(2,1)S(1)} %convolution_convert_fusion.6), channel_id=1, source_target_pairs={{0,2},{1,3},{2,0},{3,1},{4,6},{5,7},{6,4},{7,5},{8,10},{9,11},{10,... | collective-permute-start | bytes 196616 | tf_op jit(solution)/shard_map/ppermute | solution.py:40
  21.2 5.2 %collective-permute-start.5 = (bf16[64,512]{1,0:T(8,128)(2,1)S(1)}, bf16[64,512]{1,0:T(8,128)(2,1)S(1)}, u32[]{:S(2)}, u32[]{:S(2)}) collective-permute-start(bf16[64,512]{1,0:T(8,128)(2,1)S(1)} %convolution_convert_fusion.5), channel_id=1, source_target_pairs={{0,3},{1,2},{2,1},{3,0},{4,7},{5,6},{6,5},{7,4},{8,11},{9,10},{10,... | collective-permute-start | bytes 196616 | tf_op jit(solution)/shard_map/ppermute | solution.py:40
  28.4 13.3 %all-to-all-start = ((bf16[8,24,512]{2,1,0:T(8,128)(2,1)}), bf16[8,24,512]{2,1,0:T(8,128)(2,1)}, u32[]{:S(2)}, u32[]{:S(2)}) async-start(bf16[8,24,512]{2,1,0:T(8,128)(2,1)} %bitcast.7), calls=%async_computation | async-start | bytes 393216 | tf_op jit(solution)/shard_map/all_to_all | solution.py:131
  41.7 8.4 %collective-permute-start.6 = (bf16[192,512]{1,0:T(8,128)(2,1)}, bf16[192,512]{1,0:T(8,128)(2,1)}, u32[]{:S(2)}, u32[]{:S(2)}) collective-permute-start(bf16[192,512]{1,0:T(8,128)(2,1)} %bitcast.10), channel_id=1, source_target_pairs={{0,1},{1,0},{2,3},{3,2},{4,5},{5,4},{6,7},{7,6},{8,9},{9,8},{10,11... | collective-permute-start | bytes 589832 | tf_op jit(solution)/shard_map/ppermute | solution.py:40
  42.6 9.9 %collective-permute-start.7 = (bf16[192,512]{1,0:T(8,128)(2,1)}, bf16[192,512]{1,0:T(8,128)(2,1)}, u32[]{:S(2)}, u32[]{:S(2)}) collective-permute-start(bf16[192,512]{1,0:T(8,128)(2,1)} %bitcast.10), channel_id=1, source_target_pairs={{0,2},{1,3},{2,0},{3,1},{4,6},{5,7},{6,4},{7,5},{8,10},{9,11},{10,... | collective-permute-start | bytes 589832 | tf_op jit(solution)/shard_map/ppermute | solution.py:40
  43.7 9.9 %collective-permute-start.8 = (bf16[192,512]{1,0:T(8,128)(2,1)}, bf16[192,512]{1,0:T(8,128)(2,1)}, u32[]{:S(2)}, u32[]{:S(2)}) collective-permute-start(bf16[192,512]{1,0:T(8,128)(2,1)} %bitcast.10), channel_id=1, source_target_pairs={{0,3},{1,2},{2,1},{3,0},{4,7},{5,6},{6,5},{7,4},{8,11},{9,10},{10,... | collective-permute-start | bytes 589832 | tf_op jit(solution)/shard_map/ppermute | solution.py:40
  50.0 10.4 %copy-start.1 = (bf16[1,2048,896]{2,1,0:T(8,128)(2,1)S(1)}, bf16[1,2048,896]{2,1,0:T(8,128)(2,1)}, u32[]{:S(2)}) copy-start(bf16[1,2048,896]{2,1,0:T(8,128)(2,1)} %param.41) | copy-start | bytes 11010052
  61.7 3.2 %copy-start.2 = (bf16[1,896,2048]{2,1,0:T(8,128)(2,1)S(1)}, bf16[1,896,2048]{2,1,0:T(8,128)(2,1)}, u32[]{:S(2)}) copy-start(bf16[1,896,2048]{2,1,0:T(8,128)(2,1)} %param.43) | copy-start | bytes 11010052
  65.4 18.3 %copy-start.10 = (f32[64,2]{0,1:T(2,128)S(1)}, f32[64,2]{0,1:T(2,128)}, u32[]{:S(2)}) copy-start(f32[64,2]{0,1:T(2,128)} %param.40) | copy-start | bytes 1540
  65.4 18.4 %copy-start.6 = (pred[192,64,2]{0,1,2:T(32,128)(4,1)S(1)}, pred[192,64,2]{0,1,2:T(32,128)(4,1)}, u32[]{:S(2)}) copy-start(pred[192,64,2]{0,1,2:T(32,128)(4,1)} %get-tuple-element.27) | copy-start | bytes 73732
  66.2 6.7 %collective-permute-start.10 = (bf16[192,512]{1,0:T(8,128)(2,1)S(1)}, bf16[192,512]{1,0:T(8,128)(2,1)S(1)}, u32[]{:S(2)}, u32[]{:S(2)}) collective-permute-start(bf16[192,512]{1,0:T(8,128)(2,1)S(1)} %convolution_convert_fusion.2), channel_id=1, source_target_pairs={{0,2},{1,3},{2,0},{3,1},{4,6},{5,7},{6,4},{7,5},{8,10},{9,11},{10,... | collective-permute-start | bytes 589832 | tf_op jit(solution)/shard_map/ppermute | solution.py:40
  67.2 5.8 %collective-permute-start.9 = (bf16[192,512]{1,0:T(8,128)(2,1)S(1)}, bf16[192,512]{1,0:T(8,128)(2,1)S(1)}, u32[]{:S(2)}, u32[]{:S(2)}) collective-permute-start(bf16[192,512]{1,0:T(8,128)(2,1)S(1)} %convolution_convert_fusion.3), channel_id=1, source_target_pairs={{0,1},{1,0},{2,3},{3,2},{4,5},{5,4},{6,7},{7,6},{8,9},{9,8},{10,11... | collective-permute-start | bytes 589832 | tf_op jit(solution)/shard_map/ppermute | solution.py:40
  68.4 7.1 %collective-permute-start.11 = (bf16[192,512]{1,0:T(8,128)(2,1)S(1)}, bf16[192,512]{1,0:T(8,128)(2,1)S(1)}, u32[]{:S(2)}, u32[]{:S(2)}) collective-permute-start(bf16[192,512]{1,0:T(8,128)(2,1)S(1)} %convolution_convert_fusion.1), channel_id=1, source_target_pairs={{0,3},{1,2},{2,1},{3,0},{4,7},{5,6},{6,5},{7,4},{8,11},{9,10},{10,... | collective-permute-start | bytes 589832 | tf_op jit(solution)/shard_map/ppermute | solution.py:40
  76.6 13.2 %all-to-all-start.1 = ((bf16[8,24,512]{2,1,0:T(8,128)(2,1)}), bf16[8,24,512]{2,1,0:T(8,128)(2,1)S(1)}, u32[]{:S(2)}, u32[]{:S(2)}) async-start(bf16[8,24,512]{2,1,0:T(8,128)(2,1)} %bitcast.22), calls=%async_computation.1 | async-start | bytes 393216 | tf_op jit(solution)/shard_map/all_to_all | solution.py:164

commit v2 on v1

--- a/solution.py
+++ b/solution.py
@@ -38,6 +38,29 @@
 def partner_swap(value, offset):
     count = lax.axis_size("tp")
     return lax.ppermute(value, "tp", [(source, source ^ offset) for source in range(count)])
+
+
+def ep_swap(value, offset):
+    count = lax.axis_size("ep")
+    return lax.ppermute(value, "ep", [(source, source ^ offset) for source in range(count)])
+
+
+def to_experts(rows):
+    pairs = rows.shape[1]
+    near = rows[0]
+    crossed = ep_swap(rows[1], 1)
+    joined = jnp.stack([near, crossed], axis=1)
+    moved = [None] + [ep_swap(joined[step], 2 * step) for step in range(pairs - 1, 0, -1)][::-1]
+    moved[0] = joined[0]
+    return jnp.stack(moved, axis=0)
+
+
+def from_experts(rows):
+    pairs = rows.shape[0]
+    moved = [None] + [ep_swap(rows[step], 2 * step) for step in range(pairs - 1, 0, -1)][::-1]
+    moved[0] = rows[0]
+    moved = jnp.stack(moved, axis=1)
+    return jnp.stack([moved[0], ep_swap(moved[1], 1)], axis=0)
 
 
 def local(
@@ -121,20 +144,17 @@
     flat_route = route.reshape(-1)
     hits = (flat_route[:, None] == jnp.arange(experts)[None, :]).astype(jnp.int32)
     rank = jnp.sum((jnp.cumsum(hits, axis=0) - hits) * hits, axis=1)
-    slot = flat_route * slot_cap + rank
+    relative = flat_route ^ lax.axis_index("ep")
+    pairs = experts // 2
+    slot = ((relative % 2) * pairs + relative // 2) * slot_cap + rank
     slot_ids = jnp.arange(rows_all)
     picks = (slot[None, :] == slot_ids[:, None]).reshape(rows_all, seq_count, top_count)
     select = jnp.any(picks, axis=2).astype(jnp.bfloat16)
     combine = jnp.einsum("ask,sk->sa", picks.astype(jnp.float32), route_weight)
 
     outbound = jnp.dot(select, resid_part, preferred_element_type=jnp.float32).astype(jnp.bfloat16)
-    arrived = lax.all_to_all(
-        outbound.reshape(experts, slot_cap, local_width),
-        "ep",
-        split_axis=0,
-        concat_axis=0,
-        tiled=True,
-    ).reshape(rows_all, local_width)
+    arrived = to_experts(outbound.reshape(2, pairs, slot_cap, local_width))
+    arrived = arrived.reshape(rows_all, local_width)
     blocks = [(0, arrived)] + [(offset, partner_swap(arrived, offset)) for offset in offsets]
     gate_rows = up_rows = squares = 0.0
     for offset, block in blocks:
@@ -161,12 +181,8 @@
     back_rows = result(0).astype(jnp.float32)
     for block in arrived_results:
         back_rows = back_rows + block.astype(jnp.float32)
-    returned = lax.all_to_all(
-        back_rows.astype(jnp.bfloat16).reshape(experts, slot_cap, local_width),
-        "ep",
-        split_axis=0,
-        concat_axis=0,
-        tiled=True,
+    returned = from_experts(
+        back_rows.astype(jnp.bfloat16).reshape(pairs, 2, slot_cap, local_width)
     ).reshape(rows_all, local_width)
     expert_total = lax.dot_general(
         combine,

time: 91.5 us -> 85 us (0.929)
  waiting for transfers between devices: 27 us -> 21.9 us
  matrix products: 24.9 us -> 23.5 us
    all_to_all x2 -> x0, waiting for transfers between devices: 14.1 us -> none  [the longest x1 8.31 us: local(): lax.all_to_all(outbound.reshape(experts, slot_cap, local_width), 'ep', sp...]
    all_to_all x2 -> x0, starting transfers between devices: 9.73 us -> none  [the longest x1 4.88 us: local(): lax.all_to_all(outbound.reshape(experts, slot_cap, local_width), 'ep', sp...]
    ppermute x0 -> x8, waiting for transfers between devices: none -> 9.7 us  [ep_swap(): lax.ppermute(value, 'ep', [(source, source ^ offset) for source in range(...]
    ppermute x0 -> x8, starting transfers between devices: none -> 9.05 us  [ep_swap(): lax.ppermute(value, 'ep', [(source, source ^ offset) for source in range(...]
    convert_element_type x0 -> x1, other arithmetic: none -> 0.99 us  [local(): scaled = (values * gain).astype(jnp.bfloat16)]
    unnamed x28 -> x29, local copies, waits for them, and re-layouts: 2.47 us -> 2.49 us
  transfers between devices with their start and end apart: 14 -> 20, of which waited for: 9 -> 13; matrix products, arithmetic and copies ran while one was open for 14% -> 14% of each run, Pallas kernels for 0% -> 0%
where the time goes in v2:
time: 85 us; the launch traced here: 84.3 us
  starting transfers between devices  24.3 us (29%)
  matrix products  23.5 us (28%)
  waiting for transfers between devices  21.9 us (26%)
  other arithmetic  8.86 us (10%)
  local copies, waits for them, and re-layouts  4.58 us (5%)
  between operations  1.15 us (1%)
    ppermute x12, starting transfers between devices, partner_swap(): lax.ppermute(value, 'tp', [(source, source ^ offset) for source in range(...  15.3 us
    ppermute x12, waiting for transfers between devices, partner_swap(): lax.ppermute(value, 'tp', [(source, source ^ offset) for source in range(...  12.2 us
    ppermute x8, waiting for transfers between devices, ep_swap(): lax.ppermute(value, 'ep', [(source, source ^ offset) for source in range(...  9.7 us
    ppermute x8, starting transfers between devices, ep_swap(): lax.ppermute(value, 'ep', [(source, source ^ offset) for source in range(...  9.05 us
    dot_general x4, matrix products, local(): jnp.dot(scaled, rows_of(up_local, offset, local_width), preferred_element...  6.67 us
    dot_general x4, matrix products, local(): jnp.dot(scaled, rows_of(gate_local, offset, local_width), preferred_eleme...  6.03 us
    reduce_sum x4, other arithmetic, local(): squares = squares + jnp.sum(values * values, axis=1, keepdims=True)  4 us
    unnamed x29, local copies, waits for them, and re-layouts  2.49 us
  transfers between devices with their start and end apart: 20, of which 13 were waited for; matrix products, arithmetic and copies ran while one was open for 14% of the time, Pallas kernels for 0%

profile of v2, /device:TPU:0, one launch (start us, length us, event | category | flops | bytes accessed | tf_op | source)
XLA Modules:
  0.0 84.3 jit_solution(6423310976163191921)
XLA Ops:
  0.7 0.8 exp.13
  1.5 1.1 %fusion.44 = f32[64]{0:T(128)S(1)} fusion(bf16[64,2048]{1,0:T(8,128)(2,1)} %param.22), kind=kLoop, calls=%fused_computation.64 | loop fusion | flops 393152 | bytes 262400 | tf_op jit(solution)/shard_map/reduce_sum | solution.py:11
  2.6 1.7 %convolution_convert_fusion.9 = bf16[64,256]{1,0:T(8,128)(2,1)S(1)} fusion(bf16[2048,256]{1,0:T(8,128)(2,1)} %param.24, bf16[64,2048]{1,0:T(8,128)(2,1)} %param.22, f32[2048]{0:T(1024)} %param.23, f32[64]{0:T(128)S(1)} %add_rsqrt_fusion.1), kind=kOutput, calls=%fused_computation.31 | convolution fusion | flops 67649536 | bytes 1351936 | tf_op jit(solution)/shard_map/dot_general | solution.py:112
  4.4 1.1 %fusion.130 = f32[16,64,64]{2,1,0:T(8,128)S(1)} fusion(bf16[64,16,16]{0,2,1:T(8,128)(2,1)S(1)} %bitcast.122, bf16[16,16,64]{2,1,0:T(8,128)(2,1)} %param.29), kind=kOutput, calls=%fused_computation.177 | convolution fusion | flops 2097152 | bytes 327680 | tf_op jit(solution)/shard_map/sgh,ghp->sgp/dot_general | solution.py:27
  5.5 0.8 cosine_multiply_fusion
  6.4 1.8 %bitcast_add_fusion = (f32[64,16,64]{2,0,1:T(8,128)S(1)}, f32[64,16,64]{2,0,1:T(8,128)S(1)}) fusion(f32[16,64,64]{2,1,0:T(8,128)S(1)} %fusion.130, f32[64,16,64]{2,1,0:T(8,128)} %param.34, f32[64,16,64]{2,1,0:T(8,128)} %param.33, f32[16,64]{1,0:T(8,128)S(1)} %get-tuple-element.33, f32[16,64]{1,0:T(8,128)S(1)} %get-tuple-element.34, ...), kind=kOutput, calls=%fused_computation.67 | convolution fusion | flops 3014656 | bytes 1392640 | tf_op jit(solution)/shard_map/sgh,ghp->sgp/dot_general | solution.py:26
  9.2 3.0 %collective-permute-start = (bf16[64,256]{0,1:T(8,128)(2,1)S(1)}, bf16[64,256]{0,1:T(8,128)(2,1)S(1)}, u32[]{:S(2)}, u32[]{:S(2)}) collective-permute-start(bf16[64,256]{0,1:T(8,128)(2,1)S(1)} %bitcast.126), channel_id=1, source_target_pairs={{0,1},{1,0},{2,3},{3,2},{4,5},{5,4},{6,7},{7,6},{8,9},{9,8},{10,11... | collective-permute-start | bytes 98312 | tf_op jit(solution)/shard_map/ppermute | solution.py:40
  12.3 1.5 %collective-permute-start.2 = (bf16[64,256]{0,1:T(8,128)(2,1)S(1)}, bf16[64,256]{0,1:T(8,128)(2,1)S(1)}, u32[]{:S(2)}, u32[]{:S(2)}) collective-permute-start(bf16[64,256]{0,1:T(8,128)(2,1)S(1)} %bitcast.127), channel_id=1, source_target_pairs={{0,3},{1,2},{2,1},{3,0},{4,7},{5,6},{6,5},{7,4},{8,11},{9,10},{10,... | collective-permute-start | bytes 98312 | tf_op jit(solution)/shard_map/ppermute | solution.py:40
  15.3 2.2 %collective-permute-done.2 = bf16[64,256]{0,1:T(8,128)(2,1)S(1)} collective-permute-done((bf16[64,256]{0,1:T(8,128)(2,1)S(1)}, bf16[64,256]{0,1:T(8,128)(2,1)S(1)}, u32[]{:S(2)}, u32[]{:S(2)}) %collective-permute-start.2) | collective-permute-done | bytes 32800 | tf_op jit(solution)/shard_map/ppermute | solution.py:40
  18.7 1.3 %collective-permute-start.3 = (bf16[64,512]{1,0:T(8,128)(2,1)S(1)}, bf16[64,512]{1,0:T(8,128)(2,1)S(1)}, u32[]{:S(2)}, u32[]{:S(2)}) collective-permute-start(bf16[64,512]{1,0:T(8,128)(2,1)S(1)} %convolution_convert_fusion.7), channel_id=1, source_target_pairs={{0,1},{1,0},{2,3},{3,2},{4,5},{5,4},{6,7},{7,6},{8,9},{9,8},{10,11... | collective-permute-start | bytes 196616 | tf_op jit(solution)/shard_map/ppermute | solution.py:40
  20.2 0.9 %collective-permute-start.4 = (bf16[64,512]{1,0:T(8,128)(2,1)S(1)}, bf16[64,512]{1,0:T(8,128)(2,1)S(1)}, u32[]{:S(2)}, u32[]{:S(2)}) collective-permute-start(bf16[64,512]{1,0:T(8,128)(2,1)S(1)} %convolution_convert_fusion.6), channel_id=1, source_target_pairs={{0,2},{1,3},{2,0},{3,1},{4,6},{5,7},{6,4},{7,5},{8,10},{9,11},{10,... | collective-permute-start | bytes 196616 | tf_op jit(solution)/shard_map/ppermute | solution.py:40
  21.2 1.5 %collective-permute-start.5 = (bf16[64,512]{1,0:T(8,128)(2,1)S(1)}, bf16[64,512]{1,0:T(8,128)(2,1)S(1)}, u32[]{:S(2)}, u32[]{:S(2)}) collective-permute-start(bf16[64,512]{1,0:T(8,128)(2,1)S(1)} %convolution_convert_fusion.5), channel_id=1, source_target_pairs={{0,3},{1,2},{2,1},{3,0},{4,7},{5,6},{6,5},{7,4},{8,11},{9,10},{10,... | collective-permute-start | bytes 196616 | tf_op jit(solution)/shard_map/ppermute | solution.py:40
  23.4 1.7 %collective-permute-done.4 = bf16[64,512]{1,0:T(8,128)(2,1)S(1)} collective-permute-done((bf16[64,512]{1,0:T(8,128)(2,1)S(1)}, bf16[64,512]{1,0:T(8,128)(2,1)S(1)}, u32[]{:S(2)}, u32[]{:S(2)}) %collective-permute-start.4) | collective-permute-done | bytes 65568 | tf_op jit(solution)/shard_map/ppermute | solution.py:40
  25.1 1.3 %collective-permute-done.5 = bf16[64,512]{1,0:T(8,128)(2,1)S(1)} collective-permute-done((bf16[64,512]{1,0:T(8,128)(2,1)S(1)}, bf16[64,512]{1,0:T(8,128)(2,1)S(1)}, u32[]{:S(2)}, u32[]{:S(2)}) %collective-permute-start.5) | collective-permute-done | bytes 65568 | tf_op jit(solution)/shard_map/ppermute | solution.py:40
  26.4 1.0 %add_convert_fusion.2 = bf16[64,512]{1,0:T(8,128)(2,1)S(1)} fusion(bf16[64,512]{1,0:T(8,128)(2,1)S(1)} %collective-permute-done.5, bf16[64,512]{1,0:T(8,128)(2,1)S(1)} %collective-permute-done.4, bf16[64,512]{1,0:T(8,128)(2,1)S(1)} %collective-permute-done.3, bf16[64,2048]{1,0:T(8,128)(2,1)} %param.22, s32[]{:T(128)S(6)} %select_n.61, ...), kind=kOutput, calls=%fused_computation.114 | convolution fusion | flops 17137664 | bytes 623616 | tf_op jit(solution)/shard_map/dot_general | solution.py:131
  27.8 1.3 %collective-permute-done.6 = bf16[4,24,512]{2,1,0:T(8,128)(2,1)S(1)} collective-permute-done((bf16[4,24,512]{2,1,0:T(8,128)(2,1)S(1)}, bf16[4,24,512]{2,1,0:T(8,128)(2,1)S(1)}, u32[]{:S(2)}, u32[]{:S(2)}) %collective-permute-start.6) | collective-permute-done | bytes 98336 | tf_op jit(solution)/shard_map/ppermute | solution.py:45
  29.1 1.6 %collective-permute-start.7 = (bf16[2,24,512]{2,1,0:T(8,128)(2,1)S(1)}, bf16[2,24,512]{2,1,0:T(8,128)(2,1)S(1)}, u32[]{:S(2)}, u32[]{:S(2)}) collective-permute-start(bf16[2,24,512]{2,1,0:T(8,128)(2,1)S(1)} %get-tuple-element.26), channel_id=1, source_target_pairs={{0,8},{4,12},{8,0},{12,4},{16,24},{20,28},{24,16},{28,20},{1,9},{5... | collective-permute-start | bytes 147464 | tf_op jit(solution)/shard_map/ppermute | solution.py:45
  30.8 2.6 %collective-permute-start.8 = (bf16[2,24,512]{2,1,0:T(8,128)(2,1)S(1)}, bf16[2,24,512]{2,1,0:T(8,128)(2,1)S(1)}, u32[]{:S(2)}, u32[]{:S(2)}) collective-permute-start(bf16[2,24,512]{2,1,0:T(8,128)(2,1)S(1)} %get-tuple-element.28), channel_id=1, source_target_pairs={{0,16},{4,20},{8,24},{12,28},{16,0},{20,4},{24,8},{28,12},{1,17},{... | collective-permute-start | bytes 147464 | tf_op jit(solution)/shard_map/ppermute | solution.py:45
  33.7 3.0 %collective-permute-done.8 = bf16[2,24,512]{2,1,0:T(8,128)(2,1)S(1)} collective-permute-done((bf16[2,24,512]{2,1,0:T(8,128)(2,1)S(1)}, bf16[2,24,512]{2,1,0:T(8,128)(2,1)S(1)}, u32[]{:S(2)}, u32[]{:S(2)}) %collective-permute-start.8) | collective-permute-done | bytes 49184 | tf_op jit(solution)/shard_map/ppermute | solution.py:45
  36.6 2.6 %collective-permute-done.9 = bf16[2,24,512]{2,1,0:T(8,128)(2,1)S(1)} collective-permute-done((bf16[2,24,512]{2,1,0:T(8,128)(2,1)S(1)}, bf16[2,24,512]{2,1,0:T(8,128)(2,1)S(1)}, u32[]{:S(2)}, u32[]{:S(2)}) %collective-permute-start.9) | collective-permute-done | bytes 49184 | tf_op jit(solution)/shard_map/ppermute | solution.py:45
  39.9 1.0 %collective-permute-start.10 = (bf16[192,512]{1,0:T(8,128)(2,1)}, bf16[192,512]{1,0:T(8,128)(2,1)}, u32[]{:S(2)}, u32[]{:S(2)}) collective-permute-start(bf16[192,512]{1,0:T(8,128)(2,1)} %bitcast.18), channel_id=1, source_target_pairs={{0,1},{1,0},{2,3},{3,2},{4,5},{5,4},{6,7},{7,6},{8,9},{9,8},{10,11... | collective-permute-start | bytes 589832 | tf_op jit(solution)/shard_map/ppermute | solution.py:40
  40.9 1.1 %collective-permute-start.11 = (bf16[192,512]{1,0:T(8,128)(2,1)}, bf16[192,512]{1,0:T(8,128)(2,1)}, u32[]{:S(2)}, u32[]{:S(2)}) collective-permute-start(bf16[192,512]{1,0:T(8,128)(2,1)} %bitcast.18), channel_id=1, source_target_pairs={{0,2},{1,3},{2,0},{3,1},{4,6},{5,7},{6,4},{7,5},{8,10},{9,11},{10,... | collective-permute-start | bytes 589832 | tf_op jit(solution)/shard_map/ppermute | solution.py:40
  42.0 1.5 %collective-permute-start.12 = (bf16[192,512]{1,0:T(8,128)(2,1)}, bf16[192,512]{1,0:T(8,128)(2,1)}, u32[]{:S(2)}, u32[]{:S(2)}) collective-permute-start(bf16[192,512]{1,0:T(8,128)(2,1)} %bitcast.18), channel_id=1, source_target_pairs={{0,3},{1,2},{2,1},{3,0},{4,7},{5,6},{6,5},{7,4},{8,11},{9,10},{10,... | collective-permute-start | bytes 589832 | tf_op jit(solution)/shard_map/ppermute | solution.py:40
  43.4 1.0 %fusion.47 = bf16[4,2,24,512]{3,2,1,0:T(8,128)(2,1)S(1)} fusion(bf16[4,2,24,512]{3,2,1,0:T(8,128)(2,1)} %get-tuple-element.16, f32[512]{0:T(512)S(1)} %get-tuple-element.37), kind=kLoop, calls=%fused_computation.77 | loop fusion | flops 294912 | bytes 395264 | tf_op jit(solution)/shard_map/convert_element_type | solution.py:164
  44.4 1.6 %fusion.24 = f32[192,896]{1,0:T(8,128)S(1)} fusion(bf16[192,512]{1,0:T(8,128)(2,1)S(1)} %bitcast.120, bf16[1,2048,896]{2,1,0:T(8,128)(2,1)} %param.42, s32[]{:T(128)S(6)} %select_n.61), kind=kOutput, calls=%fused_computation.41 | convolution fusion | flops 176160768 | bytes 1802244 | tf_op jit(solution)/shard_map/dot_general | solution.py:168
  46.0 1.6 %fusion.30 = f32[192,896]{1,0:T(8,128)S(1)} fusion(bf16[192,512]{1,0:T(8,128)(2,1)S(1)} %bitcast.121, bf16[1,2048,896]{2,1,0:T(8,128)(2,1)} %param.41, s32[]{:T(128)S(6)} %select_n.61), kind=kOutput, calls=%fused_computation.47 | convolution fusion | flops 176160768 | bytes 1802244 | tf_op jit(solution)/shard_map/dot_general | solution.py:165
  48.2 1.2 %fusion.50 = f32[192]{0:T(256)S(1)} fusion(bf16[192,512]{1,0:T(8,128)(2,1)} %collective-permute-done.10), kind=kLoop, calls=%fused_computation.80 | loop fusion | flops 294720 | bytes 197376 | tf_op jit(solution)/shard_map/reduce_sum | solution.py:162
  49.4 1.1 %collective-permute-done.11 = bf16[192,512]{1,0:T(8,128)(2,1)} collective-permute-done((bf16[192,512]{1,0:T(8,128)(2,1)}, bf16[192,512]{1,0:T(8,128)(2,1)}, u32[]{:S(2)}, u32[]{:S(2)}) %collective-permute-start.11) | collective-permute-done | bytes 196640 | tf_op jit(solution)/shard_map/ppermute | solution.py:40
  50.5 1.0 %fusion.52 = f32[192]{0:T(256)S(1)} fusion(bf16[192,512]{1,0:T(8,128)(2,1)} %collective-permute-done.11), kind=kLoop, calls=%fused_computation.82 | loop fusion | flops 294720 | bytes 197376 | tf_op jit(solution)/shard_map/reduce_sum | solution.py:162
  51.6 1.0 %fusion.54 = f32[192]{0:T(256)S(1)} fusion(bf16[192,512]{1,0:T(8,128)(2,1)} %collective-permute-done.12), kind=kLoop, calls=%fused_computation.84 | loop fusion | flops 294720 | bytes 197376 | tf_op jit(solution)/shard_map/reduce_sum | solution.py:162
  53.3 1.7 %fusion.26 = f32[192,896]{1,0:T(8,128)S(1)} fusion(bf16[1,2048,896]{2,1,0:T(8,128)(2,1)} %param.41, s32[]{:T(128)S(6)} %select_n.68, bf16[192,512]{1,0:T(8,128)(2,1)} %collective-permute-done.12, f32[512]{0:T(512)S(1)} %get-tuple-element.38), kind=kOutput, calls=%fused_computation.43 | convolution fusion | flops 176455680 | bytes 1804292 | tf_op jit(solution)/shard_map/dot_general | solution.py:165
  55.0 1.7 %fusion.20 = f32[192,896]{1,0:T(8,128)S(1)} fusion(bf16[1,2048,896]{2,1,0:T(8,128)(2,1)} %param.42, s32[]{:T(128)S(6)} %select_n.68, bf16[192,512]{1,0:T(8,128)(2,1)} %collective-permute-done.12, f32[512]{0:T(512)S(1)} %get-tuple-element.38), kind=kOutput, calls=%fused_computation.37 | convolution fusion | flops 176455680 | bytes 1804292 | tf_op jit(solution)/shard_map/dot_general | solution.py:168
  56.7 1.7 %convolution_add_fusion.1 = f32[192,896]{1,0:T(8,128)S(1)} fusion(f32[192,896]{1,0:T(8,128)S(1)} %fusion.24, bf16[1,2048,896]{2,1,0:T(8,128)(2,1)} %param.42, s32[]{:T(128)S(6)} %select_n.66, bf16[192,512]{1,0:T(8,128)(2,1)} %collective-permute-done.10, f32[512]{0:T(512)S(1)} %get-tuple-element.36), kind=kOutput, calls=%fused_computation.1 | convolution fusion | flops 176627712 | bytes 2492420 | tf_op jit(solution)/shard_map/dot_general | solution.py:168
  58.4 1.3 %convolution_add_fusion.3 = f32[192,896]{1,0:T(8,128)S(1)} fusion(f32[192,896]{1,0:T(8,128)S(1)} %fusion.30, bf16[1,2048,896]{2,1,0:T(8,128)(2,1)S(1)} %copy-done.1, s32[]{:T(128)S(6)} %select_n.66, bf16[192,512]{1,0:T(8,128)(2,1)} %collective-permute-done.10, f32[512]{0:T(512)S(1)} %get-tuple-element.36), kind=kOutput, calls=%fused_computation.3 | convolution fusion | flops 176627712 | bytes 2492420 | tf_op jit(solution)/shard_map/dot_general | solution.py:165
  59.8 1.5 %fusion.1 = f32[192,896]{1,0:T(8,128)S(1)} fusion(f32[192,896]{1,0:T(8,128)S(1)} %fusion.26, f32[192,896]{1,0:T(8,128)S(1)} %convolution_add_fusion.3, bf16[1,2048,896]{2,1,0:T(8,128)(2,1)S(1)} %copy-done.1, s32[]{:T(128)S(6)} %select_n.67, f32[192]{0:T(256)S(1)} %add_rsqrt_fusion, bf16[192,512]{1,0:T(8,128)(2,1)} %collective-permute-done.11, ...), kind=kOutput, calls=%fused_computation.5 | convolution fusion | flops 176971776 | bytes 3181572 | tf_op jit(solution)/shard_map/dot_general | solution.py:165
  61.2 1.7 %multiply_convert_fusion = bf16[192,896]{1,0:T(8,128)(2,1)S(1)} fusion(f32[192,896]{1,0:T(8,128)S(1)} %fusion.1, f32[192]{0:T(256)S(1)} %add_rsqrt_fusion, f32[192,896]{1,0:T(8,128)S(1)} %fusion.20, f32[192,896]{1,0:T(8,128)S(1)} %convolution_add_fusion.1, bf16[1,2048,896]{2,1,0:T(8,128)(2,1)} %param.42, s32[]{:T(128)S(6)} %select_n.67, ...), kind=kOutput, calls=%fused_computation.61 | convolution fusion | flops 178003968 | bytes 3525380 | tf_op jit(solution)/shard_map/dot_general | solution.py:168
  64.2 1.0 %collective-permute-start.13 = (bf16[192,512]{1,0:T(8,128)(2,1)S(1)}, bf16[192,512]{1,0:T(8,128)(2,1)S(1)}, u32[]{:S(2)}, u32[]{:S(2)}) collective-permute-start(bf16[192,512]{1,0:T(8,128)(2,1)S(1)} %convolution_convert_fusion.3), channel_id=1, source_target_pairs={{0,1},{1,0},{2,3},{3,2},{4,5},{5,4},{6,7},{7,6},{8,9},{9,8},{10,11... | collective-permute-start | bytes 589832 | tf_op jit(solution)/shard_map/ppermute | solution.py:40
  65.2 1.2 %collective-permute-start.14 = (bf16[192,512]{1,0:T(8,128)(2,1)S(1)}, bf16[192,512]{1,0:T(8,128)(2,1)S(1)}, u32[]{:S(2)}, u32[]{:S(2)}) collective-permute-start(bf16[192,512]{1,0:T(8,128)(2,1)S(1)} %convolution_convert_fusion.2), channel_id=1, source_target_pairs={{0,2},{1,3},{2,0},{3,1},{4,6},{5,7},{6,4},{7,5},{8,10},{9,11},{10,... | collective-permute-start | bytes 589832 | tf_op jit(solution)/shard_map/ppermute | solution.py:40
  66.4 1.3 %collective-permute-start.15 = (bf16[192,512]{1,0:T(8,128)(2,1)S(1)}, bf16[192,512]{1,0:T(8,128)(2,1)S(1)}, u32[]{:S(2)}, u32[]{:S(2)}) collective-permute-start(bf16[192,512]{1,0:T(8,128)(2,1)S(1)} %convolution_convert_fusion.1), channel_id=1, source_target_pairs={{0,3},{1,2},{2,1},{3,0},{4,7},{5,6},{6,5},{7,4},{8,11},{9,10},{10,... | collective-permute-start | bytes 589832 | tf_op jit(solution)/shard_map/ppermute | solution.py:40
  67.8 2.2 %collective-permute-done.13 = bf16[192,512]{1,0:T(8,128)(2,1)S(1)} collective-permute-done((bf16[192,512]{1,0:T(8,128)(2,1)S(1)}, bf16[192,512]{1,0:T(8,128)(2,1)S(1)}, u32[]{:S(2)}, u32[]{:S(2)}) %collective-permute-start.13) | collective-permute-done | bytes 196640 | tf_op jit(solution)/shard_map/ppermute | solution.py:40
  69.9 1.8 %collective-permute-done.14 = bf16[192,512]{1,0:T(8,128)(2,1)S(1)} collective-permute-done((bf16[192,512]{1,0:T(8,128)(2,1)S(1)}, bf16[192,512]{1,0:T(8,128)(2,1)S(1)}, u32[]{:S(2)}, u32[]{:S(2)}) %collective-permute-start.14) | collective-permute-done | bytes 196640 | tf_op jit(solution)/shard_map/ppermute | solution.py:40
  71.8 1.2 %collective-permute-done.15 = bf16[192,512]{1,0:T(8,128)(2,1)S(1)} collective-permute-done((bf16[192,512]{1,0:T(8,128)(2,1)S(1)}, bf16[192,512]{1,0:T(8,128)(2,1)S(1)}, u32[]{:S(2)}, u32[]{:S(2)}) %collective-permute-start.15) | collective-permute-done | bytes 196640 | tf_op jit(solution)/shard_map/ppermute | solution.py:40
  73.7 1.3 %collective-permute-start.17 = (bf16[2,24,512]{2,1,0:T(8,128)(2,1)S(1)}, bf16[2,24,512]{2,1,0:T(8,128)(2,1)S(1)}, u32[]{:S(2)}, u32[]{:S(2)}) collective-permute-start(bf16[2,24,512]{2,1,0:T(8,128)(2,1)S(1)} %bitcast.141), channel_id=1, source_target_pairs={{0,16},{4,20},{8,24},{12,28},{16,0},{20,4},{24,8},{28,12},{1,17},{... | collective-permute-start | bytes 147464 | tf_op jit(solution)/shard_map/ppermute | solution.py:45
  75.0 2.9 %collective-permute-start.18 = (bf16[2,24,512]{2,1,0:T(8,128)(2,1)S(1)}, bf16[2,24,512]{2,1,0:T(8,128)(2,1)S(1)}, u32[]{:S(2)}, u32[]{:S(2)}) collective-permute-start(bf16[2,24,512]{2,1,0:T(8,128)(2,1)S(1)} %bitcast.139), channel_id=1, source_target_pairs={{0,24},{4,28},{8,16},{12,20},{16,8},{20,12},{24,0},{28,4},{1,25},{... | collective-permute-start | bytes 147464 | tf_op jit(solution)/shard_map/ppermute | solution.py:45
  78.7 2.2 %collective-permute-done.18 = bf16[2,24,512]{2,1,0:T(8,128)(2,1)S(1)} collective-permute-done((bf16[2,24,512]{2,1,0:T(8,128)(2,1)S(1)}, bf16[2,24,512]{2,1,0:T(8,128)(2,1)S(1)}, u32[]{:S(2)}, u32[]{:S(2)}) %collective-permute-start.18) | collective-permute-done | bytes 49184 | tf_op jit(solution)/shard_map/ppermute | solution.py:45
  81.2 1.1 %copy.82 = f32[64,16,64]{2,1,0:T(8,128)} copy(f32[64,16,64]{2,0,1:T(8,128)S(1)} %get-tuple-element.18) | data formatting | bytes 524288
  82.3 1.1 %copy.83 = f32[64,16,64]{2,1,0:T(8,128)} copy(f32[64,16,64]{2,0,1:T(8,128)S(1)} %get-tuple-element.17) | data formatting | bytes 524288
  83.5 0.9 %add_convert_fusion.1 = bf16[64,512]{1,0:T(8,128)(2,1)} fusion(bf16[64,512]{1,0:T(8,128)(2,1)S(1)} %add_convert_fusion.2, bf16[192,512]{1,0:T(8,128)(2,1)S(1)} %bitcast.125, f32[64,1,192]{2,1,0:T(1,128)S(1)} %fusion.64), kind=kOutput, calls=%fused_computation.112 | convolution fusion | flops 75595776 | bytes 376832 | tf_op jit(solution)/shard_map/dot_general | solution.py:187
  (76 shorter events, 10.5 us)
Async XLA Ops:
  0.6 17.9 %copy-start = (bf16[256,2048]{1,0:T(8,128)(2,1)S(1)}, bf16[256,2048]{1,0:T(8,128)(2,1)}, u32[]{:S(2)}) copy-start(bf16[256,2048]{1,0:T(8,128)(2,1)} %param.37) | copy-start | bytes 3145732
  0.6 7.5 %copy-start.4 = (bf16[16,16,64]{2,1,0:T(8,128)(2,1)S(1)}, bf16[16,16,64]{2,1,0:T(8,128)(2,1)}, u32[]{:S(2)}) copy-start(bf16[16,16,64]{2,1,0:T(8,128)(2,1)} %param.30) | copy-start | bytes 98308
  0.7 8.0 %copy-start.5 = (bf16[16,16,64]{2,1,0:T(8,128)(2,1)S(1)}, bf16[16,16,64]{2,1,0:T(8,128)(2,1)}, u32[]{:S(2)}) copy-start(bf16[16,16,64]{2,1,0:T(8,128)(2,1)} %param.31) | copy-start | bytes 98308
  0.7 8.0 %copy-start.7 = (f32[16,16]{1,0:T(8,128)S(1)}, f32[16,16]{1,0:T(8,128)}, u32[]{:S(2)}) copy-start(f32[16,16]{1,0:T(8,128)} %param.32) | copy-start | bytes 3076
  0.7 13.1 %copy-start.9 = (s32[64,2]{0,1:T(2,128)S(1)}, s32[64,2]{0,1:T(2,128)}, u32[]{:S(2)}) copy-start(s32[64,2]{0,1:T(2,128)} %param.39) | copy-start | bytes 1540
  0.7 14.0 %copy-start.3 = (bf16[1024,256]{1,0:T(8,128)(2,1)S(1)}, bf16[1024,256]{1,0:T(8,128)(2,1)}, u32[]{:S(2)}) copy-start(bf16[1024,256]{1,0:T(8,128)(2,1)} %param.35) | copy-start | bytes 1572868
  2.6 15.7 %copy-start.11 = (f32[256]{0:T(256)S(1)}, f32[256]{0:T(256)}, u32[]{:S(2)}) copy-start(f32[256]{0:T(256)} %param.36) | copy-start | bytes 3076
  8.1 25.4 %copy-start.8 = (f32[2048]{0:T(1024)S(1)}, f32[2048]{0:T(1024)}, u32[]{:S(2)}) copy-start(f32[2048]{0:T(1024)} %param.38) | copy-start | bytes 24580
  9.2 5.8 %collective-permute-start = (bf16[64,256]{0,1:T(8,128)(2,1)S(1)}, bf16[64,256]{0,1:T(8,128)(2,1)S(1)}, u32[]{:S(2)}, u32[]{:S(2)}) collective-permute-start(bf16[64,256]{0,1:T(8,128)(2,1)S(1)} %bitcast.126), channel_id=1, source_target_pairs={{0,1},{1,0},{2,3},{3,2},{4,5},{5,4},{6,7},{7,6},{8,9},{9,8},{10,11... | collective-permute-start | bytes 98312 | tf_op jit(solution)/shard_map/ppermute | solution.py:40
  12.3 5.2 %collective-permute-start.2 = (bf16[64,256]{0,1:T(8,128)(2,1)S(1)}, bf16[64,256]{0,1:T(8,128)(2,1)S(1)}, u32[]{:S(2)}, u32[]{:S(2)}) collective-permute-start(bf16[64,256]{0,1:T(8,128)(2,1)S(1)} %bitcast.127), channel_id=1, source_target_pairs={{0,3},{1,2},{2,1},{3,0},{4,7},{5,6},{6,5},{7,4},{8,11},{9,10},{10,... | collective-permute-start | bytes 98312 | tf_op jit(solution)/shard_map/ppermute | solution.py:40
  13.8 4.5 %collective-permute-start.1 = (bf16[64,256]{0,1:T(8,128)(2,1)S(1)}, bf16[64,256]{0,1:T(8,128)(2,1)S(1)}, u32[]{:S(2)}, u32[]{:S(2)}) collective-permute-start(bf16[64,256]{0,1:T(8,128)(2,1)S(1)} %bitcast.128), channel_id=1, source_target_pairs={{0,2},{1,3},{2,0},{3,1},{4,6},{5,7},{6,4},{7,5},{8,10},{9,11},{10,... | collective-permute-start | bytes 98312 | tf_op jit(solution)/shard_map/ppermute | solution.py:40
  18.7 4.7 %collective-permute-start.3 = (bf16[64,512]{1,0:T(8,128)(2,1)S(1)}, bf16[64,512]{1,0:T(8,128)(2,1)S(1)}, u32[]{:S(2)}, u32[]{:S(2)}) collective-permute-start(bf16[64,512]{1,0:T(8,128)(2,1)S(1)} %convolution_convert_fusion.7), channel_id=1, source_target_pairs={{0,1},{1,0},{2,3},{3,2},{4,5},{5,4},{6,7},{7,6},{8,9},{9,8},{10,11... | collective-permute-start | bytes 196616 | tf_op jit(solution)/shard_map/ppermute | solution.py:40
  20.2 4.9 %collective-permute-start.4 = (bf16[64,512]{1,0:T(8,128)(2,1)S(1)}, bf16[64,512]{1,0:T(8,128)(2,1)S(1)}, u32[]{:S(2)}, u32[]{:S(2)}) collective-permute-start(bf16[64,512]{1,0:T(8,128)(2,1)S(1)} %convolution_convert_fusion.6), channel_id=1, source_target_pairs={{0,2},{1,3},{2,0},{3,1},{4,6},{5,7},{6,4},{7,5},{8,10},{9,11},{10,... | collective-permute-start | bytes 196616 | tf_op jit(solution)/shard_map/ppermute | solution.py:40
  21.2 5.2 %collective-permute-start.5 = (bf16[64,512]{1,0:T(8,128)(2,1)S(1)}, bf16[64,512]{1,0:T(8,128)(2,1)S(1)}, u32[]{:S(2)}, u32[]{:S(2)}) collective-permute-start(bf16[64,512]{1,0:T(8,128)(2,1)S(1)} %convolution_convert_fusion.5), channel_id=1, source_target_pairs={{0,3},{1,2},{2,1},{3,0},{4,7},{5,6},{6,5},{7,4},{8,11},{9,10},{10,... | collective-permute-start | bytes 196616 | tf_op jit(solution)/shard_map/ppermute | solution.py:40
  27.7 1.4 %collective-permute-start.6 = (bf16[4,24,512]{2,1,0:T(8,128)(2,1)S(1)}, bf16[4,24,512]{2,1,0:T(8,128)(2,1)S(1)}, u32[]{:S(2)}, u32[]{:S(2)}) collective-permute-start(bf16[4,24,512]{2,1,0:T(8,128)(2,1)S(1)} %bitcast.135), channel_id=1, source_target_pairs={{0,4},{4,0},{8,12},{12,8},{16,20},{20,16},{24,28},{28,24},{1,5},{5... | collective-permute-start | bytes 294920 | tf_op jit(solution)/shard_map/ppermute | solution.py:45
  29.1 4.5 %collective-permute-start.7 = (bf16[2,24,512]{2,1,0:T(8,128)(2,1)S(1)}, bf16[2,24,512]{2,1,0:T(8,128)(2,1)S(1)}, u32[]{:S(2)}, u32[]{:S(2)}) collective-permute-start(bf16[2,24,512]{2,1,0:T(8,128)(2,1)S(1)} %get-tuple-element.26), channel_id=1, source_target_pairs={{0,8},{4,12},{8,0},{12,4},{16,24},{20,28},{24,16},{28,20},{1,9},{5... | collective-permute-start | bytes 147464 | tf_op jit(solution)/shard_map/ppermute | solution.py:45
  30.8 5.9 %collective-permute-start.8 = (bf16[2,24,512]{2,1,0:T(8,128)(2,1)S(1)}, bf16[2,24,512]{2,1,0:T(8,128)(2,1)S(1)}, u32[]{:S(2)}, u32[]{:S(2)}) collective-permute-start(bf16[2,24,512]{2,1,0:T(8,128)(2,1)S(1)} %get-tuple-element.28), channel_id=1, source_target_pairs={{0,16},{4,20},{8,24},{12,28},{16,0},{20,4},{24,8},{28,12},{1,17},{... | collective-permute-start | bytes 147464 | tf_op jit(solution)/shard_map/ppermute | solution.py:45
  33.3 5.9 %collective-permute-start.9 = (bf16[2,24,512]{2,1,0:T(8,128)(2,1)S(1)}, bf16[2,24,512]{2,1,0:T(8,128)(2,1)S(1)}, u32[]{:S(2)}, u32[]{:S(2)}) collective-permute-start(bf16[2,24,512]{2,1,0:T(8,128)(2,1)S(1)} %get-tuple-element.27), channel_id=1, source_target_pairs={{0,24},{4,28},{8,16},{12,20},{16,8},{20,12},{24,0},{28,4},{1,25},{... | collective-permute-start | bytes 147464 | tf_op jit(solution)/shard_map/ppermute | solution.py:45
  39.9 8.3 %collective-permute-start.10 = (bf16[192,512]{1,0:T(8,128)(2,1)}, bf16[192,512]{1,0:T(8,128)(2,1)}, u32[]{:S(2)}, u32[]{:S(2)}) collective-permute-start(bf16[192,512]{1,0:T(8,128)(2,1)} %bitcast.18), channel_id=1, source_target_pairs={{0,1},{1,0},{2,3},{3,2},{4,5},{5,4},{6,7},{7,6},{8,9},{9,8},{10,11... | collective-permute-start | bytes 589832 | tf_op jit(solution)/shard_map/ppermute | solution.py:40
  40.9 9.6 %collective-permute-start.11 = (bf16[192,512]{1,0:T(8,128)(2,1)}, bf16[192,512]{1,0:T(8,128)(2,1)}, u32[]{:S(2)}, u32[]{:S(2)}) collective-permute-start(bf16[192,512]{1,0:T(8,128)(2,1)} %bitcast.18), channel_id=1, source_target_pairs={{0,2},{1,3},{2,0},{3,1},{4,6},{5,7},{6,4},{7,5},{8,10},{9,11},{10,... | collective-permute-start | bytes 589832 | tf_op jit(solution)/shard_map/ppermute | solution.py:40
  42.0 9.6 %collective-permute-start.12 = (bf16[192,512]{1,0:T(8,128)(2,1)}, bf16[192,512]{1,0:T(8,128)(2,1)}, u32[]{:S(2)}, u32[]{:S(2)}) collective-permute-start(bf16[192,512]{1,0:T(8,128)(2,1)} %bitcast.18), channel_id=1, source_target_pairs={{0,3},{1,2},{2,1},{3,0},{4,7},{5,6},{6,5},{7,4},{8,11},{9,10},{10,... | collective-permute-start | bytes 589832 | tf_op jit(solution)/shard_map/ppermute | solution.py:40
  48.2 10.2 %copy-start.1 = (bf16[1,2048,896]{2,1,0:T(8,128)(2,1)S(1)}, bf16[1,2048,896]{2,1,0:T(8,128)(2,1)}, u32[]{:S(2)}) copy-start(bf16[1,2048,896]{2,1,0:T(8,128)(2,1)} %param.41) | copy-start | bytes 11010052
  59.7 3.2 %copy-start.2 = (bf16[1,896,2048]{2,1,0:T(8,128)(2,1)S(1)}, bf16[1,896,2048]{2,1,0:T(8,128)(2,1)}, u32[]{:S(2)}) copy-start(bf16[1,896,2048]{2,1,0:T(8,128)(2,1)} %param.43) | copy-start | bytes 11010052
  63.0 14.9 %copy-start.10 = (f32[64,2]{0,1:T(2,128)S(1)}, f32[64,2]{0,1:T(2,128)}, u32[]{:S(2)}) copy-start(f32[64,2]{0,1:T(2,128)} %param.40) | copy-start | bytes 1540
  63.0 18.0 %copy-start.6 = (pred[192,64,2]{0,1,2:T(32,128)(4,1)S(1)}, pred[192,64,2]{0,1,2:T(32,128)(4,1)}, u32[]{:S(2)}) copy-start(pred[192,64,2]{0,1,2:T(32,128)(4,1)} %get-tuple-element.39) | copy-start | bytes 73732
  64.2 5.7 %collective-permute-start.13 = (bf16[192,512]{1,0:T(8,128)(2,1)S(1)}, bf16[192,512]{1,0:T(8,128)(2,1)S(1)}, u32[]{:S(2)}, u32[]{:S(2)}) collective-permute-start(bf16[192,512]{1,0:T(8,128)(2,1)S(1)} %convolution_convert_fusion.3), channel_id=1, source_target_pairs={{0,1},{1,0},{2,3},{3,2},{4,5},{5,4},{6,7},{7,6},{8,9},{9,8},{10,11... | collective-permute-start | bytes 589832 | tf_op jit(solution)/shard_map/ppermute | solution.py:40
  65.2 6.5 %collective-permute-start.14 = (bf16[192,512]{1,0:T(8,128)(2,1)S(1)}, bf16[192,512]{1,0:T(8,128)(2,1)S(1)}, u32[]{:S(2)}, u32[]{:S(2)}) collective-permute-start(bf16[192,512]{1,0:T(8,128)(2,1)S(1)} %convolution_convert_fusion.2), channel_id=1, source_target_pairs={{0,2},{1,3},{2,0},{3,1},{4,6},{5,7},{6,4},{7,5},{8,10},{9,11},{10,... | collective-permute-start | bytes 589832 | tf_op jit(solution)/shard_map/ppermute | solution.py:40
  66.4 6.6 %collective-permute-start.15 = (bf16[192,512]{1,0:T(8,128)(2,1)S(1)}, bf16[192,512]{1,0:T(8,128)(2,1)S(1)}, u32[]{:S(2)}, u32[]{:S(2)}) collective-permute-start(bf16[192,512]{1,0:T(8,128)(2,1)S(1)} %convolution_convert_fusion.1), channel_id=1, source_target_pairs={{0,3},{1,2},{2,1},{3,0},{4,7},{5,6},{6,5},{7,4},{8,11},{9,10},{10,... | collective-permute-start | bytes 589832 | tf_op jit(solution)/shard_map/ppermute | solution.py:40
  73.4 4.6 %collective-permute-start.16 = (bf16[2,24,512]{2,1,0:T(8,128)(2,1)S(1)}, bf16[2,24,512]{2,1,0:T(8,128)(2,1)S(1)}, u32[]{:S(2)}, u32[]{:S(2)}) collective-permute-start(bf16[2,24,512]{2,1,0:T(8,128)(2,1)S(1)} %bitcast.143), channel_id=1, source_target_pairs={{0,8},{4,12},{8,0},{12,4},{16,24},{20,28},{24,16},{28,20},{1,9},{5... | collective-permute-start | bytes 147464 | tf_op jit(solution)/shard_map/ppermute | solution.py:45
  73.7 5.0 %collective-permute-start.17 = (bf16[2,24,512]{2,1,0:T(8,128)(2,1)S(1)}, bf16[2,24,512]{2,1,0:T(8,128)(2,1)S(1)}, u32[]{:S(2)}, u32[]{:S(2)}) collective-permute-start(bf16[2,24,512]{2,1,0:T(8,128)(2,1)S(1)} %bitcast.141), channel_id=1, source_target_pairs={{0,16},{4,20},{8,24},{12,28},{16,0},{20,4},{24,8},{28,12},{1,17},{... | collective-permute-start | bytes 147464 | tf_op jit(solution)/shard_map/ppermute | solution.py:45
  75.0 5.9 %collective-permute-start.18 = (bf16[2,24,512]{2,1,0:T(8,128)(2,1)S(1)}, bf16[2,24,512]{2,1,0:T(8,128)(2,1)S(1)}, u32[]{:S(2)}, u32[]{:S(2)}) collective-permute-start(bf16[2,24,512]{2,1,0:T(8,128)(2,1)S(1)} %bitcast.139), channel_id=1, source_target_pairs={{0,24},{4,28},{8,16},{12,20},{16,8},{20,12},{24,0},{28,4},{1,25},{... | collective-permute-start | bytes 147464 | tf_op jit(solution)/shard_map/ppermute | solution.py:45
  80.9 2.5 %collective-permute-start.19 = (bf16[4,24,512]{2,1,0:T(8,128)(2,1)S(1)}, bf16[4,24,512]{2,1,0:T(8,128)(2,1)S(1)}, u32[]{:S(2)}, u32[]{:S(2)}) collective-permute-start(bf16[4,24,512]{2,1,0:T(8,128)(2,1)S(1)} %get-tuple-element.20), channel_id=1, source_target_pairs={{0,4},{4,0},{8,12},{12,8},{16,20},{20,16},{24,28},{28,24},{1,5},{5... | collective-permute-start | bytes 294920 | tf_op jit(solution)/shard_map/ppermute | solution.py:45

commit v3 on v2

--- a/solution.py
+++ b/solution.py
@@ -1,38 +1,13 @@
+import functools
+
 import jax
 import jax.numpy as jnp
 from jax import lax
+from jax.experimental import pallas as pl
+from jax.experimental.pallas import tpu as pltpu
 from jax.sharding import PartitionSpec as P
 
 norm_eps = 1e-06
-
-
-def rms_scale(rows, gain):
-    values = rows.astype(jnp.float32)
-    scaled = values * lax.rsqrt(jnp.mean(values * values, axis=-1, keepdims=True) + norm_eps)
-    return (scaled * gain).astype(jnp.bfloat16)
-
-
-def state_step(
-    inputs, state_re, state_im, decay_re, freq, log_step, in_re, in_im, out_re, out_im, skip
-):
-    highest = lax.Precision.HIGHEST
-    step = jnp.exp(log_step)[:, None]
-    magnitude = jnp.exp(decay_re * step)
-    turn_re = magnitude * jnp.cos(freq * step)
-    turn_im = magnitude * jnp.sin(freq * step)
-    denom = decay_re * decay_re + freq * freq
-    coef_re = ((turn_re - 1.0) * decay_re + turn_im * freq) / denom
-    coef_im = (turn_im * decay_re - (turn_re - 1.0) * freq) / denom
-    drive_re = jnp.einsum("sgh,ghp->sgp", inputs, in_re, preferred_element_type=jnp.float32)
-    drive_im = jnp.einsum("sgh,ghp->sgp", inputs, in_im, preferred_element_type=jnp.float32)
-    push_re = coef_re * drive_re - coef_im * drive_im
-    push_im = coef_re * drive_im + coef_im * drive_re
-    new_re = turn_re * state_re - turn_im * state_im + push_re
-    new_im = turn_re * state_im + turn_im * state_re + push_im
-    read = jnp.einsum("ghp,sgp->sgh", out_re.astype(jnp.float32), new_re, precision=highest)
-    read = read - jnp.einsum("ghp,sgp->sgh", out_im.astype(jnp.float32), new_im, precision=highest)
-    read = read + skip * inputs.astype(jnp.float32)
-    return (read, new_re, new_im)
 
 
 def partner_swap(value, offset):
@@ -52,7 +27,7 @@
     joined = jnp.stack([near, crossed], axis=1)
     moved = [None] + [ep_swap(joined[step], 2 * step) for step in range(pairs - 1, 0, -1)][::-1]
     moved[0] = joined[0]
-    return jnp.stack(moved, axis=0)
+    return jnp.stack(moved, axis=0), joined
 
 
 def from_experts(rows):
@@ -61,6 +36,258 @@
     moved[0] = rows[0]
     moved = jnp.stack(moved, axis=1)
     return jnp.stack([moved[0], ep_swap(moved[1], 1)], axis=0)
+
+
+def lane_sums(values):
+    total = values[:, :128]
+    for start in range(128, values.shape[1], 128):
+        total = total + values[:, start : start + 128]
+    return total
+
+
+def mixer_front(
+    at_ref,
+    gain_ref,
+    log_step_ref,
+    decay_ref,
+    freq_ref,
+    in_re_ref,
+    in_im_ref,
+    out_re_ref,
+    out_im_ref,
+    skip_ref,
+    tokens_hbm,
+    w_in_hbm,
+    state_re_hbm,
+    state_im_hbm,
+    mixed_ref,
+    kept_ref,
+    new_re_ref,
+    new_im_ref,
+    tokens_ref,
+    w_in_ref,
+    state_re_ref,
+    state_im_ref,
+    in_ref,
+    out_ref,
+    split_ref,
+    sems,
+):
+    groups, heads, entries = in_re_ref.shape
+    seqs, width = tokens_ref.shape
+    per_half = min(groups, max(1, 128 // heads))
+    lanes = 2 * entries
+    copies = [
+        pltpu.make_async_copy(source, target, sems.at[place])
+        for place, (source, target) in enumerate(
+            (
+                (tokens_hbm, tokens_ref),
+                (w_in_hbm, w_in_ref),
+                (state_re_hbm, state_re_ref),
+                (state_im_hbm, state_im_ref),
+            )
+        )
+    ]
+    for copy in copies:
+        copy.start()
+
+    in_ref[...] = jnp.zeros_like(in_ref)
+    out_ref[...] = jnp.zeros_like(out_ref)
+    for g in range(groups):
+        rows = pl.ds((g % per_half) * heads, heads)
+        in_ref[rows, g * lanes : (g + 1) * lanes] = jnp.concatenate(
+            [in_re_ref[g], in_im_ref[g]], axis=1
+        )
+        out_ref[rows, g * lanes : (g + 1) * lanes] = jnp.concatenate(
+            [out_re_ref[g], -out_im_ref[g]], axis=1
+        )
+
+    diagonal = lax.broadcasted_iota(jnp.int32, (groups, groups), 0) == lax.broadcasted_iota(
+        jnp.int32, (groups, groups), 1
+    )
+    step = jnp.sum(
+        jnp.where(diagonal, jnp.exp(log_step_ref[...]), 0.0), axis=1, keepdims=True
+    )
+    decay, freq = decay_ref[...], freq_ref[...]
+    magnitude = jnp.exp(decay * step)
+    turn_re = magnitude * jnp.cos(freq * step)
+    turn_im = magnitude * jnp.sin(freq * step)
+    denom = decay * decay + freq * freq
+    coef_re = ((turn_re - 1.0) * decay + turn_im * freq) / denom
+    coef_im = (turn_im * decay - (turn_re - 1.0) * freq) / denom
+
+    block = per_half * heads
+    skip_tiled = jnp.concatenate([skip_ref[...]] * per_half, axis=1)
+    owner = lax.broadcasted_iota(jnp.int32, skip_tiled.shape, 1) // heads
+    group = lax.broadcasted_iota(jnp.int32, skip_tiled.shape, 0)
+    skip_rows = [
+        jnp.sum(jnp.where(owner + start == group, skip_tiled, 0.0), axis=0, keepdims=True)
+        for start in range(0, groups, per_half)
+    ]
+
+    copies[0].wait()
+    values = tokens_ref[...].astype(jnp.float32)
+    squares = jnp.sum(lane_sums(values * values), axis=1, keepdims=True)
+    scale = lax.rsqrt(squares / width + norm_eps)
+    normed = (values * scale * gain_ref[...]).astype(jnp.bfloat16)
+    kept = kept_ref.shape[1]
+    kept_ref[...] = tokens_ref[:, pl.ds(pl.multiple_of(at_ref[0] * kept, 128), kept)]
+    copies[1].wait()
+    drive = jnp.dot(normed, w_in_ref[...], preferred_element_type=jnp.float32).astype(jnp.bfloat16)
+    copies[2].wait()
+    copies[3].wait()
+    for half, skip_row in enumerate(skip_rows):
+        cols = slice(half * block, (half + 1) * block)
+        spans = slice(half * per_half * lanes, (half + 1) * per_half * lanes)
+        part = drive[:, cols]
+        driven = jnp.dot(part, in_ref[:, spans], preferred_element_type=jnp.float32)
+        for place in range(per_half):
+            g = half * per_half + place
+            row = slice(g, g + 1)
+            drive_re = driven[:, place * lanes : place * lanes + entries]
+            drive_im = driven[:, place * lanes + entries : (place + 1) * lanes]
+            old_re, old_im = state_re_ref[:, g, :], state_im_ref[:, g, :]
+            push_re = coef_re[row] * drive_re - coef_im[row] * drive_im
+            push_im = coef_re[row] * drive_im + coef_im[row] * drive_re
+            new_re = turn_re[row] * old_re - turn_im[row] * old_im + push_re
+            new_im = turn_re[row] * old_im + turn_im[row] * old_re + push_im
+            new_re_ref[:, g, :] = new_re
+            new_im_ref[:, g, :] = new_im
+            both = jnp.concatenate([new_re, new_im], axis=1)
+            high = both.astype(jnp.bfloat16)
+            low = (both - high.astype(jnp.float32)).astype(jnp.bfloat16)
+            split_ref[:seqs, g * lanes : (g + 1) * lanes] = high
+            split_ref[seqs:, g * lanes : (g + 1) * lanes] = low
+        terms = lax.dot_general(
+            split_ref[:, spans],
+            out_ref[:, spans],
+            (((1,), (1,)), ((), ())),
+            preferred_element_type=jnp.float32,
+        )
+        read = terms[:seqs] + terms[seqs:] + skip_row * part.astype(jnp.float32)
+        mixed_ref[:, cols] = jax.nn.gelu(read).astype(jnp.bfloat16)
+
+
+def front(
+    at, tokens, mix_gain, w_in, decay_re, freq, log_step, in_re, in_im, out_re, out_im, skip,
+    state_re, state_im, kept_width,
+):
+    groups, heads, entries = in_re.shape
+    seqs = tokens.shape[0]
+    per_half = min(groups, max(1, 128 // heads))
+    vmem = pl.BlockSpec(memory_space=pltpu.VMEM)
+    hbm = pl.BlockSpec(memory_space=pltpu.HBM)
+    wide = (per_half * heads, groups * 2 * entries)
+    return pl.pallas_call(
+        mixer_front,
+        out_shape=[
+            pltpu.VMEM((seqs, groups * heads), jnp.bfloat16),
+            pltpu.VMEM((seqs, kept_width), jnp.bfloat16),
+            jax.ShapeDtypeStruct(state_re.shape, jnp.float32),
+            jax.ShapeDtypeStruct(state_im.shape, jnp.float32),
+        ],
+        in_specs=[pl.BlockSpec(memory_space=pltpu.SMEM)] + [vmem] * 9 + [hbm] * 4,
+        out_specs=[vmem] * 4,
+        scratch_shapes=[
+            pltpu.VMEM(tokens.shape, tokens.dtype),
+            pltpu.VMEM(w_in.shape, w_in.dtype),
+            pltpu.VMEM(state_re.shape, state_re.dtype),
+            pltpu.VMEM(state_im.shape, state_im.dtype),
+            pltpu.VMEM(wide, jnp.bfloat16),
+            pltpu.VMEM(wide, jnp.bfloat16),
+            pltpu.VMEM((2 * seqs, wide[1]), jnp.bfloat16),
+            pltpu.SemaphoreType.DMA((4,)),
+        ],
+        compiler_params=pltpu.CompilerParams(vmem_limit_bytes=60 * 1024 * 1024),
+        cost_estimate=pl.CostEstimate(
+            flops=8_000_000_000, bytes_accessed=4_000_000, transcendentals=0
+        ),
+        name="mixer_front",
+    )(
+        at, mix_gain[None, :], log_step[None, :], decay_re, freq, in_re, in_im, out_re, out_im,
+        skip, tokens, w_in, state_re, state_im,
+    )
+
+
+def fetch_weights(pieces, *refs):
+    count = (len(refs) - 2) // 2
+    sources, targets, sems = refs[1 : 1 + count], refs[1 + count : 1 + 2 * count], refs[-1]
+    copies = []
+    for source, target in zip(sources, targets):
+        rows = source.shape[0] // pieces
+        for piece in range(pieces):
+            span = pl.ds(piece * rows, rows)
+            copies.append(
+                pltpu.make_async_copy(source.at[span], target.at[span], sems.at[len(copies)])
+            )
+    for copy in copies:
+        copy.start()
+    for copy in copies:
+        copy.wait()
+
+
+def fetched(after, *weights):
+    pieces = 4
+    return pl.pallas_call(
+        functools.partial(fetch_weights, pieces),
+        out_shape=[pltpu.VMEM(weight.shape, weight.dtype) for weight in weights],
+        in_specs=[pl.BlockSpec(memory_space=pl.ANY)]
+        + [pl.BlockSpec(memory_space=pltpu.HBM)] * len(weights),
+        out_specs=[pl.BlockSpec(memory_space=pltpu.VMEM)] * len(weights),
+        scratch_shapes=[pltpu.SemaphoreType.DMA((pieces * len(weights),))],
+        compiler_params=pltpu.CompilerParams(vmem_limit_bytes=1024 * 1024),
+        cost_estimate=pl.CostEstimate(
+            flops=1_000_000_000, bytes_accessed=4_000_000 * len(weights), transcendentals=0
+        ),
+        name="fetch_weights",
+    )(after, *(pltpu.with_memory_space_constraint(weight, pltpu.HBM) for weight in weights))
+
+
+def expert_step(first, last, model_width, at_ref, block_ref, gain_ref, gate_ref, up_ref, *rest):
+    held, results = (() if first else rest[:3]), (rest if first else rest[3:])
+    width = block_ref.shape[1]
+    start = pl.multiple_of(at_ref[0] * width, 128)
+    values = block_ref[...].astype(jnp.float32)
+    scaled = (values * gain_ref[:, pl.ds(start, width)]).astype(jnp.bfloat16)
+    sums = lane_sums(values * values)
+    gate = jnp.dot(scaled, gate_ref[pl.ds(start, width), :], preferred_element_type=jnp.float32)
+    up = jnp.dot(scaled, up_ref[pl.ds(start, width), :], preferred_element_type=jnp.float32)
+    if not first:
+        gate, up, sums = gate + held[0][...], up + held[1][...], sums + held[2][...]
+    if not last:
+        results[0][...], results[1][...], results[2][...] = gate, up, sums
+        return
+    squares = jnp.sum(sums, axis=1, keepdims=True)
+    scale = lax.rsqrt(squares / model_width + norm_eps)
+    gate = gate * scale
+    results[0][...] = (gate / (1.0 + jnp.exp(-gate)) * (up * scale)).astype(jnp.bfloat16)
+
+
+def expert_part(block, at, gain, gate_w, up_w, held, last):
+    rows, hidden_width = block.shape[0], gate_w.shape[1]
+    model_width = gate_w.shape[0]
+    if last:
+        shapes = [jax.ShapeDtypeStruct((rows, hidden_width), jnp.bfloat16)]
+    else:
+        shapes = [
+            jax.ShapeDtypeStruct((rows, hidden_width), jnp.float32),
+            jax.ShapeDtypeStruct((rows, hidden_width), jnp.float32),
+            jax.ShapeDtypeStruct((rows, 128), jnp.float32),
+        ]
+    vmem = pl.BlockSpec(memory_space=pltpu.VMEM)
+    return pl.pallas_call(
+        functools.partial(expert_step, not held, last, model_width),
+        out_shape=shapes,
+        in_specs=[pl.BlockSpec(memory_space=pltpu.SMEM)] + [vmem] * (4 + len(held)),
+        out_specs=[vmem] * len(shapes),
+        compiler_params=pltpu.CompilerParams(vmem_limit_bytes=24 * 1024 * 1024),
+        cost_estimate=pl.CostEstimate(
+            flops=4 * rows * block.shape[1] * hidden_width,
+            bytes_accessed=4 * block.shape[1] * hidden_width,
+            transcendentals=0,
+        ),
+        name="expert_last" if last else "expert_part",
+    )(at, block, gain, gate_w, up_w, *held)
 
 
 def local(
@@ -108,13 +335,11 @@
     def cols_of(array, offset, width):
         return lax.dynamic_slice_in_dim(array, (own ^ offset) * width, width, 1)
 
-    normed = rms_scale(tokens, mix_gain)
-    drive = jnp.dot(normed, w_in, preferred_element_type=jnp.float32).astype(jnp.bfloat16)
-    inputs = drive.reshape(seq_count, groups_local, -1)
-    read, new_re, new_im = state_step(
-        inputs, state_re, state_im, decay_re, freq, log_step, in_re, in_im, out_re, out_im, skip
-    )
-    mixed_in = jax.nn.gelu(read).reshape(seq_count, -1).astype(jnp.bfloat16)
+    own_at = own.astype(jnp.int32).reshape(1)
+    mixed_in, token_part, new_re, new_im = front(
+        own_at, tokens, mix_gain, w_in, decay_re, freq, log_step, in_re, in_im, out_re, out_im,
+        skip, state_re, state_im, local_width,
+    )
     chan_width = mixed_in.shape[1]
 
     arrived_mix = [partner_swap(mixed_in, offset) for offset in offsets]
@@ -126,6 +351,8 @@
             block, rows_of(glu_weight, offset, chan_width), preferred_element_type=jnp.float32
         )
     gated = (mixed_in.astype(jnp.float32) * jax.nn.sigmoid(gate + glu_bias)).astype(jnp.bfloat16)
+
+    (down_near,) = fetched(gated, down_local)
 
     def share(offset):
         block = jnp.dot(
@@ -137,7 +364,7 @@
     mix_part = share(0).astype(jnp.float32)
     for block in arrived_shares:
         mix_part = mix_part + block.astype(jnp.float32)
-    resid_part = (cols_of(tokens, 0, local_width).astype(jnp.float32) + mix_part).astype(
+    resid_part = (token_part.astype(jnp.float32) + mix_part).astype(
         jnp.bfloat16
     )
 
@@ -153,27 +380,21 @@
     combine = jnp.einsum("ask,sk->sa", picks.astype(jnp.float32), route_weight)
 
     outbound = jnp.dot(select, resid_part, preferred_element_type=jnp.float32).astype(jnp.bfloat16)
-    arrived = to_experts(outbound.reshape(2, pairs, slot_cap, local_width))
+    arrived, joined = to_experts(outbound.reshape(2, pairs, slot_cap, local_width))
     arrived = arrived.reshape(rows_all, local_width)
+    gate_near, up_near = fetched(joined, gate_local, up_local)
     blocks = [(0, arrived)] + [(offset, partner_swap(arrived, offset)) for offset in offsets]
-    gate_rows = up_rows = squares = 0.0
+    held = ()
     for offset, block in blocks:
-        values = block.astype(jnp.float32)
-        squares = squares + jnp.sum(values * values, axis=1, keepdims=True)
-        gain = lax.dynamic_slice_in_dim(ffn_gain, (own ^ offset) * local_width, local_width, 0)
-        scaled = (values * gain).astype(jnp.bfloat16)
-        gate_rows = gate_rows + jnp.dot(
-            scaled, rows_of(gate_local, offset, local_width), preferred_element_type=jnp.float32
-        )
-        up_rows = up_rows + jnp.dot(
-            scaled, rows_of(up_local, offset, local_width), preferred_element_type=jnp.float32
-        )
-    row_scale = lax.rsqrt(squares / model_width + norm_eps)
-    hidden = (jax.nn.silu(gate_rows * row_scale) * (up_rows * row_scale)).astype(jnp.bfloat16)
+        at = (own ^ offset).astype(jnp.int32).reshape(1)
+        held = expert_part(
+            block, at, ffn_gain[None, :], gate_near, up_near, held, offset == shards - 1
+        )
+    hidden = held[0]
 
     def result(offset):
         block = jnp.dot(
-            hidden, cols_of(down_local, offset, local_width), preferred_element_type=jnp.float32
+            hidden, cols_of(down_near, offset, local_width), preferred_element_type=jnp.float32
         )
         return block.astype(jnp.bfloat16)
 

time: 85 us -> 66.9 us (0.79)
  matrix products: 23.5 us -> 4.27 us
  Pallas kernels: 0 us -> 13.1 us
  other arithmetic: 8.86 us -> 0.66 us
  local copies, waits for them, and re-layouts: 4.58 us -> 0.64 us
    dot_general x17 -> x4, matrix products: 19.9 us -> 1.59 us  [result(): jnp.dot(hidden, cols_of(down_near, offset, local_width), preferred_elemen...]
    pallas_call x0 -> x7, Pallas kernels: none -> 13.1 us  [the longest x1 5.39 us: front(): pl.pallas_call(mixer_front, out_shape=[pltpu.VMEM((seqs, groups * heads),...]
    reduce_sum x5 -> x0, other arithmetic: 5.1 us -> none  [the longest x4 4 us: local(): squares = squares + jnp.sum(values * values, axis=1, keepdims=True)]
    unnamed x29 -> x15, local copies, waits for them, and re-layouts: 2.49 us -> 0.26 us
    ppermute x12, waiting for transfers between devices: 12.2 us -> 13.9 us  [partner_swap(): lax.ppermute(value, 'tp', [(source, source ^ offset) for source in range(...]
    convert_element_type x1 -> x0, other arithmetic: 0.99 us -> none  [local(): scaled = (values * gain).astype(jnp.bfloat16)]
    ppermute x8, waiting for transfers between devices: 9.7 us -> 8.78 us  [ep_swap(): lax.ppermute(value, 'ep', [(source, source ^ offset) for source in range(...]
  transfers between devices with their start and end apart: 20 -> 20, of which waited for: 13 -> 17; matrix products, arithmetic and copies ran while one was open for 14% -> 3% of each run, Pallas kernels for 0% -> 10%
where the time goes in v3:
time: 66.9 us; the launch traced here: 66.8 us
  starting transfers between devices  24.4 us (36%)
  waiting for transfers between devices  22.7 us (34%)
  Pallas kernels  13.1 us (20%)
  matrix products  4.27 us (6%)
  between operations  1.02 us (2%)
    ppermute x12, starting transfers between devices, partner_swap(): lax.ppermute(value, 'tp', [(source, source ^ offset) for source in range(...  15.4 us
    ppermute x12, waiting for transfers between devices, partner_swap(): lax.ppermute(value, 'tp', [(source, source ^ offset) for source in range(...  13.9 us
    ppermute x8, starting transfers between devices, ep_swap(): lax.ppermute(value, 'ep', [(source, source ^ offset) for source in range(...  9.05 us
    ppermute x8, waiting for transfers between devices, ep_swap(): lax.ppermute(value, 'ep', [(source, source ^ offset) for source in range(...  8.78 us
    pallas_call x1, Pallas kernels, front(): pl.pallas_call(mixer_front, out_shape=[pltpu.VMEM((seqs, groups * heads),...  5.39 us
    pallas_call x2, Pallas kernels, fetched(): pl.pallas_call(functools.partial(fetch_weights, pieces), out_shape=[pltpu...  5.21 us
    pallas_call x4, Pallas kernels, expert_part(): pl.pallas_call(functools.partial(expert_step, not held, last, model_width...  2.46 us
    dot_general x4, matrix products, result(): jnp.dot(hidden, cols_of(down_near, offset, local_width), preferred_elemen...  1.59 us
  transfers between devices with their start and end apart: 20, of which 17 were waited for; matrix products, arithmetic and copies ran while one was open for 3% of the time, Pallas kernels for 10%

profile of v3, /device:TPU:0, one launch (start us, length us, event | category | flops | bytes accessed | tf_op | source)
XLA Modules:
  0.0 66.8 jit_solution(11258863084431850861)
XLA Ops:
  0.7 5.4 %mixer_front.1 = (bf16[64,256]{1,0:T(8,128)(2,1)S(1)}, bf16[64,512]{1,0:T(8,128)(2,1)S(1)}, f32[64,16,64]{2,1,0:T(8,128)}, f32[64,16,64]{2,1,0:T(8,128)}) custom-call(s32[1]{0:T(128)} %bitcast.at_ref, f32[1,2048]{1,0:T(1,128)} %bitcast.87, f32[1,16]{1,0:T(1,128)} %bitcast.88, f32[16,64]{1,0:T(8,128)} %decay_ref.1, f32[16,64]{1,0:T(8,128)} %freq_ref.1, ...), custom_call_target="tpu_custom_call" | custom-call | flops 8000000000 | bytes 4000000 | tf_op jit(solution)/shard_map/mixer_front/pallas_call | solution.py:181
  6.1 3.0 %collective-permute-start = (bf16[64,256]{1,0:T(8,128)(2,1)S(1)}, bf16[64,256]{1,0:T(8,128)(2,1)S(1)}, u32[]{:S(2)}, u32[]{:S(2)}) collective-permute-start(bf16[64,256]{1,0:T(8,128)(2,1)S(1)} %get-tuple-element.19), channel_id=1, source_target_pairs={{0,1},{1,0},{2,3},{3,2},{4,5},{5,4},{6,7},{7,6},{8,9},{9,8},{10,11... | collective-permute-start | bytes 98312 | tf_op jit(solution)/shard_map/ppermute | solution.py:15
  9.1 1.5 %collective-permute-start.2 = (bf16[64,256]{1,0:T(8,128)(2,1)S(1)}, bf16[64,256]{1,0:T(8,128)(2,1)S(1)}, u32[]{:S(2)}, u32[]{:S(2)}) collective-permute-start(bf16[64,256]{1,0:T(8,128)(2,1)S(1)} %get-tuple-element.19), channel_id=1, source_target_pairs={{0,3},{1,2},{2,1},{3,0},{4,7},{5,6},{6,5},{7,4},{8,11},{9,10},{10,... | collective-permute-start | bytes 98312 | tf_op jit(solution)/shard_map/ppermute | solution.py:15
  12.0 2.0 %collective-permute-done.2 = bf16[64,256]{1,0:T(8,128)(2,1)S(1)} collective-permute-done((bf16[64,256]{1,0:T(8,128)(2,1)S(1)}, bf16[64,256]{1,0:T(8,128)(2,1)S(1)}, u32[]{:S(2)}, u32[]{:S(2)}) %collective-permute-start.2) | collective-permute-done | bytes 32800 | tf_op jit(solution)/shard_map/ppermute | solution.py:15
  14.1 0.5 collective-permute-done.1
  14.9 1.6 %collective-permute-start.3 = (bf16[64,512]{1,0:T(8,128)(2,1)S(1)}, bf16[64,512]{1,0:T(8,128)(2,1)S(1)}, u32[]{:S(2)}, u32[]{:S(2)}) collective-permute-start(bf16[64,512]{1,0:T(8,128)(2,1)S(1)} %convolution_convert_fusion.7), channel_id=1, source_target_pairs={{0,1},{1,0},{2,3},{3,2},{4,5},{5,4},{6,7},{7,6},{8,9},{9,8},{10,11... | collective-permute-start | bytes 196616 | tf_op jit(solution)/shard_map/ppermute | solution.py:15
  16.6 0.6 collective-permute-start.4
  17.4 1.6 %collective-permute-start.5 = (bf16[64,512]{1,0:T(8,128)(2,1)S(1)}, bf16[64,512]{1,0:T(8,128)(2,1)S(1)}, u32[]{:S(2)}, u32[]{:S(2)}) collective-permute-start(bf16[64,512]{1,0:T(8,128)(2,1)S(1)} %convolution_convert_fusion.5), channel_id=1, source_target_pairs={{0,3},{1,2},{2,1},{3,0},{4,7},{5,6},{6,5},{7,4},{8,11},{9,10},{10,... | collective-permute-start | bytes 196616 | tf_op jit(solution)/shard_map/ppermute | solution.py:15
  19.0 0.5 collective-permute-done.3
  19.6 1.4 %collective-permute-done.4 = bf16[64,512]{1,0:T(8,128)(2,1)S(1)} collective-permute-done((bf16[64,512]{1,0:T(8,128)(2,1)S(1)}, bf16[64,512]{1,0:T(8,128)(2,1)S(1)}, u32[]{:S(2)}, u32[]{:S(2)}) %collective-permute-start.4) | collective-permute-done | bytes 65568 | tf_op jit(solution)/shard_map/ppermute | solution.py:15
  21.0 1.6 %collective-permute-done.5 = bf16[64,512]{1,0:T(8,128)(2,1)S(1)} collective-permute-done((bf16[64,512]{1,0:T(8,128)(2,1)S(1)}, bf16[64,512]{1,0:T(8,128)(2,1)S(1)}, u32[]{:S(2)}, u32[]{:S(2)}) %collective-permute-start.5) | collective-permute-done | bytes 65568 | tf_op jit(solution)/shard_map/ppermute | solution.py:15
  22.6 0.2 add_convert_fusion.1
  22.8 0.2 convolution_convert_fusion
  23.2 1.3 %collective-permute-done.6 = bf16[4,24,512]{2,1,0:T(8,128)(2,1)S(1)} collective-permute-done((bf16[4,24,512]{2,1,0:T(8,128)(2,1)S(1)}, bf16[4,24,512]{2,1,0:T(8,128)(2,1)S(1)}, u32[]{:S(2)}, u32[]{:S(2)}) %collective-permute-start.6) | collective-permute-done | bytes 98336 | tf_op jit(solution)/shard_map/ppermute | solution.py:20
  24.5 1.6 %collective-permute-start.7 = (bf16[2,24,512]{2,1,0:T(8,128)(2,1)S(1)}, bf16[2,24,512]{2,1,0:T(8,128)(2,1)S(1)}, u32[]{:S(2)}, u32[]{:S(2)}) collective-permute-start(bf16[2,24,512]{2,1,0:T(8,128)(2,1)S(1)} %get-tuple-element.40), channel_id=1, source_target_pairs={{0,8},{4,12},{8,0},{12,4},{16,24},{20,28},{24,16},{28,20},{1,9},{5... | collective-permute-start | bytes 147464 | tf_op jit(solution)/shard_map/ppermute | solution.py:20
  26.1 2.6 %collective-permute-start.8 = (bf16[2,24,512]{2,1,0:T(8,128)(2,1)S(1)}, bf16[2,24,512]{2,1,0:T(8,128)(2,1)S(1)}, u32[]{:S(2)}, u32[]{:S(2)}) collective-permute-start(bf16[2,24,512]{2,1,0:T(8,128)(2,1)S(1)} %get-tuple-element.41), channel_id=1, source_target_pairs={{0,16},{4,20},{8,24},{12,28},{16,0},{20,4},{24,8},{28,12},{1,17},{... | collective-permute-start | bytes 147464 | tf_op jit(solution)/shard_map/ppermute | solution.py:20
  28.7 0.2 collective-permute-start.9
  28.9 2.0 %fetch_weights.3 = bf16[896,2048]{1,0:T(8,128)(2,1)S(1)} custom-call(bf16[64,256]{1,0:T(8,128)(2,1)S(1)} %fusion.13.refs_0_, bf16[896,2048]{1,0:T(8,128)(2,1)} %bitcast.68), custom_call_target="tpu_custom_call" | custom-call | flops 1000000000 | bytes 4000000 | tf_op jit(solution)/shard_map/fetch_weights/pallas_call | solution.py:231
  31.0 1.0 %collective-permute-done.8 = bf16[2,24,512]{2,1,0:T(8,128)(2,1)S(1)} collective-permute-done((bf16[2,24,512]{2,1,0:T(8,128)(2,1)S(1)}, bf16[2,24,512]{2,1,0:T(8,128)(2,1)S(1)}, u32[]{:S(2)}, u32[]{:S(2)}) %collective-permute-start.8) | collective-permute-done | bytes 49184 | tf_op jit(solution)/shard_map/ppermute | solution.py:20
  32.0 2.6 %collective-permute-done.9 = bf16[2,24,512]{2,1,0:T(8,128)(2,1)S(1)} collective-permute-done((bf16[2,24,512]{2,1,0:T(8,128)(2,1)S(1)}, bf16[2,24,512]{2,1,0:T(8,128)(2,1)S(1)}, u32[]{:S(2)}, u32[]{:S(2)}) %collective-permute-start.9) | collective-permute-done | bytes 49184 | tf_op jit(solution)/shard_map/ppermute | solution.py:20
  34.6 1.2 %collective-permute-start.12 = (bf16[192,512]{1,0:T(8,128)(2,1)S(1)}, bf16[192,512]{1,0:T(8,128)(2,1)S(1)}, u32[]{:S(2)}, u32[]{:S(2)}) collective-permute-start(bf16[192,512]{1,0:T(8,128)(2,1)S(1)} %bitcast.58), channel_id=1, source_target_pairs={{0,1},{1,0},{2,3},{3,2},{4,5},{5,4},{6,7},{7,6},{8,9},{9,8},{10,11... | collective-permute-start | bytes 589832 | tf_op jit(solution)/shard_map/ppermute | solution.py:15
  35.8 0.9 %collective-permute-start.11 = (bf16[192,512]{1,0:T(8,128)(2,1)S(1)}, bf16[192,512]{1,0:T(8,128)(2,1)S(1)}, u32[]{:S(2)}, u32[]{:S(2)}) collective-permute-start(bf16[192,512]{1,0:T(8,128)(2,1)S(1)} %bitcast.59), channel_id=1, source_target_pairs={{0,2},{1,3},{2,0},{3,1},{4,6},{5,7},{6,4},{7,5},{8,10},{9,11},{10,... | collective-permute-start | bytes 589832 | tf_op jit(solution)/shard_map/ppermute | solution.py:15
  36.7 1.4 %collective-permute-start.10 = (bf16[192,512]{1,0:T(8,128)(2,1)S(1)}, bf16[192,512]{1,0:T(8,128)(2,1)S(1)}, u32[]{:S(2)}, u32[]{:S(2)}) collective-permute-start(bf16[192,512]{1,0:T(8,128)(2,1)S(1)} %bitcast.60), channel_id=1, source_target_pairs={{0,3},{1,2},{2,1},{3,0},{4,7},{5,6},{6,5},{7,4},{8,11},{9,10},{10,... | collective-permute-start | bytes 589832 | tf_op jit(solution)/shard_map/ppermute | solution.py:15
  38.2 3.2 %fetch_weights.2 = (bf16[2048,896]{1,0:T(8,128)(2,1)S(1)}, bf16[2048,896]{1,0:T(8,128)(2,1)S(1)}) custom-call(bf16[4,2,24,512]{3,2,1,0:T(8,128)(2,1)S(1)} %pad_maximum_fusion.refs_0_, bf16[2048,896]{1,0:T(8,128)(2,1)} %bitcast.66, bf16[2048,896]{1,0:T(8,128)(2,1)} %bitcast.67), custom_call_target="tpu_custom_call" | custom-call | flops 1000000000 | bytes 8000000 | tf_op jit(solution)/shard_map/fetch_weights/pallas_call | solution.py:231
  41.4 0.6 expert_part.3
  42.1 0.6 expert_part.4
  42.7 0.8 %collective-permute-done.11.block_ref = bf16[192,512]{1,0:T(8,128)(2,1)S(1)} collective-permute-done((bf16[192,512]{1,0:T(8,128)(2,1)S(1)}, bf16[192,512]{1,0:T(8,128)(2,1)S(1)}, u32[]{:S(2)}, u32[]{:S(2)}) %collective-permute-start.11) | collective-permute-done | bytes 196640 | tf_op jit(solution)/shard_map/ppermute | solution.py:15
  43.5 0.6 expert_part.5
  44.1 1.1 %collective-permute-done.10.block_ref = bf16[192,512]{1,0:T(8,128)(2,1)S(1)} collective-permute-done((bf16[192,512]{1,0:T(8,128)(2,1)S(1)}, bf16[192,512]{1,0:T(8,128)(2,1)S(1)}, u32[]{:S(2)}, u32[]{:S(2)}) %collective-permute-start.10) | collective-permute-done | bytes 196640 | tf_op jit(solution)/shard_map/ppermute | solution.py:15
  45.2 0.7 %expert_last.1 = bf16[192,896]{1,0:T(8,128)(2,1)S(1)} custom-call(s32[1]{0:T(128)} %bitcast.5.at_ref, bf16[192,512]{1,0:T(8,128)(2,1)S(1)} %collective-permute-done.10.block_ref, f32[1,2048]{1,0:T(1,128)S(1)} %bitcast.65, bf16[2048,896]{1,0:T(8,128)(2,1)S(1)} %get-tuple-element.20.gate_ref, bf16[2048,896]{1,0:T(8,128)(2,1)S(1)} %get-tuple-element.21.up_ref, ...), custom_call_target="tpu_custom_call" | custom-call | flops 352321536 | bytes 1835008 | tf_op jit(solution)/shard_map/expert_last/pallas_call | solution.py:278
  45.9 0.4 convolution_convert_fusion.3
  46.3 0.4 convolution_convert_fusion.2
  46.7 0.4 convolution_convert_fusion.1
  47.1 1.7 %collective-permute-start.13 = (bf16[192,512]{1,0:T(8,128)(2,1)S(1)}, bf16[192,512]{1,0:T(8,128)(2,1)S(1)}, u32[]{:S(2)}, u32[]{:S(2)}) collective-permute-start(bf16[192,512]{1,0:T(8,128)(2,1)S(1)} %convolution_convert_fusion.3), channel_id=1, source_target_pairs={{0,1},{1,0},{2,3},{3,2},{4,5},{5,4},{6,7},{7,6},{8,9},{9,8},{10,11... | collective-permute-start | bytes 589832 | tf_op jit(solution)/shard_map/ppermute | solution.py:15
  48.8 1.2 %collective-permute-start.14 = (bf16[192,512]{1,0:T(8,128)(2,1)S(1)}, bf16[192,512]{1,0:T(8,128)(2,1)S(1)}, u32[]{:S(2)}, u32[]{:S(2)}) collective-permute-start(bf16[192,512]{1,0:T(8,128)(2,1)S(1)} %convolution_convert_fusion.2), channel_id=1, source_target_pairs={{0,2},{1,3},{2,0},{3,1},{4,6},{5,7},{6,4},{7,5},{8,10},{9,11},{10,... | collective-permute-start | bytes 589832 | tf_op jit(solution)/shard_map/ppermute | solution.py:15
  50.0 0.6 collective-permute-start.15
  50.6 2.6 %collective-permute-done.13 = bf16[192,512]{1,0:T(8,128)(2,1)S(1)} collective-permute-done((bf16[192,512]{1,0:T(8,128)(2,1)S(1)}, bf16[192,512]{1,0:T(8,128)(2,1)S(1)}, u32[]{:S(2)}, u32[]{:S(2)}) %collective-permute-start.13) | collective-permute-done | bytes 196640 | tf_op jit(solution)/shard_map/ppermute | solution.py:15
  53.3 2.1 %collective-permute-done.14 = bf16[192,512]{1,0:T(8,128)(2,1)S(1)} collective-permute-done((bf16[192,512]{1,0:T(8,128)(2,1)S(1)}, bf16[192,512]{1,0:T(8,128)(2,1)S(1)}, u32[]{:S(2)}, u32[]{:S(2)}) %collective-permute-start.14) | collective-permute-done | bytes 196640 | tf_op jit(solution)/shard_map/ppermute | solution.py:15
  55.3 1.2 %collective-permute-done.15 = bf16[192,512]{1,0:T(8,128)(2,1)S(1)} collective-permute-done((bf16[192,512]{1,0:T(8,128)(2,1)S(1)}, bf16[192,512]{1,0:T(8,128)(2,1)S(1)}, u32[]{:S(2)}, u32[]{:S(2)}) %collective-permute-start.15) | collective-permute-done | bytes 196640 | tf_op jit(solution)/shard_map/ppermute | solution.py:15
  56.6 0.4 fusion.4
  57.0 0.4 collective-permute-start.16
  57.4 1.2 %collective-permute-start.17 = (bf16[2,24,512]{2,1,0:T(8,128)(2,1)S(1)}, bf16[2,24,512]{2,1,0:T(8,128)(2,1)S(1)}, u32[]{:S(2)}, u32[]{:S(2)}) collective-permute-start(bf16[2,24,512]{2,1,0:T(8,128)(2,1)S(1)} %bitcast.81), channel_id=1, source_target_pairs={{0,16},{4,20},{8,24},{12,28},{16,0},{20,4},{24,8},{28,12},{1,17},{... | collective-permute-start | bytes 147464 | tf_op jit(solution)/shard_map/ppermute | solution.py:20
  58.6 2.9 %collective-permute-start.18 = (bf16[2,24,512]{2,1,0:T(8,128)(2,1)S(1)}, bf16[2,24,512]{2,1,0:T(8,128)(2,1)S(1)}, u32[]{:S(2)}, u32[]{:S(2)}) collective-permute-start(bf16[2,24,512]{2,1,0:T(8,128)(2,1)S(1)} %bitcast.78), channel_id=1, source_target_pairs={{0,24},{4,28},{8,16},{12,20},{16,8},{20,12},{24,0},{28,4},{1,25},{... | collective-permute-start | bytes 147464 | tf_op jit(solution)/shard_map/ppermute | solution.py:20
  61.6 0.8 %collective-permute-done.17 = bf16[2,24,512]{2,1,0:T(8,128)(2,1)S(1)} collective-permute-done((bf16[2,24,512]{2,1,0:T(8,128)(2,1)S(1)}, bf16[2,24,512]{2,1,0:T(8,128)(2,1)S(1)}, u32[]{:S(2)}, u32[]{:S(2)}) %collective-permute-start.17) | collective-permute-done | bytes 49184 | tf_op jit(solution)/shard_map/ppermute | solution.py:20
  62.4 2.1 %collective-permute-done.18 = bf16[2,24,512]{2,1,0:T(8,128)(2,1)S(1)} collective-permute-done((bf16[2,24,512]{2,1,0:T(8,128)(2,1)S(1)}, bf16[2,24,512]{2,1,0:T(8,128)(2,1)S(1)}, u32[]{:S(2)}, u32[]{:S(2)}) %collective-permute-start.18) | collective-permute-done | bytes 49184 | tf_op jit(solution)/shard_map/ppermute | solution.py:20
  64.6 0.2 fusion.22
  64.8 1.1 %collective-permute-done.19 = bf16[4,24,512]{2,1,0:T(8,128)(2,1)S(1)} collective-permute-done((bf16[4,24,512]{2,1,0:T(8,128)(2,1)S(1)}, bf16[4,24,512]{2,1,0:T(8,128)(2,1)S(1)}, u32[]{:S(2)}, u32[]{:S(2)}) %collective-permute-start.19) | collective-permute-done | bytes 98336 | tf_op jit(solution)/shard_map/ppermute | solution.py:20
  65.9 0.9 %add_convert_fusion = bf16[64,512]{1,0:T(8,128)(2,1)} fusion(bf16[64,512]{1,0:T(8,128)(2,1)S(1)} %add_convert_fusion.1, bf16[192,512]{1,0:T(8,128)(2,1)S(1)} %bitcast.71, f32[64,1,192]{2,1,0:T(1,128)S(1)} %fusion.22), kind=kOutput, calls=%fused_computation.47 | convolution fusion | flops 75595776 | bytes 376832 | tf_op jit(solution)/shard_map/dot_general | solution.py:408
  (44 shorter events, 2.7 us)
Async XLA Ops:
  0.6 14.1 %copy-start = (bf16[256,2048]{1,0:T(8,128)(2,1)S(1)}, bf16[256,2048]{1,0:T(8,128)(2,1)}, u32[]{:S(2)}) copy-start(bf16[256,2048]{1,0:T(8,128)(2,1)} %param.37) | copy-start | bytes 3145732
  0.7 10.0 %copy-start.3 = (s32[64,2]{0,1:T(2,128)S(1)}, s32[64,2]{0,1:T(2,128)}, u32[]{:S(2)}) copy-start(s32[64,2]{0,1:T(2,128)} %param.39) | copy-start | bytes 1540
  0.7 10.9 %copy-start.2 = (bf16[1024,256]{1,0:T(8,128)(2,1)S(1)}, bf16[1024,256]{1,0:T(8,128)(2,1)}, u32[]{:S(2)}) copy-start(bf16[1024,256]{1,0:T(8,128)(2,1)} %param.35) | copy-start | bytes 1572868
  0.7 13.8 %copy-start.5 = (f32[256]{0:T(256)S(1)}, f32[256]{0:T(256)}, u32[]{:S(2)}) copy-start(f32[256]{0:T(256)} %param.36) | copy-start | bytes 3076
  6.1 5.7 %collective-permute-start = (bf16[64,256]{1,0:T(8,128)(2,1)S(1)}, bf16[64,256]{1,0:T(8,128)(2,1)S(1)}, u32[]{:S(2)}, u32[]{:S(2)}) collective-permute-start(bf16[64,256]{1,0:T(8,128)(2,1)S(1)} %get-tuple-element.19), channel_id=1, source_target_pairs={{0,1},{1,0},{2,3},{3,2},{4,5},{5,4},{6,7},{7,6},{8,9},{9,8},{10,11... | collective-permute-start | bytes 98312 | tf_op jit(solution)/shard_map/ppermute | solution.py:15
  9.1 4.8 %collective-permute-start.2 = (bf16[64,256]{1,0:T(8,128)(2,1)S(1)}, bf16[64,256]{1,0:T(8,128)(2,1)S(1)}, u32[]{:S(2)}, u32[]{:S(2)}) collective-permute-start(bf16[64,256]{1,0:T(8,128)(2,1)S(1)} %get-tuple-element.19), channel_id=1, source_target_pairs={{0,3},{1,2},{2,1},{3,0},{4,7},{5,6},{6,5},{7,4},{8,11},{9,10},{10,... | collective-permute-start | bytes 98312 | tf_op jit(solution)/shard_map/ppermute | solution.py:15
  10.6 3.9 %collective-permute-start.1 = (bf16[64,256]{1,0:T(8,128)(2,1)S(1)}, bf16[64,256]{1,0:T(8,128)(2,1)S(1)}, u32[]{:S(2)}, u32[]{:S(2)}) collective-permute-start(bf16[64,256]{1,0:T(8,128)(2,1)S(1)} %get-tuple-element.19), channel_id=1, source_target_pairs={{0,2},{1,3},{2,0},{3,1},{4,6},{5,7},{6,4},{7,5},{8,10},{9,11},{10,... | collective-permute-start | bytes 98312 | tf_op jit(solution)/shard_map/ppermute | solution.py:15
  14.9 4.7 %collective-permute-start.3 = (bf16[64,512]{1,0:T(8,128)(2,1)S(1)}, bf16[64,512]{1,0:T(8,128)(2,1)S(1)}, u32[]{:S(2)}, u32[]{:S(2)}) collective-permute-start(bf16[64,512]{1,0:T(8,128)(2,1)S(1)} %convolution_convert_fusion.7), channel_id=1, source_target_pairs={{0,1},{1,0},{2,3},{3,2},{4,5},{5,4},{6,7},{7,6},{8,9},{9,8},{10,11... | collective-permute-start | bytes 196616 | tf_op jit(solution)/shard_map/ppermute | solution.py:15
  16.6 4.3 %collective-permute-start.4 = (bf16[64,512]{1,0:T(8,128)(2,1)S(1)}, bf16[64,512]{1,0:T(8,128)(2,1)S(1)}, u32[]{:S(2)}, u32[]{:S(2)}) collective-permute-start(bf16[64,512]{1,0:T(8,128)(2,1)S(1)} %convolution_convert_fusion.6), channel_id=1, source_target_pairs={{0,2},{1,3},{2,0},{3,1},{4,6},{5,7},{6,4},{7,5},{8,10},{9,11},{10,... | collective-permute-start | bytes 196616 | tf_op jit(solution)/shard_map/ppermute | solution.py:15
  17.4 5.2 %collective-permute-start.5 = (bf16[64,512]{1,0:T(8,128)(2,1)S(1)}, bf16[64,512]{1,0:T(8,128)(2,1)S(1)}, u32[]{:S(2)}, u32[]{:S(2)}) collective-permute-start(bf16[64,512]{1,0:T(8,128)(2,1)S(1)} %convolution_convert_fusion.5), channel_id=1, source_target_pairs={{0,3},{1,2},{2,1},{3,0},{4,7},{5,6},{6,5},{7,4},{8,11},{9,10},{10,... | collective-permute-start | bytes 196616 | tf_op jit(solution)/shard_map/ppermute | solution.py:15
  23.1 1.4 %collective-permute-start.6 = (bf16[4,24,512]{2,1,0:T(8,128)(2,1)S(1)}, bf16[4,24,512]{2,1,0:T(8,128)(2,1)S(1)}, u32[]{:S(2)}, u32[]{:S(2)}) collective-permute-start(bf16[4,24,512]{2,1,0:T(8,128)(2,1)S(1)} %bitcast.76), channel_id=1, source_target_pairs={{0,4},{4,0},{8,12},{12,8},{16,20},{20,16},{24,28},{28,24},{1,5},{5... | collective-permute-start | bytes 294920 | tf_op jit(solution)/shard_map/ppermute | solution.py:20
  24.5 6.5 %collective-permute-start.7 = (bf16[2,24,512]{2,1,0:T(8,128)(2,1)S(1)}, bf16[2,24,512]{2,1,0:T(8,128)(2,1)S(1)}, u32[]{:S(2)}, u32[]{:S(2)}) collective-permute-start(bf16[2,24,512]{2,1,0:T(8,128)(2,1)S(1)} %get-tuple-element.40), channel_id=1, source_target_pairs={{0,8},{4,12},{8,0},{12,4},{16,24},{20,28},{24,16},{28,20},{1,9},{5... | collective-permute-start | bytes 147464 | tf_op jit(solution)/shard_map/ppermute | solution.py:20
  26.1 5.9 %collective-permute-start.8 = (bf16[2,24,512]{2,1,0:T(8,128)(2,1)S(1)}, bf16[2,24,512]{2,1,0:T(8,128)(2,1)S(1)}, u32[]{:S(2)}, u32[]{:S(2)}) collective-permute-start(bf16[2,24,512]{2,1,0:T(8,128)(2,1)S(1)} %get-tuple-element.41), channel_id=1, source_target_pairs={{0,16},{4,20},{8,24},{12,28},{16,0},{20,4},{24,8},{28,12},{1,17},{... | collective-permute-start | bytes 147464 | tf_op jit(solution)/shard_map/ppermute | solution.py:20
  28.7 5.9 %collective-permute-start.9 = (bf16[2,24,512]{2,1,0:T(8,128)(2,1)S(1)}, bf16[2,24,512]{2,1,0:T(8,128)(2,1)S(1)}, u32[]{:S(2)}, u32[]{:S(2)}) collective-permute-start(bf16[2,24,512]{2,1,0:T(8,128)(2,1)S(1)} %get-tuple-element.42), channel_id=1, source_target_pairs={{0,24},{4,28},{8,16},{12,20},{16,8},{20,12},{24,0},{28,4},{1,25},{... | collective-permute-start | bytes 147464 | tf_op jit(solution)/shard_map/ppermute | solution.py:20
  34.6 7.4 %collective-permute-start.12 = (bf16[192,512]{1,0:T(8,128)(2,1)S(1)}, bf16[192,512]{1,0:T(8,128)(2,1)S(1)}, u32[]{:S(2)}, u32[]{:S(2)}) collective-permute-start(bf16[192,512]{1,0:T(8,128)(2,1)S(1)} %bitcast.58), channel_id=1, source_target_pairs={{0,1},{1,0},{2,3},{3,2},{4,5},{5,4},{6,7},{7,6},{8,9},{9,8},{10,11... | collective-permute-start | bytes 589832 | tf_op jit(solution)/shard_map/ppermute | solution.py:15
  35.8 7.7 %collective-permute-start.11 = (bf16[192,512]{1,0:T(8,128)(2,1)S(1)}, bf16[192,512]{1,0:T(8,128)(2,1)S(1)}, u32[]{:S(2)}, u32[]{:S(2)}) collective-permute-start(bf16[192,512]{1,0:T(8,128)(2,1)S(1)} %bitcast.59), channel_id=1, source_target_pairs={{0,2},{1,3},{2,0},{3,1},{4,6},{5,7},{6,4},{7,5},{8,10},{9,11},{10,... | collective-permute-start | bytes 589832 | tf_op jit(solution)/shard_map/ppermute | solution.py:15
  36.7 8.5 %collective-permute-start.10 = (bf16[192,512]{1,0:T(8,128)(2,1)S(1)}, bf16[192,512]{1,0:T(8,128)(2,1)S(1)}, u32[]{:S(2)}, u32[]{:S(2)}) collective-permute-start(bf16[192,512]{1,0:T(8,128)(2,1)S(1)} %bitcast.60), channel_id=1, source_target_pairs={{0,3},{1,2},{2,1},{3,0},{4,7},{5,6},{6,5},{7,4},{8,11},{9,10},{10,... | collective-permute-start | bytes 589832 | tf_op jit(solution)/shard_map/ppermute | solution.py:15
  38.2 3.2 %copy-start.1 = (f32[2048]{0:T(1024)S(1)}, f32[2048]{0:T(1024)}, u32[]{:S(2)}) copy-start(f32[2048]{0:T(1024)} %param.38) | copy-start | bytes 24580
  45.9 15.6 %copy-start.4 = (f32[64,2]{0,1:T(2,128)S(1)}, f32[64,2]{0,1:T(2,128)}, u32[]{:S(2)}) copy-start(f32[64,2]{0,1:T(2,128)} %param.40) | copy-start | bytes 1540
  47.1 6.2 %collective-permute-start.13 = (bf16[192,512]{1,0:T(8,128)(2,1)S(1)}, bf16[192,512]{1,0:T(8,128)(2,1)S(1)}, u32[]{:S(2)}, u32[]{:S(2)}) collective-permute-start(bf16[192,512]{1,0:T(8,128)(2,1)S(1)} %convolution_convert_fusion.3), channel_id=1, source_target_pairs={{0,1},{1,0},{2,3},{3,2},{4,5},{5,4},{6,7},{7,6},{8,9},{9,8},{10,11... | collective-permute-start | bytes 589832 | tf_op jit(solution)/shard_map/ppermute | solution.py:15
  48.8 6.6 %collective-permute-start.14 = (bf16[192,512]{1,0:T(8,128)(2,1)S(1)}, bf16[192,512]{1,0:T(8,128)(2,1)S(1)}, u32[]{:S(2)}, u32[]{:S(2)}) collective-permute-start(bf16[192,512]{1,0:T(8,128)(2,1)S(1)} %convolution_convert_fusion.2), channel_id=1, source_target_pairs={{0,2},{1,3},{2,0},{3,1},{4,6},{5,7},{6,4},{7,5},{8,10},{9,11},{10,... | collective-permute-start | bytes 589832 | tf_op jit(solution)/shard_map/ppermute | solution.py:15
  50.0 6.6 %collective-permute-start.15 = (bf16[192,512]{1,0:T(8,128)(2,1)S(1)}, bf16[192,512]{1,0:T(8,128)(2,1)S(1)}, u32[]{:S(2)}, u32[]{:S(2)}) collective-permute-start(bf16[192,512]{1,0:T(8,128)(2,1)S(1)} %convolution_convert_fusion.1), channel_id=1, source_target_pairs={{0,3},{1,2},{2,1},{3,0},{4,7},{5,6},{6,5},{7,4},{8,11},{9,10},{10,... | collective-permute-start | bytes 589832 | tf_op jit(solution)/shard_map/ppermute | solution.py:15
  57.0 4.6 %collective-permute-start.16 = (bf16[2,24,512]{2,1,0:T(8,128)(2,1)S(1)}, bf16[2,24,512]{2,1,0:T(8,128)(2,1)S(1)}, u32[]{:S(2)}, u32[]{:S(2)}) collective-permute-start(bf16[2,24,512]{2,1,0:T(8,128)(2,1)S(1)} %bitcast.84), channel_id=1, source_target_pairs={{0,8},{4,12},{8,0},{12,4},{16,24},{20,28},{24,16},{28,20},{1,9},{5... | collective-permute-start | bytes 147464 | tf_op jit(solution)/shard_map/ppermute | solution.py:20
  57.4 5.0 %collective-permute-start.17 = (bf16[2,24,512]{2,1,0:T(8,128)(2,1)S(1)}, bf16[2,24,512]{2,1,0:T(8,128)(2,1)S(1)}, u32[]{:S(2)}, u32[]{:S(2)}) collective-permute-start(bf16[2,24,512]{2,1,0:T(8,128)(2,1)S(1)} %bitcast.81), channel_id=1, source_target_pairs={{0,16},{4,20},{8,24},{12,28},{16,0},{20,4},{24,8},{28,12},{1,17},{... | collective-permute-start | bytes 147464 | tf_op jit(solution)/shard_map/ppermute | solution.py:20
  58.6 5.9 %collective-permute-start.18 = (bf16[2,24,512]{2,1,0:T(8,128)(2,1)S(1)}, bf16[2,24,512]{2,1,0:T(8,128)(2,1)S(1)}, u32[]{:S(2)}, u32[]{:S(2)}) collective-permute-start(bf16[2,24,512]{2,1,0:T(8,128)(2,1)S(1)} %bitcast.78), channel_id=1, source_target_pairs={{0,24},{4,28},{8,16},{12,20},{16,8},{20,12},{24,0},{28,4},{1,25},{... | collective-permute-start | bytes 147464 | tf_op jit(solution)/shard_map/ppermute | solution.py:20
  64.5 1.4 %collective-permute-start.19 = (bf16[4,24,512]{2,1,0:T(8,128)(2,1)S(1)}, bf16[4,24,512]{2,1,0:T(8,128)(2,1)S(1)}, u32[]{:S(2)}, u32[]{:S(2)}) collective-permute-start(bf16[4,24,512]{2,1,0:T(8,128)(2,1)S(1)} %get-tuple-element.34), channel_id=1, source_target_pairs={{0,4},{4,0},{8,12},{12,8},{16,20},{20,16},{24,28},{28,24},{1,5},{5... | collective-permute-start | bytes 294920 | tf_op jit(solution)/shard_map/ppermute | solution.py:20

commit v4 on v3

--- a/solution.py
+++ b/solution.py
@@ -7,35 +7,39 @@
 from jax.experimental.pallas import tpu as pltpu
 from jax.sharding import PartitionSpec as P
 
+
 norm_eps = 1e-06
 
 
-def partner_swap(value, offset):
-    count = lax.axis_size("tp")
-    return lax.ppermute(value, "tp", [(source, source ^ offset) for source in range(count)])
-
-
-def ep_swap(value, offset):
-    count = lax.axis_size("ep")
-    return lax.ppermute(value, "ep", [(source, source ^ offset) for source in range(count)])
+def swap(value, axis, offset):
+    pairs = [(source, source ^ offset) for source in range(lax.axis_size(axis))]
+    return lax.ppermute(value, axis, pairs)
+
+
+def near_first(count):
+    return sorted(range(1, count), key=lambda offset: (offset.bit_count(), offset))
+
+
+def far_first(count):
+    return sorted(range(1, count), key=lambda offset: (-offset.bit_count(), offset))
 
 
 def to_experts(rows):
     pairs = rows.shape[1]
     near = rows[0]
-    crossed = ep_swap(rows[1], 1)
+    crossed = swap(rows[1], "ep", 1)
     joined = jnp.stack([near, crossed], axis=1)
-    moved = [None] + [ep_swap(joined[step], 2 * step) for step in range(pairs - 1, 0, -1)][::-1]
+    moved = [None] + [swap(joined[step], "ep", 2 * step) for step in range(pairs - 1, 0, -1)][::-1]
     moved[0] = joined[0]
     return jnp.stack(moved, axis=0), joined
 
 
 def from_experts(rows):
     pairs = rows.shape[0]
-    moved = [None] + [ep_swap(rows[step], 2 * step) for step in range(pairs - 1, 0, -1)][::-1]
+    moved = [None] + [swap(rows[step], "ep", 2 * step) for step in range(pairs - 1, 0, -1)][::-1]
     moved[0] = rows[0]
     moved = jnp.stack(moved, axis=1)
-    return jnp.stack([moved[0], ep_swap(moved[1], 1)], axis=0)
+    return moved[0], swap(moved[1], "ep", 1)
 
 
 def lane_sums(values):
@@ -46,61 +50,46 @@
 
 
 def mixer_front(
-    at_ref,
-    gain_ref,
-    log_step_ref,
-    decay_ref,
-    freq_ref,
-    in_re_ref,
-    in_im_ref,
-    out_re_ref,
-    out_im_ref,
-    skip_ref,
-    tokens_hbm,
-    w_in_hbm,
-    state_re_hbm,
-    state_im_hbm,
-    mixed_ref,
-    kept_ref,
-    new_re_ref,
-    new_im_ref,
-    tokens_ref,
-    w_in_ref,
-    state_re_ref,
-    state_im_ref,
-    in_ref,
-    out_ref,
-    split_ref,
-    sems,
+    at_ref, *refs
 ):
+    count = 13
+    sources, (mixed_ref, kept_ref, new_re_ref, new_im_ref) = refs[:count], refs[count : count + 4]
+    targets = refs[count + 4 : 2 * count + 4]
+    in_ref, out_ref, split_ref, sems = refs[2 * count + 4 :]
+    copies = [
+        pltpu.make_async_copy(source, target, sems.at[place])
+        for place, (source, target) in enumerate(zip(sources, targets))
+    ]
+    for copy in copies:
+        copy.start()
+    (
+        tokens_ref, gain_ref, in_re_ref, in_im_ref, log_step_ref, decay_ref, freq_ref, w_in_ref,
+        state_re_ref, state_im_ref, out_re_ref, out_im_ref, skip_ref,
+    ) = targets
     groups, heads, entries = in_re_ref.shape
     seqs, width = tokens_ref.shape
     per_half = min(groups, max(1, 128 // heads))
     lanes = 2 * entries
-    copies = [
-        pltpu.make_async_copy(source, target, sems.at[place])
-        for place, (source, target) in enumerate(
-            (
-                (tokens_hbm, tokens_ref),
-                (w_in_hbm, w_in_ref),
-                (state_re_hbm, state_re_ref),
-                (state_im_hbm, state_im_ref),
-            )
-        )
-    ]
-    for copy in copies:
-        copy.start()
-
     in_ref[...] = jnp.zeros_like(in_ref)
     out_ref[...] = jnp.zeros_like(out_ref)
+    copies[0].wait()
+    copies[1].wait()
+    values = tokens_ref[...].astype(jnp.float32)
+    squares = jnp.sum(lane_sums(values * values), axis=1, keepdims=True)
+    scale = lax.rsqrt(squares / width + norm_eps)
+    normed = (values * scale * gain_ref[...]).astype(jnp.bfloat16)
+    kept = kept_ref.shape[1]
+    kept_ref[...] = tokens_ref[:, pl.ds(pl.multiple_of(at_ref[0] * kept, 128), kept)]
+
+    copies[2].wait()
+    copies[3].wait()
     for g in range(groups):
         rows = pl.ds((g % per_half) * heads, heads)
         in_ref[rows, g * lanes : (g + 1) * lanes] = jnp.concatenate(
             [in_re_ref[g], in_im_ref[g]], axis=1
         )
-        out_ref[rows, g * lanes : (g + 1) * lanes] = jnp.concatenate(
-            [out_re_ref[g], -out_im_ref[g]], axis=1
-        )
+    for copy in copies[4:7]:
+        copy.wait()
 
     diagonal = lax.broadcasted_iota(jnp.int32, (groups, groups), 0) == lax.broadcasted_iota(
         jnp.int32, (groups, groups), 1
@@ -116,6 +105,15 @@
     coef_re = ((turn_re - 1.0) * decay + turn_im * freq) / denom
     coef_im = (turn_im * decay - (turn_re - 1.0) * freq) / denom
 
+    copies[7].wait()
+    drive = jnp.dot(normed, w_in_ref[...], preferred_element_type=jnp.float32).astype(jnp.bfloat16)
+    for copy in copies[8:]:
+        copy.wait()
+    for g in range(groups):
+        rows = pl.ds((g % per_half) * heads, heads)
+        out_ref[rows, g * lanes : (g + 1) * lanes] = jnp.concatenate(
+            [out_re_ref[g], -out_im_ref[g]], axis=1
+        )
     block = per_half * heads
     skip_tiled = jnp.concatenate([skip_ref[...]] * per_half, axis=1)
     owner = lax.broadcasted_iota(jnp.int32, skip_tiled.shape, 1) // heads
@@ -125,17 +123,6 @@
         for start in range(0, groups, per_half)
     ]
 
-    copies[0].wait()
-    values = tokens_ref[...].astype(jnp.float32)
-    squares = jnp.sum(lane_sums(values * values), axis=1, keepdims=True)
-    scale = lax.rsqrt(squares / width + norm_eps)
-    normed = (values * scale * gain_ref[...]).astype(jnp.bfloat16)
-    kept = kept_ref.shape[1]
-    kept_ref[...] = tokens_ref[:, pl.ds(pl.multiple_of(at_ref[0] * kept, 128), kept)]
-    copies[1].wait()
-    drive = jnp.dot(normed, w_in_ref[...], preferred_element_type=jnp.float32).astype(jnp.bfloat16)
-    copies[2].wait()
-    copies[3].wait()
     for half, skip_row in enumerate(skip_rows):
         cols = slice(half * block, (half + 1) * block)
         spans = slice(half * per_half * lanes, (half + 1) * per_half * lanes)
@@ -175,6 +162,10 @@
     groups, heads, entries = in_re.shape
     seqs = tokens.shape[0]
     per_half = min(groups, max(1, 128 // heads))
+    inputs = (
+        tokens, mix_gain[None, :], in_re, in_im, log_step[None, :], decay_re, freq, w_in,
+        state_re, state_im, out_re, out_im, skip,
+    )
     vmem = pl.BlockSpec(memory_space=pltpu.VMEM)
     hbm = pl.BlockSpec(memory_space=pltpu.HBM)
     wide = (per_half * heads, groups * 2 * entries)
@@ -183,33 +174,27 @@
         out_shape=[
             pltpu.VMEM((seqs, groups * heads), jnp.bfloat16),
             pltpu.VMEM((seqs, kept_width), jnp.bfloat16),
-            jax.ShapeDtypeStruct(state_re.shape, jnp.float32),
-            jax.ShapeDtypeStruct(state_im.shape, jnp.float32),
+            pltpu.VMEM(state_re.shape, jnp.float32),
+            pltpu.VMEM(state_im.shape, jnp.float32),
         ],
-        in_specs=[pl.BlockSpec(memory_space=pltpu.SMEM)] + [vmem] * 9 + [hbm] * 4,
+        in_specs=[pl.BlockSpec(memory_space=pltpu.SMEM)] + [hbm] * len(inputs),
         out_specs=[vmem] * 4,
         scratch_shapes=[
-            pltpu.VMEM(tokens.shape, tokens.dtype),
-            pltpu.VMEM(w_in.shape, w_in.dtype),
-            pltpu.VMEM(state_re.shape, state_re.dtype),
-            pltpu.VMEM(state_im.shape, state_im.dtype),
+            *(pltpu.VMEM(value.shape, value.dtype) for value in inputs),
             pltpu.VMEM(wide, jnp.bfloat16),
             pltpu.VMEM(wide, jnp.bfloat16),
             pltpu.VMEM((2 * seqs, wide[1]), jnp.bfloat16),
-            pltpu.SemaphoreType.DMA((4,)),
+            pltpu.SemaphoreType.DMA((len(inputs),)),
         ],
-        compiler_params=pltpu.CompilerParams(vmem_limit_bytes=60 * 1024 * 1024),
+        compiler_params=pltpu.CompilerParams(vmem_limit_bytes=12 * 1024 * 1024),
         cost_estimate=pl.CostEstimate(
             flops=8_000_000_000, bytes_accessed=4_000_000, transcendentals=0
         ),
         name="mixer_front",
-    )(
-        at, mix_gain[None, :], log_step[None, :], decay_re, freq, in_re, in_im, out_re, out_im,
-        skip, tokens, w_in, state_re, state_im,
-    )
-
-
-def fetch_weights(pieces, *refs):
+    )(at, *(pltpu.with_memory_space_constraint(value, pltpu.HBM) for value in inputs))
+
+
+def move_arrays(pieces, *refs):
     count = (len(refs) - 2) // 2
     sources, targets, sems = refs[1 : 1 + count], refs[1 + count : 1 + 2 * count], refs[-1]
     copies = []
@@ -226,21 +211,27 @@
         copy.wait()
 
 
-def fetched(after, *weights):
+def moved(after, fetches, stores=()):
     pieces = 4
+    count = len(fetches) + len(stores)
+    hbm, vmem = pl.BlockSpec(memory_space=pltpu.HBM), pl.BlockSpec(memory_space=pltpu.VMEM)
     return pl.pallas_call(
-        functools.partial(fetch_weights, pieces),
-        out_shape=[pltpu.VMEM(weight.shape, weight.dtype) for weight in weights],
-        in_specs=[pl.BlockSpec(memory_space=pl.ANY)]
-        + [pl.BlockSpec(memory_space=pltpu.HBM)] * len(weights),
-        out_specs=[pl.BlockSpec(memory_space=pltpu.VMEM)] * len(weights),
-        scratch_shapes=[pltpu.SemaphoreType.DMA((pieces * len(weights),))],
+        functools.partial(move_arrays, pieces),
+        out_shape=[pltpu.VMEM(value.shape, value.dtype) for value in fetches]
+        + [pltpu.HBM(value.shape, value.dtype) for value in stores],
+        in_specs=[pl.BlockSpec(memory_space=pl.ANY)] + [hbm] * len(fetches) + [vmem] * len(stores),
+        out_specs=[vmem] * len(fetches) + [hbm] * len(stores),
+        scratch_shapes=[pltpu.SemaphoreType.DMA((pieces * count,))],
         compiler_params=pltpu.CompilerParams(vmem_limit_bytes=1024 * 1024),
         cost_estimate=pl.CostEstimate(
-            flops=1_000_000_000, bytes_accessed=4_000_000 * len(weights), transcendentals=0
+            flops=1_000_000_000, bytes_accessed=4_000_000 * count, transcendentals=0
         ),
-        name="fetch_weights",
-    )(after, *(pltpu.with_memory_space_constraint(weight, pltpu.HBM) for weight in weights))
+        name="move_arrays",
+    )(
+        after,
+        *(pltpu.with_memory_space_constraint(value, pltpu.HBM) for value in fetches),
+        *stores,
+    )
 
 
 def expert_step(first, last, model_width, at_ref, block_ref, gain_ref, gate_ref, up_ref, *rest):
@@ -315,7 +306,6 @@
     expert_down,
 ):
     seq_count = tokens.shape[0]
-    groups_local = decay_re.shape[0]
     model_width = tokens.shape[1]
     shards = lax.axis_size("tp")
     local_width = model_width // shards
@@ -324,7 +314,7 @@
     slot_cap = (3 * seq_count * top_count + 2 * experts - 1) // (2 * experts)
     rows_all = experts * slot_cap
     own = lax.axis_index("tp")
-    offsets = list(range(1, shards))
+    offsets = near_first(shards)
     gate_local = expert_gate[0]
     up_local = expert_up[0]
     down_local = expert_down[0]
@@ -342,7 +332,7 @@
     )
     chan_width = mixed_in.shape[1]
 
-    arrived_mix = [partner_swap(mixed_in, offset) for offset in offsets]
+    arrived_mix = [swap(mixed_in, "tp", offset) for offset in offsets]
     gate = jnp.dot(
         mixed_in, rows_of(glu_weight, 0, chan_width), preferred_element_type=jnp.float32
     )
@@ -352,7 +342,7 @@
         )
     gated = (mixed_in.astype(jnp.float32) * jax.nn.sigmoid(gate + glu_bias)).astype(jnp.bfloat16)
 
-    (down_near,) = fetched(gated, down_local)
+    down_near, new_re, new_im = moved(gated, (down_local,), (new_re, new_im))
 
     def share(offset):
         block = jnp.dot(
@@ -360,7 +350,10 @@
         )
         return block.astype(jnp.bfloat16)
 
-    arrived_shares = [partner_swap(share(offset), offset) for offset in offsets]
+    arrived_shares = []
+    for offset in far_first(shards):
+        block = share(offset)
+        arrived_shares.append(swap(block, "tp", offset))
     mix_part = share(0).astype(jnp.float32)
     for block in arrived_shares:
         mix_part = mix_part + block.astype(jnp.float32)
@@ -382,13 +375,13 @@
     outbound = jnp.dot(select, resid_part, preferred_element_type=jnp.float32).astype(jnp.bfloat16)
     arrived, joined = to_experts(outbound.reshape(2, pairs, slot_cap, local_width))
     arrived = arrived.reshape(rows_all, local_width)
-    gate_near, up_near = fetched(joined, gate_local, up_local)
-    blocks = [(0, arrived)] + [(offset, partner_swap(arrived, offset)) for offset in offsets]
+    gate_near, up_near = moved(joined, (gate_local, up_local))
+    blocks = [(0, arrived)] + [(offset, swap(arrived, "tp", offset)) for offset in offsets]
     held = ()
-    for offset, block in blocks:
+    for place, (offset, block) in enumerate(blocks):
         at = (own ^ offset).astype(jnp.int32).reshape(1)
         held = expert_part(
-            block, at, ffn_gain[None, :], gate_near, up_near, held, offset == shards - 1
+            block, at, ffn_gain[None, :], gate_near, up_near, held, place == shards - 1
         )
     hidden = held[0]
 
@@ -398,20 +391,29 @@
         )
         return block.astype(jnp.bfloat16)
 
-    arrived_results = [partner_swap(result(offset), offset) for offset in offsets]
-    back_rows = result(0).astype(jnp.float32)
+    arrived_results = []
+    for offset in offsets:
+        block = result(offset)
+        arrived_results.append(swap(block, "tp", offset))
+    kept_result = lax.optimization_barrier(result(0))
+    back_rows = kept_result.astype(jnp.float32)
     for block in arrived_results:
         back_rows = back_rows + block.astype(jnp.float32)
-    returned = from_experts(
+    near, crossed = from_experts(
         back_rows.astype(jnp.bfloat16).reshape(pairs, 2, slot_cap, local_width)
-    ).reshape(rows_all, local_width)
-    expert_total = lax.dot_general(
-        combine,
-        returned.astype(jnp.float32),
-        (((1,), (0,)), ((), ())),
-        precision=lax.Precision.HIGHEST,
-    )
-    mixed = (resid_part.astype(jnp.float32) + expert_total).astype(jnp.bfloat16)
+    )
+    half = rows_all // 2
+
+    def weighed(rows, start):
+        return lax.dot_general(
+            combine[:, start : start + half],
+            rows.reshape(half, local_width).astype(jnp.float32),
+            (((1,), (0,)), ((), ())),
+            precision=lax.Precision.HIGHEST,
+        )
+
+    total = lax.optimization_barrier(resid_part.astype(jnp.float32) + weighed(near, 0))
+    mixed = (total + weighed(crossed, half)).astype(jnp.bfloat16)
     return (mixed, new_re, new_im)
 
 

time: 66.9 us -> 64.9 us (0.970)
  waiting for transfers between devices: 22.7 us -> 21.5 us
  Pallas kernels: 13.1 us -> 12.1 us
    pallas_call x1, Pallas kernels: 5.39 us -> 3.93 us  [front(): pl.pallas_call(mixer_front, out_shape=[pltpu.VMEM((seqs, groups * heads),...]
    ppermute x20, waiting for transfers between devices: 22.7 us -> 21.5 us  [swap(): return lax.ppermute(value, axis, pairs)]
  transfers between devices with their start and end apart: 20 -> 20, of which waited for: 17 -> 16; matrix products, arithmetic and copies ran while one was open for 3% -> 4% of each run, Pallas kernels for 10% -> 12%
where the time goes in v4:
time: 64.9 us; the launch traced here: 64.8 us
  starting transfers between devices  24.4 us (38%)
  waiting for transfers between devices  21.5 us (33%)
  Pallas kernels  12.1 us (19%)
  matrix products  4.43 us (7%)
  between operations  1.05 us (2%)
  other arithmetic  0.75 us (1%)
    ppermute x20, starting transfers between devices, swap(): return lax.ppermute(value, axis, pairs)  24.4 us
    ppermute x20, waiting for transfers between devices, swap(): return lax.ppermute(value, axis, pairs)  21.5 us
    pallas_call x2, Pallas kernels, moved(): pl.pallas_call(functools.partial(move_arrays, pieces), out_shape=[pltpu.V...  5.67 us
    pallas_call x1, Pallas kernels, front(): pl.pallas_call(mixer_front, out_shape=[pltpu.VMEM((seqs, groups * heads),...  3.93 us
    pallas_call x4, Pallas kernels, expert_part(): pl.pallas_call(functools.partial(expert_step, not held, last, model_width...  2.46 us
    dot_general x4, matrix products, result(): jnp.dot(hidden, cols_of(down_near, offset, local_width), preferred_elemen...  1.54 us
  transfers between devices with their start and end apart: 20, of which 16 were waited for; matrix products, arithmetic and copies ran while one was open for 4% of the time, Pallas kernels for 12%

profile of v4, /device:TPU:0, one launch (start us, length us, event | category | flops | bytes accessed | tf_op | source)
XLA Modules:
  0.0 64.8 jit_solution(3918037997802309264)
XLA Ops:
  0.7 3.9 %mixer_front.1 = (bf16[64,256]{1,0:T(8,128)(2,1)S(1)}, bf16[64,512]{1,0:T(8,128)(2,1)S(1)}, f32[64,16,64]{2,1,0:T(8,128)S(1)}, f32[64,16,64]{2,1,0:T(8,128)S(1)}) custom-call(s32[1]{0:T(128)} %bitcast.at_ref, bf16[64,2048]{1,0:T(8,128)(2,1)} %refs_0_.1, f32[1,2048]{1,0:T(1,128)} %bitcast.86, bf16[16,16,64]{2,1,0:T(8,128)(2,1)} %refs_2_.1, ...), custom_call_target="tpu_custom_call" | custom-call | flops 8000000000 | bytes 4000000 | tf_op jit(solution)/shard_map/mixer_front/pallas_call | solution.py:172
  4.6 3.0 %collective-permute-start = (bf16[64,256]{1,0:T(8,128)(2,1)S(1)}, bf16[64,256]{1,0:T(8,128)(2,1)S(1)}, u32[]{:S(2)}, u32[]{:S(2)}) collective-permute-start(bf16[64,256]{1,0:T(8,128)(2,1)S(1)} %get-tuple-element.22), channel_id=1, source_target_pairs={{0,1},{1,0},{2,3},{3,2},{4,5},{5,4},{6,7},{7,6},{8,9},{9,8},{10,11... | collective-permute-start | bytes 98312 | tf_op jit(solution)/shard_map/ppermute | solution.py:16
  7.7 1.5 %collective-permute-start.2 = (bf16[64,256]{1,0:T(8,128)(2,1)S(1)}, bf16[64,256]{1,0:T(8,128)(2,1)S(1)}, u32[]{:S(2)}, u32[]{:S(2)}) collective-permute-start(bf16[64,256]{1,0:T(8,128)(2,1)S(1)} %get-tuple-element.22), channel_id=1, source_target_pairs={{0,3},{1,2},{2,1},{3,0},{4,7},{5,6},{6,5},{7,4},{8,11},{9,10},{10,... | collective-permute-start | bytes 98312 | tf_op jit(solution)/shard_map/ppermute | solution.py:16
  10.5 2.0 %collective-permute-done.2 = bf16[64,256]{1,0:T(8,128)(2,1)S(1)} collective-permute-done((bf16[64,256]{1,0:T(8,128)(2,1)S(1)}, bf16[64,256]{1,0:T(8,128)(2,1)S(1)}, u32[]{:S(2)}, u32[]{:S(2)}) %collective-permute-start.2) | collective-permute-done | bytes 32800 | tf_op jit(solution)/shard_map/ppermute | solution.py:16
  12.6 0.5 collective-permute-done.1
  13.5 1.5 %collective-permute-start.3 = (bf16[64,512]{1,0:T(8,128)(2,1)S(1)}, bf16[64,512]{1,0:T(8,128)(2,1)S(1)}, u32[]{:S(2)}, u32[]{:S(2)}) collective-permute-start(bf16[64,512]{1,0:T(8,128)(2,1)S(1)} %convolution_convert_fusion.7), channel_id=1, source_target_pairs={{0,3},{1,2},{2,1},{3,0},{4,7},{5,6},{6,5},{7,4},{8,11},{9,10},{10,... | collective-permute-start | bytes 196616 | tf_op jit(solution)/shard_map/ppermute | solution.py:16
  15.1 1.2 %collective-permute-start.4 = (bf16[64,512]{1,0:T(8,128)(2,1)S(1)}, bf16[64,512]{1,0:T(8,128)(2,1)S(1)}, u32[]{:S(2)}, u32[]{:S(2)}) collective-permute-start(bf16[64,512]{1,0:T(8,128)(2,1)S(1)} %convolution_convert_fusion.6), channel_id=1, source_target_pairs={{0,1},{1,0},{2,3},{3,2},{4,5},{5,4},{6,7},{7,6},{8,9},{9,8},{10,11... | collective-permute-start | bytes 196616 | tf_op jit(solution)/shard_map/ppermute | solution.py:16
  16.5 1.0 %collective-permute-start.5 = (bf16[64,512]{1,0:T(8,128)(2,1)S(1)}, bf16[64,512]{1,0:T(8,128)(2,1)S(1)}, u32[]{:S(2)}, u32[]{:S(2)}) collective-permute-start(bf16[64,512]{1,0:T(8,128)(2,1)S(1)} %convolution_convert_fusion.5), channel_id=1, source_target_pairs={{0,2},{1,3},{2,0},{3,1},{4,6},{5,7},{6,4},{7,5},{8,10},{9,11},{10,... | collective-permute-start | bytes 196616 | tf_op jit(solution)/shard_map/ppermute | solution.py:16
  17.6 1.1 %collective-permute-done.3 = bf16[64,512]{1,0:T(8,128)(2,1)S(1)} collective-permute-done((bf16[64,512]{1,0:T(8,128)(2,1)S(1)}, bf16[64,512]{1,0:T(8,128)(2,1)S(1)}, u32[]{:S(2)}, u32[]{:S(2)}) %collective-permute-start.3) | collective-permute-done | bytes 65568 | tf_op jit(solution)/shard_map/ppermute | solution.py:16
  18.7 0.8 %collective-permute-done.4 = bf16[64,512]{1,0:T(8,128)(2,1)S(1)} collective-permute-done((bf16[64,512]{1,0:T(8,128)(2,1)S(1)}, bf16[64,512]{1,0:T(8,128)(2,1)S(1)}, u32[]{:S(2)}, u32[]{:S(2)}) %collective-permute-start.4) | collective-permute-done | bytes 65568 | tf_op jit(solution)/shard_map/ppermute | solution.py:16
  19.5 1.4 %collective-permute-done.5 = bf16[64,512]{1,0:T(8,128)(2,1)S(1)} collective-permute-done((bf16[64,512]{1,0:T(8,128)(2,1)S(1)}, bf16[64,512]{1,0:T(8,128)(2,1)S(1)}, u32[]{:S(2)}, u32[]{:S(2)}) %collective-permute-start.5) | collective-permute-done | bytes 65568 | tf_op jit(solution)/shard_map/ppermute | solution.py:16
  20.8 0.2 add_convert_fusion.1
  21.0 0.2 convolution_convert_fusion
  21.5 1.2 %collective-permute-done.6 = bf16[4,24,512]{2,1,0:T(8,128)(2,1)S(1)} collective-permute-done((bf16[4,24,512]{2,1,0:T(8,128)(2,1)S(1)}, bf16[4,24,512]{2,1,0:T(8,128)(2,1)S(1)}, u32[]{:S(2)}, u32[]{:S(2)}) %collective-permute-start.6) | collective-permute-done | bytes 98336 | tf_op jit(solution)/shard_map/ppermute | solution.py:16
  22.7 1.6 %collective-permute-start.7 = (bf16[2,24,512]{2,1,0:T(8,128)(2,1)S(1)}, bf16[2,24,512]{2,1,0:T(8,128)(2,1)S(1)}, u32[]{:S(2)}, u32[]{:S(2)}) collective-permute-start(bf16[2,24,512]{2,1,0:T(8,128)(2,1)S(1)} %get-tuple-element.46), channel_id=1, source_target_pairs={{0,8},{4,12},{8,0},{12,4},{16,24},{20,28},{24,16},{28,20},{1,9},{5... | collective-permute-start | bytes 147464 | tf_op jit(solution)/shard_map/ppermute | solution.py:16
  24.3 2.6 %collective-permute-start.8 = (bf16[2,24,512]{2,1,0:T(8,128)(2,1)S(1)}, bf16[2,24,512]{2,1,0:T(8,128)(2,1)S(1)}, u32[]{:S(2)}, u32[]{:S(2)}) collective-permute-start(bf16[2,24,512]{2,1,0:T(8,128)(2,1)S(1)} %get-tuple-element.47), channel_id=1, source_target_pairs={{0,16},{4,20},{8,24},{12,28},{16,0},{20,4},{24,8},{28,12},{1,17},{... | collective-permute-start | bytes 147464 | tf_op jit(solution)/shard_map/ppermute | solution.py:16
  26.9 0.2 collective-permute-start.9
  27.1 2.5 %move_arrays.3 = (bf16[896,2048]{1,0:T(8,128)(2,1)S(1)}, f32[64,16,64]{2,1,0:T(8,128)}, f32[64,16,64]{2,1,0:T(8,128)}) custom-call(bf16[64,256]{1,0:T(8,128)(2,1)S(1)} %fusion.9.refs_0_, bf16[896,2048]{1,0:T(8,128)(2,1)} %bitcast.65, f32[64,16,64]{2,1,0:T(8,128)S(1)} %get-tuple-element.34.refs_2_, f32[64,16,64]{2,1,0:T(8,128)S(1)} %get-tuple-element.35.refs_3_), custom_call_target="tpu_custom_call" | custom-call | flops 1000000000 | bytes 12000000 | tf_op jit(solution)/shard_map/move_arrays/pallas_call | solution.py:218
  29.7 0.5 collective-permute-done.8
  30.2 2.6 %collective-permute-done.9 = bf16[2,24,512]{2,1,0:T(8,128)(2,1)S(1)} collective-permute-done((bf16[2,24,512]{2,1,0:T(8,128)(2,1)S(1)}, bf16[2,24,512]{2,1,0:T(8,128)(2,1)S(1)}, u32[]{:S(2)}, u32[]{:S(2)}) %collective-permute-start.9) | collective-permute-done | bytes 49184 | tf_op jit(solution)/shard_map/ppermute | solution.py:16
  32.8 1.0 %collective-permute-start.12 = (bf16[192,512]{1,0:T(8,128)(2,1)S(1)}, bf16[192,512]{1,0:T(8,128)(2,1)S(1)}, u32[]{:S(2)}, u32[]{:S(2)}) collective-permute-start(bf16[192,512]{1,0:T(8,128)(2,1)S(1)} %bitcast.55), channel_id=1, source_target_pairs={{0,1},{1,0},{2,3},{3,2},{4,5},{5,4},{6,7},{7,6},{8,9},{9,8},{10,11... | collective-permute-start | bytes 589832 | tf_op jit(solution)/shard_map/ppermute | solution.py:16
  33.8 1.5 %collective-permute-start.11 = (bf16[192,512]{1,0:T(8,128)(2,1)S(1)}, bf16[192,512]{1,0:T(8,128)(2,1)S(1)}, u32[]{:S(2)}, u32[]{:S(2)}) collective-permute-start(bf16[192,512]{1,0:T(8,128)(2,1)S(1)} %bitcast.56), channel_id=1, source_target_pairs={{0,2},{1,3},{2,0},{3,1},{4,6},{5,7},{6,4},{7,5},{8,10},{9,11},{10,... | collective-permute-start | bytes 589832 | tf_op jit(solution)/shard_map/ppermute | solution.py:16
  35.3 1.1 %collective-permute-start.10 = (bf16[192,512]{1,0:T(8,128)(2,1)S(1)}, bf16[192,512]{1,0:T(8,128)(2,1)S(1)}, u32[]{:S(2)}, u32[]{:S(2)}) collective-permute-start(bf16[192,512]{1,0:T(8,128)(2,1)S(1)} %bitcast.57), channel_id=1, source_target_pairs={{0,3},{1,2},{2,1},{3,0},{4,7},{5,6},{6,5},{7,4},{8,11},{9,10},{10,... | collective-permute-start | bytes 589832 | tf_op jit(solution)/shard_map/ppermute | solution.py:16
  36.4 3.2 %move_arrays.2 = (bf16[2048,896]{1,0:T(8,128)(2,1)S(1)}, bf16[2048,896]{1,0:T(8,128)(2,1)S(1)}) custom-call(bf16[4,2,24,512]{3,2,1,0:T(8,128)(2,1)S(1)} %pad_maximum_fusion.refs_0_, bf16[2048,896]{1,0:T(8,128)(2,1)} %bitcast.63, bf16[2048,896]{1,0:T(8,128)(2,1)} %bitcast.64), custom_call_target="tpu_custom_call" | custom-call | flops 1000000000 | bytes 8000000 | tf_op jit(solution)/shard_map/move_arrays/pallas_call | solution.py:218
  39.6 0.6 expert_part.3
  40.3 0.6 expert_part.4
  40.9 2.4 %collective-permute-done.11.block_ref = bf16[192,512]{1,0:T(8,128)(2,1)S(1)} collective-permute-done((bf16[192,512]{1,0:T(8,128)(2,1)S(1)}, bf16[192,512]{1,0:T(8,128)(2,1)S(1)}, u32[]{:S(2)}, u32[]{:S(2)}) %collective-permute-start.11) | collective-permute-done | bytes 196640 | tf_op jit(solution)/shard_map/ppermute | solution.py:16
  43.3 0.6 expert_part.5
  43.9 0.7 %expert_last.1 = bf16[192,896]{1,0:T(8,128)(2,1)S(1)} custom-call(s32[1]{0:T(128)} %bitcast.5.at_ref, bf16[192,512]{1,0:T(8,128)(2,1)S(1)} %collective-permute-done.10.block_ref, f32[1,2048]{1,0:T(1,128)S(1)} %bitcast.62, bf16[2048,896]{1,0:T(8,128)(2,1)S(1)} %get-tuple-element.23.gate_ref, bf16[2048,896]{1,0:T(8,128)(2,1)S(1)} %get-tuple-element.24.up_ref, ...), custom_call_target="tpu_custom_call" | custom-call | flops 352321536 | bytes 1835008 | tf_op jit(solution)/shard_map/expert_last/pallas_call | solution.py:269
  44.6 0.4 convolution_convert_fusion.3
  45.0 0.4 convolution_convert_fusion.2
  45.4 0.4 convolution_convert_fusion.1
  45.8 0.5 collective-permute-start.13
  46.3 1.4 %collective-permute-start.14 = (bf16[192,512]{1,0:T(8,128)(2,1)S(1)}, bf16[192,512]{1,0:T(8,128)(2,1)S(1)}, u32[]{:S(2)}, u32[]{:S(2)}) collective-permute-start(bf16[192,512]{1,0:T(8,128)(2,1)S(1)} %convolution_convert_fusion.2), channel_id=1, source_target_pairs={{0,2},{1,3},{2,0},{3,1},{4,6},{5,7},{6,4},{7,5},{8,10},{9,11},{10,... | collective-permute-start | bytes 589832 | tf_op jit(solution)/shard_map/ppermute | solution.py:16
  47.6 1.7 %collective-permute-start.15 = (bf16[192,512]{1,0:T(8,128)(2,1)S(1)}, bf16[192,512]{1,0:T(8,128)(2,1)S(1)}, u32[]{:S(2)}, u32[]{:S(2)}) collective-permute-start(bf16[192,512]{1,0:T(8,128)(2,1)S(1)} %convolution_convert_fusion.1), channel_id=1, source_target_pairs={{0,3},{1,2},{2,1},{3,0},{4,7},{5,6},{6,5},{7,4},{8,11},{9,10},{10,... | collective-permute-start | bytes 589832 | tf_op jit(solution)/shard_map/ppermute | solution.py:16
  49.3 0.4 convolution_convert_fusion.4
  49.7 1.8 %collective-permute-done.13 = bf16[192,512]{1,0:T(8,128)(2,1)S(1)} collective-permute-done((bf16[192,512]{1,0:T(8,128)(2,1)S(1)}, bf16[192,512]{1,0:T(8,128)(2,1)S(1)}, u32[]{:S(2)}, u32[]{:S(2)}) %collective-permute-start.13) | collective-permute-done | bytes 196640 | tf_op jit(solution)/shard_map/ppermute | solution.py:16
  51.5 1.4 %collective-permute-done.14 = bf16[192,512]{1,0:T(8,128)(2,1)S(1)} collective-permute-done((bf16[192,512]{1,0:T(8,128)(2,1)S(1)}, bf16[192,512]{1,0:T(8,128)(2,1)S(1)}, u32[]{:S(2)}, u32[]{:S(2)}) %collective-permute-start.14) | collective-permute-done | bytes 196640 | tf_op jit(solution)/shard_map/ppermute | solution.py:16
  52.9 1.4 %collective-permute-done.15 = bf16[192,512]{1,0:T(8,128)(2,1)S(1)} collective-permute-done((bf16[192,512]{1,0:T(8,128)(2,1)S(1)}, bf16[192,512]{1,0:T(8,128)(2,1)S(1)}, u32[]{:S(2)}, u32[]{:S(2)}) %collective-permute-start.15) | collective-permute-done | bytes 196640 | tf_op jit(solution)/shard_map/ppermute | solution.py:16
  54.4 1.2 %collective-permute-start.16 = (bf16[2,24,512]{2,1,0:T(8,128)(2,1)S(1)}, bf16[2,24,512]{2,1,0:T(8,128)(2,1)S(1)}, u32[]{:S(2)}, u32[]{:S(2)}) collective-permute-start(bf16[2,24,512]{2,1,0:T(8,128)(2,1)S(1)} %bitcast.83), channel_id=1, source_target_pairs={{0,8},{4,12},{8,0},{12,4},{16,24},{20,28},{24,16},{28,20},{1,9},{5... | collective-permute-start | bytes 147464 | tf_op jit(solution)/shard_map/ppermute | solution.py:16
  55.6 1.0 %collective-permute-start.17 = (bf16[2,24,512]{2,1,0:T(8,128)(2,1)S(1)}, bf16[2,24,512]{2,1,0:T(8,128)(2,1)S(1)}, u32[]{:S(2)}, u32[]{:S(2)}) collective-permute-start(bf16[2,24,512]{2,1,0:T(8,128)(2,1)S(1)} %bitcast.80), channel_id=1, source_target_pairs={{0,16},{4,20},{8,24},{12,28},{16,0},{20,4},{24,8},{28,12},{1,17},{... | collective-permute-start | bytes 147464 | tf_op jit(solution)/shard_map/ppermute | solution.py:16
  56.6 2.3 %collective-permute-start.18 = (bf16[2,24,512]{2,1,0:T(8,128)(2,1)S(1)}, bf16[2,24,512]{2,1,0:T(8,128)(2,1)S(1)}, u32[]{:S(2)}, u32[]{:S(2)}) collective-permute-start(bf16[2,24,512]{2,1,0:T(8,128)(2,1)S(1)} %bitcast.77), channel_id=1, source_target_pairs={{0,24},{4,28},{8,16},{12,20},{16,8},{20,12},{24,0},{28,4},{1,25},{... | collective-permute-start | bytes 147464 | tf_op jit(solution)/shard_map/ppermute | solution.py:16
  58.9 0.2 fusion.18
  59.1 2.0 %collective-permute-done.17 = bf16[2,24,512]{2,1,0:T(8,128)(2,1)S(1)} collective-permute-done((bf16[2,24,512]{2,1,0:T(8,128)(2,1)S(1)}, bf16[2,24,512]{2,1,0:T(8,128)(2,1)S(1)}, u32[]{:S(2)}, u32[]{:S(2)}) %collective-permute-start.17) | collective-permute-done | bytes 49184 | tf_op jit(solution)/shard_map/ppermute | solution.py:16
  61.1 1.4 %collective-permute-done.18 = bf16[2,24,512]{2,1,0:T(8,128)(2,1)S(1)} collective-permute-done((bf16[2,24,512]{2,1,0:T(8,128)(2,1)S(1)}, bf16[2,24,512]{2,1,0:T(8,128)(2,1)S(1)}, u32[]{:S(2)}, u32[]{:S(2)}) %collective-permute-start.18) | collective-permute-done | bytes 49184 | tf_op jit(solution)/shard_map/ppermute | solution.py:16
  62.6 0.2 convert_add_fusion
  62.8 1.1 %collective-permute-done.19 = bf16[4,24,512]{2,1,0:T(8,128)(2,1)S(1)} collective-permute-done((bf16[4,24,512]{2,1,0:T(8,128)(2,1)S(1)}, bf16[4,24,512]{2,1,0:T(8,128)(2,1)S(1)}, u32[]{:S(2)}, u32[]{:S(2)}) %collective-permute-start.19) | collective-permute-done | bytes 98336 | tf_op jit(solution)/shard_map/ppermute | solution.py:16
  63.9 0.9 %fusion = bf16[64,512]{1,0:T(8,128)(2,1)} fusion(f32[64,512]{1,0:T(8,128)S(1)} %convert_add_fusion, bf16[96,512]{1,0:T(8,128)(2,1)S(1)} %bitcast.74, f32[64,192]{1,0:T(8,128)S(1)} %bitcast.72), kind=kOutput, calls=%fused_computation.6 | convolution fusion | flops 37814272 | bytes 327680 | tf_op jit(solution)/shard_map/dot_general | solution.py:408
  (46 shorter events, 2.8 us)
Async XLA Ops:
  0.6 12.6 %copy-start = (bf16[256,2048]{1,0:T(8,128)(2,1)S(1)}, bf16[256,2048]{1,0:T(8,128)(2,1)}, u32[]{:S(2)}) copy-start(bf16[256,2048]{1,0:T(8,128)(2,1)} %param.37) | copy-start | bytes 3145732
  0.7 8.6 %copy-start.3 = (s32[64,2]{0,1:T(2,128)S(1)}, s32[64,2]{0,1:T(2,128)}, u32[]{:S(2)}) copy-start(s32[64,2]{0,1:T(2,128)} %param.39) | copy-start | bytes 1540
  0.7 9.5 %copy-start.2 = (bf16[1024,256]{1,0:T(8,128)(2,1)S(1)}, bf16[1024,256]{1,0:T(8,128)(2,1)}, u32[]{:S(2)}) copy-start(bf16[1024,256]{1,0:T(8,128)(2,1)} %param.35) | copy-start | bytes 1572868
  0.7 12.4 %copy-start.5 = (f32[256]{0:T(256)S(1)}, f32[256]{0:T(256)}, u32[]{:S(2)}) copy-start(f32[256]{0:T(256)} %param.36) | copy-start | bytes 3076
  4.6 16.7 %copy-start.4 = (f32[64,2]{0,1:T(2,128)S(1)}, f32[64,2]{0,1:T(2,128)}, u32[]{:S(2)}) copy-start(f32[64,2]{0,1:T(2,128)} %param.40) | copy-start | bytes 1540
  4.6 5.7 %collective-permute-start = (bf16[64,256]{1,0:T(8,128)(2,1)S(1)}, bf16[64,256]{1,0:T(8,128)(2,1)S(1)}, u32[]{:S(2)}, u32[]{:S(2)}) collective-permute-start(bf16[64,256]{1,0:T(8,128)(2,1)S(1)} %get-tuple-element.22), channel_id=1, source_target_pairs={{0,1},{1,0},{2,3},{3,2},{4,5},{5,4},{6,7},{7,6},{8,9},{9,8},{10,11... | collective-permute-start | bytes 98312 | tf_op jit(solution)/shard_map/ppermute | solution.py:16
  7.7 4.8 %collective-permute-start.2 = (bf16[64,256]{1,0:T(8,128)(2,1)S(1)}, bf16[64,256]{1,0:T(8,128)(2,1)S(1)}, u32[]{:S(2)}, u32[]{:S(2)}) collective-permute-start(bf16[64,256]{1,0:T(8,128)(2,1)S(1)} %get-tuple-element.22), channel_id=1, source_target_pairs={{0,3},{1,2},{2,1},{3,0},{4,7},{5,6},{6,5},{7,4},{8,11},{9,10},{10,... | collective-permute-start | bytes 98312 | tf_op jit(solution)/shard_map/ppermute | solution.py:16
  9.2 3.9 %collective-permute-start.1 = (bf16[64,256]{1,0:T(8,128)(2,1)S(1)}, bf16[64,256]{1,0:T(8,128)(2,1)S(1)}, u32[]{:S(2)}, u32[]{:S(2)}) collective-permute-start(bf16[64,256]{1,0:T(8,128)(2,1)S(1)} %get-tuple-element.22), channel_id=1, source_target_pairs={{0,2},{1,3},{2,0},{3,1},{4,6},{5,7},{6,4},{7,5},{8,10},{9,11},{10,... | collective-permute-start | bytes 98312 | tf_op jit(solution)/shard_map/ppermute | solution.py:16
  13.5 5.2 %collective-permute-start.3 = (bf16[64,512]{1,0:T(8,128)(2,1)S(1)}, bf16[64,512]{1,0:T(8,128)(2,1)S(1)}, u32[]{:S(2)}, u32[]{:S(2)}) collective-permute-start(bf16[64,512]{1,0:T(8,128)(2,1)S(1)} %convolution_convert_fusion.7), channel_id=1, source_target_pairs={{0,3},{1,2},{2,1},{3,0},{4,7},{5,6},{6,5},{7,4},{8,11},{9,10},{10,... | collective-permute-start | bytes 196616 | tf_op jit(solution)/shard_map/ppermute | solution.py:16
  15.1 4.3 %collective-permute-start.4 = (bf16[64,512]{1,0:T(8,128)(2,1)S(1)}, bf16[64,512]{1,0:T(8,128)(2,1)S(1)}, u32[]{:S(2)}, u32[]{:S(2)}) collective-permute-start(bf16[64,512]{1,0:T(8,128)(2,1)S(1)} %convolution_convert_fusion.6), channel_id=1, source_target_pairs={{0,1},{1,0},{2,3},{3,2},{4,5},{5,4},{6,7},{7,6},{8,9},{9,8},{10,11... | collective-permute-start | bytes 196616 | tf_op jit(solution)/shard_map/ppermute | solution.py:16
  16.5 4.3 %collective-permute-start.5 = (bf16[64,512]{1,0:T(8,128)(2,1)S(1)}, bf16[64,512]{1,0:T(8,128)(2,1)S(1)}, u32[]{:S(2)}, u32[]{:S(2)}) collective-permute-start(bf16[64,512]{1,0:T(8,128)(2,1)S(1)} %convolution_convert_fusion.5), channel_id=1, source_target_pairs={{0,2},{1,3},{2,0},{3,1},{4,6},{5,7},{6,4},{7,5},{8,10},{9,11},{10,... | collective-permute-start | bytes 196616 | tf_op jit(solution)/shard_map/ppermute | solution.py:16
  21.3 1.4 %collective-permute-start.6 = (bf16[4,24,512]{2,1,0:T(8,128)(2,1)S(1)}, bf16[4,24,512]{2,1,0:T(8,128)(2,1)S(1)}, u32[]{:S(2)}, u32[]{:S(2)}) collective-permute-start(bf16[4,24,512]{2,1,0:T(8,128)(2,1)S(1)} %bitcast.75), channel_id=1, source_target_pairs={{0,4},{4,0},{8,12},{12,8},{16,20},{20,16},{24,28},{28,24},{1,5},{5... | collective-permute-start | bytes 294920 | tf_op jit(solution)/shard_map/ppermute | solution.py:16
  22.7 7.0 %collective-permute-start.7 = (bf16[2,24,512]{2,1,0:T(8,128)(2,1)S(1)}, bf16[2,24,512]{2,1,0:T(8,128)(2,1)S(1)}, u32[]{:S(2)}, u32[]{:S(2)}) collective-permute-start(bf16[2,24,512]{2,1,0:T(8,128)(2,1)S(1)} %get-tuple-element.46), channel_id=1, source_target_pairs={{0,8},{4,12},{8,0},{12,4},{16,24},{20,28},{24,16},{28,20},{1,9},{5... | collective-permute-start | bytes 147464 | tf_op jit(solution)/shard_map/ppermute | solution.py:16
  24.3 5.9 %collective-permute-start.8 = (bf16[2,24,512]{2,1,0:T(8,128)(2,1)S(1)}, bf16[2,24,512]{2,1,0:T(8,128)(2,1)S(1)}, u32[]{:S(2)}, u32[]{:S(2)}) collective-permute-start(bf16[2,24,512]{2,1,0:T(8,128)(2,1)S(1)} %get-tuple-element.47), channel_id=1, source_target_pairs={{0,16},{4,20},{8,24},{12,28},{16,0},{20,4},{24,8},{28,12},{1,17},{... | collective-permute-start | bytes 147464 | tf_op jit(solution)/shard_map/ppermute | solution.py:16
  26.9 5.9 %collective-permute-start.9 = (bf16[2,24,512]{2,1,0:T(8,128)(2,1)S(1)}, bf16[2,24,512]{2,1,0:T(8,128)(2,1)S(1)}, u32[]{:S(2)}, u32[]{:S(2)}) collective-permute-start(bf16[2,24,512]{2,1,0:T(8,128)(2,1)S(1)} %get-tuple-element.48), channel_id=1, source_target_pairs={{0,24},{4,28},{8,16},{12,20},{16,8},{20,12},{24,0},{28,4},{1,25},{... | collective-permute-start | bytes 147464 | tf_op jit(solution)/shard_map/ppermute | solution.py:16
  32.8 7.4 %collective-permute-start.12 = (bf16[192,512]{1,0:T(8,128)(2,1)S(1)}, bf16[192,512]{1,0:T(8,128)(2,1)S(1)}, u32[]{:S(2)}, u32[]{:S(2)}) collective-permute-start(bf16[192,512]{1,0:T(8,128)(2,1)S(1)} %bitcast.55), channel_id=1, source_target_pairs={{0,1},{1,0},{2,3},{3,2},{4,5},{5,4},{6,7},{7,6},{8,9},{9,8},{10,11... | collective-permute-start | bytes 589832 | tf_op jit(solution)/shard_map/ppermute | solution.py:16
  33.8 9.5 %collective-permute-start.11 = (bf16[192,512]{1,0:T(8,128)(2,1)S(1)}, bf16[192,512]{1,0:T(8,128)(2,1)S(1)}, u32[]{:S(2)}, u32[]{:S(2)}) collective-permute-start(bf16[192,512]{1,0:T(8,128)(2,1)S(1)} %bitcast.56), channel_id=1, source_target_pairs={{0,2},{1,3},{2,0},{3,1},{4,6},{5,7},{6,4},{7,5},{8,10},{9,11},{10,... | collective-permute-start | bytes 589832 | tf_op jit(solution)/shard_map/ppermute | solution.py:16
  35.3 8.6 %collective-permute-start.10 = (bf16[192,512]{1,0:T(8,128)(2,1)S(1)}, bf16[192,512]{1,0:T(8,128)(2,1)S(1)}, u32[]{:S(2)}, u32[]{:S(2)}) collective-permute-start(bf16[192,512]{1,0:T(8,128)(2,1)S(1)} %bitcast.57), channel_id=1, source_target_pairs={{0,3},{1,2},{2,1},{3,0},{4,7},{5,6},{6,5},{7,4},{8,11},{9,10},{10,... | collective-permute-start | bytes 589832 | tf_op jit(solution)/shard_map/ppermute | solution.py:16
  36.4 3.2 %copy-start.1 = (f32[2048]{0:T(1024)S(1)}, f32[2048]{0:T(1024)}, u32[]{:S(2)}) copy-start(f32[2048]{0:T(1024)} %param.38) | copy-start | bytes 24580
  45.8 5.7 %collective-permute-start.13 = (bf16[192,512]{1,0:T(8,128)(2,1)S(1)}, bf16[192,512]{1,0:T(8,128)(2,1)S(1)}, u32[]{:S(2)}, u32[]{:S(2)}) collective-permute-start(bf16[192,512]{1,0:T(8,128)(2,1)S(1)} %convolution_convert_fusion.3), channel_id=1, source_target_pairs={{0,1},{1,0},{2,3},{3,2},{4,5},{5,4},{6,7},{7,6},{8,9},{9,8},{10,11... | collective-permute-start | bytes 589832 | tf_op jit(solution)/shard_map/ppermute | solution.py:16
  46.3 6.7 %collective-permute-start.14 = (bf16[192,512]{1,0:T(8,128)(2,1)S(1)}, bf16[192,512]{1,0:T(8,128)(2,1)S(1)}, u32[]{:S(2)}, u32[]{:S(2)}) collective-permute-start(bf16[192,512]{1,0:T(8,128)(2,1)S(1)} %convolution_convert_fusion.2), channel_id=1, source_target_pairs={{0,2},{1,3},{2,0},{3,1},{4,6},{5,7},{6,4},{7,5},{8,10},{9,11},{10,... | collective-permute-start | bytes 589832 | tf_op jit(solution)/shard_map/ppermute | solution.py:16
  47.6 6.7 %collective-permute-start.15 = (bf16[192,512]{1,0:T(8,128)(2,1)S(1)}, bf16[192,512]{1,0:T(8,128)(2,1)S(1)}, u32[]{:S(2)}, u32[]{:S(2)}) collective-permute-start(bf16[192,512]{1,0:T(8,128)(2,1)S(1)} %convolution_convert_fusion.1), channel_id=1, source_target_pairs={{0,3},{1,2},{2,1},{3,0},{4,7},{5,6},{6,5},{7,4},{8,11},{9,10},{10,... | collective-permute-start | bytes 589832 | tf_op jit(solution)/shard_map/ppermute | solution.py:16
  54.4 4.7 %collective-permute-start.16 = (bf16[2,24,512]{2,1,0:T(8,128)(2,1)S(1)}, bf16[2,24,512]{2,1,0:T(8,128)(2,1)S(1)}, u32[]{:S(2)}, u32[]{:S(2)}) collective-permute-start(bf16[2,24,512]{2,1,0:T(8,128)(2,1)S(1)} %bitcast.83), channel_id=1, source_target_pairs={{0,8},{4,12},{8,0},{12,4},{16,24},{20,28},{24,16},{28,20},{1,9},{5... | collective-permute-start | bytes 147464 | tf_op jit(solution)/shard_map/ppermute | solution.py:16
  55.6 5.5 %collective-permute-start.17 = (bf16[2,24,512]{2,1,0:T(8,128)(2,1)S(1)}, bf16[2,24,512]{2,1,0:T(8,128)(2,1)S(1)}, u32[]{:S(2)}, u32[]{:S(2)}) collective-permute-start(bf16[2,24,512]{2,1,0:T(8,128)(2,1)S(1)} %bitcast.80), channel_id=1, source_target_pairs={{0,16},{4,20},{8,24},{12,28},{16,0},{20,4},{24,8},{28,12},{1,17},{... | collective-permute-start | bytes 147464 | tf_op jit(solution)/shard_map/ppermute | solution.py:16
  56.6 5.9 %collective-permute-start.18 = (bf16[2,24,512]{2,1,0:T(8,128)(2,1)S(1)}, bf16[2,24,512]{2,1,0:T(8,128)(2,1)S(1)}, u32[]{:S(2)}, u32[]{:S(2)}) collective-permute-start(bf16[2,24,512]{2,1,0:T(8,128)(2,1)S(1)} %bitcast.77), channel_id=1, source_target_pairs={{0,24},{4,28},{8,16},{12,20},{16,8},{20,12},{24,0},{28,4},{1,25},{... | collective-permute-start | bytes 147464 | tf_op jit(solution)/shard_map/ppermute | solution.py:16
  62.5 1.4 %collective-permute-start.19 = (bf16[4,24,512]{2,1,0:T(8,128)(2,1)S(1)}, bf16[4,24,512]{2,1,0:T(8,128)(2,1)S(1)}, u32[]{:S(2)}, u32[]{:S(2)}) collective-permute-start(bf16[4,24,512]{2,1,0:T(8,128)(2,1)S(1)} %get-tuple-element.39), channel_id=1, source_target_pairs={{0,4},{4,0},{8,12},{12,8},{16,20},{20,16},{24,28},{28,24},{1,5},{5... | collective-permute-start | bytes 294920 | tf_op jit(solution)/shard_map/ppermute | solution.py:16
